TPU v7x, 512 devices: a whole 4x4x16 slice. The times are simulated.
512 devices in a mesh: sp: 64 (over z, y), tp: 8 (over x, core).
Axes of the slice: x: 4, y: 4, z: 16, core: 2. Of those that a mesh axis runs over, the one named last changes fastest.
Arguments:
- block_source: bfloat16 [8192, 2048], P('sp'), may hold values from -28 to 28
- address_weights: bfloat16 [1024, 2048], P('tp'), may hold values from -0.125 to 0.125
- causal_filter_taps: float32 [4, 1024], P(None, 'tp'), may hold values from -3 to 3
- payload_vectors: bfloat16 [8192, 2048], P('sp', 'tp'), may hold values from -0.125 to 0.125
- probe_vectors: bfloat16 [8192, 1024], P('sp', 'tp'), may hold values from -0.5 to 0.5
- interval_preimage: float32 [8192, 32], P('sp', 'tp'), may hold values from -3.5 to 4
- channel_damping_exponent: float32 [32], P('tp'), may hold values from -14 to -3
- added_damping_jumps: float32 [8192, 32], P('sp', 'tp'), may hold values from -1 to 0
- sigmoid_argument: bfloat16 [8192, 2048], P('sp', 'tp'), may hold values from -6 to 6
- adjoint_of_result: bfloat16 [8192, 2048], P('sp', 'tp'), may hold values from -6 to 6
Outputs:
- key_weight_grad: float32 [1024, 2048], P('tp', 'sp')
- row_squares: float32 [1024], P('tp')
- input_grad: bfloat16 [2048, 8192], P('tp', 'sp')
- value_grad: bfloat16 [8192, 2048], P('sp', 'tp')
- query_grad: bfloat16 [8192, 1024], P('sp', 'tp')
- decay_grad: float32 [8192, 32], P('sp', 'tp')
- gate_grad: bfloat16 [8192, 2048], P('sp', 'tp')
All inputs are finite; a program needn't handle non-finite values.
Results may differ from a plain program's by a relative error of at most 0.015.
Values may be sent and summed in bfloat16 or wider, within the bound.
No kernel may reach another device: no remote copies, remote signals or barrier semaphores. Data moves between devices by JAX's collectives and lax.ppermute only.
A program may use at most 64 MiB of HBM per device.

v0:
```python
import jax
import jax.numpy as jnp
from jax import lax
from jax.sharding import PartitionSpec as P

STATE = 128
BLOCK = 128


HIGHEST = lax.Precision.HIGHEST


def from_partner(block, axis, bit):
    count = lax.axis_size(axis)
    route = []
    for low in range(count):
        high = low | 1 << bit
        if high != low and high < count:
            route += [(low, high), (high, low)]
    return lax.ppermute(block, axis, route)


def from_behind(block, axis, distance):
    devices = range(lax.axis_size(axis))
    route = [(i - distance, i) for i in devices if i - distance in devices]
    return lax.ppermute(block, axis, route)


def cut_along(shard, dim, peers):
    shape = shard.shape
    parts = shard.reshape(*shape[:dim], peers, shape[dim] // peers, *shape[dim + 1 :])
    return jnp.moveaxis(parts, dim, 0)


def summed_on_arrival(shard, axis, dim):
    peers = lax.axis_size(axis)
    parts = lax.all_to_all(cut_along(shard, dim, peers), axis, 0, 0, tiled=True)
    return jnp.sum(parts.astype(jnp.float32), axis=0)


def sent_to_all(shard, axis):
    copies = jnp.broadcast_to(shard, (lax.axis_size(axis), *shard.shape))
    return lax.all_to_all(copies, axis, split_axis=0, concat_axis=0, tiled=True)


def joined_along(parts, dim):
    shape = list(parts.shape[1:])
    shape[dim] *= parts.shape[0]
    return jnp.moveaxis(parts, 0, dim).reshape(shape)


def collect(shard, axis, dim):
    parts = sent_to_all(shard, axis)
    return joined_along(parts, dim)


def silu_slope(pre_act):
    sigma = jax.nn.sigmoid(pre_act)
    return sigma * (1.0 + pre_act * (1.0 - sigma))


def causal_conv(padded, causal_filter_taps, tokens):
    result = causal_filter_taps[0][None] * padded[0:tokens]
    for offset in range(1, causal_filter_taps.shape[0]):
        result = result + causal_filter_taps[offset][None] * padded[offset : offset + tokens]
    return result


def conv_transpose(extended, causal_filter_taps, tokens):
    tap_count = causal_filter_taps.shape[0]
    result = causal_filter_taps[0][None] * extended[tap_count - 1 : tap_count - 1 + tokens]
    for offset in range(1, tap_count):
        first_row = tap_count - 1 - offset
        result = (
            result + causal_filter_taps[offset][None] * extended[first_row : first_row + tokens]
        )
    return result


def block_step(carry_state, inputs):
    payload_vectors, damping_exponent, key_block, probe_vectors, step_block, scores = inputs
    block_len = payload_vectors.shape[0]
    scaled = payload_vectors * step_block[..., None]
    cumulative = jnp.cumsum(damping_exponent, axis=0)
    causal = jnp.tril(jnp.ones((block_len, block_len), dtype=bool))
    gaps = cumulative[:, None] - cumulative[None, :]
    decay_mat = jnp.exp(jnp.where(causal[:, :, None, None], gaps, -jnp.inf))
    within = jnp.einsum("gij,ijgr,jgrp->igrp", scores, decay_mat, scaled, precision=HIGHEST)
    carried = (
        jnp.einsum("ign,grpn->igrp", probe_vectors, carry_state, precision=HIGHEST)
        * jnp.exp(cumulative)[..., None]
    )
    end_decay = cumulative[-1]
    weights = jnp.exp(end_decay[None] - cumulative)
    new_state = carry_state * jnp.exp(end_decay)[..., None, None] + jnp.einsum(
        "jgn,jgr,jgrp->grpn", key_block, weights, scaled, precision=HIGHEST
    )
    return (new_state, within + carried)


def linear_scan_update(
    payload_vectors,
    interval_preimage,
    pooled_addresses,
    pooled_probes,
    blocked_scores,
    starting_memory,
    channel_damping_exponent,
    added_damping_jumps,
):
    tokens = pooled_addresses.shape[0]
    groups = pooled_addresses.shape[1]
    head_count = interval_preimage.shape[1]
    group_heads = head_count // groups
    block_count = tokens // BLOCK
    interval_widths = jax.nn.softplus(interval_preimage)
    damping_exponent = (
        added_damping_jumps - jnp.exp(channel_damping_exponent)[None] * interval_widths
    )

    def to_blocks(array):
        return array.reshape((block_count, BLOCK) + array.shape[1:])

    final_state, outputs = lax.scan(
        block_step,
        starting_memory,
        (
            to_blocks(payload_vectors.reshape(tokens, groups, group_heads, -1)),
            to_blocks(damping_exponent.reshape(tokens, groups, group_heads)),
            to_blocks(pooled_addresses),
            to_blocks(pooled_probes),
            to_blocks(interval_widths.reshape(tokens, groups, group_heads)),
            blocked_scores,
        ),
    )
    return (outputs.reshape(tokens, -1), final_state)


def join_carry(earlier, later):
    return (earlier[0] + later[0], earlier[1] * jnp.exp(later[0])[..., None, None] + later[1])


def pair_chains(span_decay, fwd_span, bwd_span):
    my_index = lax.axis_index("sp")
    levels = lax.axis_size("sp").bit_length() - 1
    pre_decay = jnp.zeros_like(span_decay)
    pre_state = jnp.zeros_like(fwd_span)
    suf_decay = jnp.zeros_like(span_decay)
    suf_grad = jnp.zeros_like(bwd_span)
    for bit_level in range(levels):
        peer_decay, peer_fwd, peer_bwd = (
            from_partner(span_decay.astype(jnp.bfloat16), "sp", bit_level).astype(span_decay.dtype),
            from_partner(fwd_span.astype(jnp.bfloat16), "sp", bit_level).astype(fwd_span.dtype),
            from_partner(bwd_span.astype(jnp.bfloat16), "sp", bit_level).astype(bwd_span.dtype),
        )
        is_upper = my_index // 2**bit_level % 2 == 1
        low_prefix = join_carry((peer_decay, peer_fwd), (pre_decay, pre_state))
        high_suffix = join_carry((peer_decay, peer_bwd), (suf_decay, suf_grad))
        fwd_after_low = join_carry((peer_decay, peer_fwd), (span_decay, fwd_span))[1]
        fwd_after_high = join_carry((span_decay, fwd_span), (peer_decay, peer_fwd))[1]
        bwd_after_low = join_carry((span_decay, bwd_span), (peer_decay, peer_bwd))[1]
        bwd_after_high = join_carry((peer_decay, peer_bwd), (span_decay, bwd_span))[1]
        pre_decay = jnp.where(is_upper, low_prefix[0], pre_decay)
        pre_state = jnp.where(is_upper, low_prefix[1], pre_state)
        suf_decay = jnp.where(is_upper, suf_decay, high_suffix[0])
        suf_grad = jnp.where(is_upper, suf_grad, high_suffix[1])
        fwd_span = jnp.where(is_upper, fwd_after_low, fwd_after_high)
        bwd_span = jnp.where(is_upper, bwd_after_low, bwd_after_high)
        span_decay = span_decay + peer_decay
    return (pre_state, suf_grad)


def per_device(
    block_source,
    address_weights,
    causal_filter_taps,
    payload_vectors,
    probe_vectors,
    interval_preimage,
    channel_damping_exponent,
    added_damping_jumps,
    sigmoid_argument,
    adjoint_of_result,
):
    tokens, feature_count = block_source.shape
    channels = address_weights.shape[0]
    groups = channels // STATE
    head_count = interval_preimage.shape[1]
    group_heads = head_count // groups
    block_count = tokens // BLOCK
    rim_rows = causal_filter_taps.shape[0] - 1
    projected = lax.dot_general(
        block_source, address_weights, (((1,), (1,)), ((), ())), preferred_element_type=jnp.float32
    ).astype(jnp.bfloat16)
    prev_rim = from_behind(projected[tokens - rim_rows :], "sp", 1)
    padded = jnp.concatenate([prev_rim, projected], axis=0).astype(jnp.float32)
    convolved = causal_conv(padded, causal_filter_taps, tokens)
    key_narrow = jax.nn.silu(convolved).astype(jnp.bfloat16).reshape(tokens, groups, STATE)
    pooled_addresses = key_narrow.astype(jnp.float32)
    query_narrow = probe_vectors.reshape(tokens, groups, STATE)
    pooled_probes = query_narrow.astype(jnp.float32)
    blocked_scores = jnp.einsum(
        "bign,bjgn->bgij",
        query_narrow.reshape(block_count, BLOCK, groups, STATE),
        key_narrow.reshape(block_count, BLOCK, groups, STATE),
        preferred_element_type=jnp.float32,
    )
    value_wide = payload_vectors.astype(jnp.float32)
    interval_widths = jax.nn.softplus(interval_preimage)
    damping_exponent = (
        added_damping_jumps - jnp.exp(channel_damping_exponent)[None] * interval_widths
    )
    running = jnp.cumsum(damping_exponent, axis=0)
    span_total = running[-1]
    scaled = (
        value_wide.reshape(tokens, groups, group_heads, -1)
        * interval_widths.reshape(tokens, groups, group_heads)[..., None]
    )
    local_state = jnp.einsum(
        "tgn,tgr,tgrp->grpn",
        pooled_addresses,
        jnp.exp(span_total[None] - running).reshape(tokens, groups, group_heads),
        scaled,
        precision=HIGHEST,
    )
    gate_wide = sigmoid_argument.astype(jnp.float32)
    grad_wide = adjoint_of_result.astype(jnp.float32)
    mixed_grad = grad_wide * jax.nn.silu(gate_wide)
    local_grad = jnp.einsum(
        "tgn,tgr,tgrp->grpn",
        pooled_probes,
        jnp.exp(running).reshape(tokens, groups, group_heads),
        mixed_grad.reshape(tokens, groups, group_heads, -1),
        precision=HIGHEST,
    )
    span_decay = span_total.reshape(groups, group_heads)
    incoming_state, grad_out = pair_chains(span_decay, local_state, local_grad)

    def mixer(
        payload_factor, interval_argument_factor, address_factor, probe_factor, score_operand
    ):
        return linear_scan_update(
            payload_factor,
            interval_argument_factor,
            address_factor,
            probe_factor,
            score_operand,
            incoming_state,
            channel_damping_exponent,
            added_damping_jumps,
        )

    mixer_pair, pullback = jax.vjp(
        mixer, value_wide, interval_preimage, pooled_addresses, pooled_probes, blocked_scores
    )
    mixer_out = mixer_pair[0]
    value_grad, decay_grad, key_state_grad, query_state_grad, score_grad = pullback(
        (mixed_grad, grad_out)
    )
    key_grad = key_state_grad + jnp.einsum(
        "bgij,bign->bjgn",
        score_grad,
        pooled_probes.reshape(block_count, BLOCK, groups, STATE),
        precision=HIGHEST,
    ).reshape(tokens, groups, STATE)
    query_grad = query_state_grad + jnp.einsum(
        "bgij,bjgn->bign",
        score_grad,
        pooled_addresses.reshape(block_count, BLOCK, groups, STATE),
        precision=HIGHEST,
    ).reshape(tokens, groups, STATE)
    gate_grad = (grad_wide * mixer_out * silu_slope(gate_wide)).astype(jnp.bfloat16)
    conv_grad = key_grad.reshape(tokens, channels) * silu_slope(convolved)
    next_rim = from_behind(conv_grad[:rim_rows], "sp", -1)
    extended = jnp.concatenate([conv_grad, next_rim], axis=0)
    projected_grad = conv_transpose(extended, causal_filter_taps, tokens).astype(jnp.bfloat16)
    input_grad = summed_on_arrival(
        lax.dot_general(
            address_weights,
            projected_grad,
            (((0,), (1,)), ((), ())),
            preferred_element_type=jnp.float32,
        ).astype(jnp.bfloat16),
        "tp",
        0,
    ).astype(jnp.bfloat16)
    summed = summed_on_arrival(
        lax.dot_general(
            projected_grad,
            block_source,
            (((0,), (0,)), ((), ())),
            preferred_element_type=jnp.float32,
        ).astype(jnp.bfloat16),
        "sp",
        0,
    )
    row_squares = collect(jnp.sum(summed * summed, axis=1), "sp", 0)
    key_weight_grad = lax.all_to_all(summed, "sp", split_axis=1, concat_axis=0, tiled=True)
    return (
        key_weight_grad,
        row_squares,
        input_grad,
        value_grad.astype(jnp.bfloat16),
        query_grad.reshape(tokens, channels).astype(jnp.bfloat16),
        decay_grad,
        gate_grad,
    )


def solution(mesh):
    in_specs = (
        P("sp", None),
        P("tp", None),
        P(None, "tp"),
        P("sp", "tp"),
        P("sp", "tp"),
        P("sp", "tp"),
        P("tp"),
        P("sp", "tp"),
        P("sp", "tp"),
        P("sp", "tp"),
    )
    out_specs = (
        P("tp", "sp"),
        P("tp"),
        P("tp", "sp"),
        P("sp", "tp"),
        P("sp", "tp"),
        P("sp", "tp"),
        P("sp", "tp"),
    )
    return jax.shard_map(
        per_device, mesh=mesh, in_specs=in_specs, out_specs=out_specs, check_vma=False
    )
```

profile of v0, /device:TPU:2, one launch (start us, length us, event | category | flops | bytes accessed | tf_op | source)
XLA Modules:
  0.0 224.0 jit_solution(2435246830219982427)
XLA Ops:
  0.7 0.8 broadcast_compare_fusion
  2.4 0.8 copy.75
  3.4 3.5 %collective-permute-start.1 = (bf16[1,4]{1,0:T(2,128)(2,1)S(1)}, bf16[1,4]{1,0:T(2,128)(2,1)S(1)}, u32[]{:S(2)}, u32[]{:S(2)}) collective-permute-start(bf16[1,4]{1,0:T(2,128)(2,1)S(1)} %slice.129), channel_id=1, source_target_pairs={{0,8},{8,0},{16,24},{24,16},{32,40},{40,32},{48,56},{56,48},{64,72... | collective-permute-start | bytes 32 | tf_op jit(solution)/shard_map/ppermute | solution.py:20
  7.2 2.4 %collective-permute-start.11 = (bf16[3,128]{1,0:T(4,128)(2,1)S(1)}, bf16[3,128]{1,0:T(4,128)(2,1)S(1)}, u32[]{:S(2)}, u32[]{:S(2)}) collective-permute-start(bf16[3,128]{1,0:T(4,128)(2,1)S(1)} %slice.67), channel_id=1, source_target_pairs={{0,8},{8,16},{16,24},{24,32},{32,40},{40,48},{48,56},{56,64},{64,7... | collective-permute-start | bytes 2312 | tf_op jit(solution)/shard_map/ppermute | solution.py:26
  10.6 0.7 copy-done.4
  11.5 0.7 copy-done.5
  12.6 5.1 %collective-permute-start.3 = (bf16[1,4]{1,0:T(2,128)(2,1)S(1)}, bf16[1,4]{1,0:T(2,128)(2,1)S(1)}, u32[]{:S(2)}, u32[]{:S(2)}) collective-permute-start(bf16[1,4]{1,0:T(2,128)(2,1)S(1)} %get-tuple-element.196), channel_id=1, source_target_pairs={{0,16},{16,0},{8,24},{24,8},{32,48},{48,32},{40,56},{56,40},{64,80... | collective-permute-start | bytes 32 | tf_op jit(solution)/shard_map/ppermute | solution.py:20
  18.8 3.7 %collective-permute-start = (bf16[1,4,64,128]{3,2,1,0:T(8,128)(2,1)S(1)}, bf16[1,4,64,128]{3,2,1,0:T(8,128)(2,1)S(1)}, u32[]{:S(2)}, u32[]{:S(2)}) collective-permute-start(bf16[1,4,64,128]{3,2,1,0:T(8,128)(2,1)S(1)} %convert_bitcast_fusion.1), channel_id=1, source_target_pairs={{0,8},{8,0},{16,24},{24,16},{32,40},{40,32},{48,56},{56,48},{64,72... | collective-permute-start | bytes 196616 | tf_op jit(solution)/shard_map/ppermute | solution.py:20
  22.6 3.8 %collective-permute-start.5 = (bf16[1,4]{1,0:T(2,128)(2,1)S(1)}, bf16[1,4]{1,0:T(2,128)(2,1)S(1)}, u32[]{:S(2)}, u32[]{:S(2)}) collective-permute-start(bf16[1,4]{1,0:T(2,128)(2,1)S(1)} %get-tuple-element.247), channel_id=1, source_target_pairs={{0,32},{32,0},{8,40},{40,8},{16,48},{48,16},{24,56},{56,24},{64,96... | collective-permute-start | bytes 32 | tf_op jit(solution)/shard_map/ppermute | solution.py:20
  26.4 1.6 collective-permute-done.5
  28.1 6.3 %collective-permute-start.7 = (bf16[1,4]{1,0:T(2,128)(2,1)S(1)}, bf16[1,4]{1,0:T(2,128)(2,1)S(1)}, u32[]{:S(2)}, u32[]{:S(2)}) collective-permute-start(bf16[1,4]{1,0:T(2,128)(2,1)S(1)} %get-tuple-element.241), channel_id=1, source_target_pairs={{0,64},{64,0},{8,72},{72,8},{16,80},{80,16},{24,88},{88,24},{32,96... | collective-permute-start | bytes 32 | tf_op jit(solution)/shard_map/ppermute | solution.py:20
  34.4 1.5 collective-permute-done.7
  35.9 9.1 %collective-permute-start.9 = (bf16[1,4]{1,0:T(2,128)(2,1)S(1)}, bf16[1,4]{1,0:T(2,128)(2,1)S(1)}, u32[]{:S(2)}, u32[]{:S(2)}) collective-permute-start(bf16[1,4]{1,0:T(2,128)(2,1)S(1)} %get-tuple-element.230), channel_id=1, source_target_pairs={{0,128},{128,0},{8,136},{136,8},{16,144},{144,16},{24,152},{152,24... | collective-permute-start | bytes 32 | tf_op jit(solution)/shard_map/ppermute | solution.py:20
  45.3 1.9 collective-permute-start.13
  47.3 4.4 %collective-permute-done.13 = bf16[1,4,64,128]{3,2,1,0:T(8,128)(2,1)S(1)} collective-permute-done((bf16[1,4,64,128]{3,2,1,0:T(8,128)(2,1)S(1)}, bf16[1,4,64,128]{3,2,1,0:T(8,128)(2,1)S(1)}, u32[]{:S(2)}, u32[]{:S(2)}) %collective-permute-start.13) | collective-permute-done | bytes 65568 | tf_op jit(solution)/shard_map/ppermute | solution.py:20
  51.9 2.3 %collective-permute-start.14 = (bf16[1,4,64,128]{3,2,1,0:T(8,128)(2,1)S(1)}, bf16[1,4,64,128]{3,2,1,0:T(8,128)(2,1)S(1)}, u32[]{:S(2)}, u32[]{:S(2)}) collective-permute-start(bf16[1,4,64,128]{3,2,1,0:T(8,128)(2,1)S(1)} %get-tuple-element.228), channel_id=1, source_target_pairs={{0,16},{16,0},{8,24},{24,8},{32,48},{48,32},{40,56},{56,40},{64,80... | collective-permute-start | bytes 196616 | tf_op jit(solution)/shard_map/ppermute | solution.py:20
  54.2 5.0 %collective-permute-start.2 = (bf16[1,4,64,128]{3,2,1,0:T(8,128)(2,1)S(1)}, bf16[1,4,64,128]{3,2,1,0:T(8,128)(2,1)S(1)}, u32[]{:S(2)}, u32[]{:S(2)}) collective-permute-start(bf16[1,4,64,128]{3,2,1,0:T(8,128)(2,1)S(1)} %get-tuple-element.227), channel_id=1, source_target_pairs={{0,16},{16,0},{8,24},{24,8},{32,48},{48,32},{40,56},{56,40},{64,80... | collective-permute-start | bytes 196616 | tf_op jit(solution)/shard_map/ppermute | solution.py:20
  59.5 2.3 %collective-permute-done.2 = bf16[1,4,64,128]{3,2,1,0:T(8,128)(2,1)S(1)} collective-permute-done((bf16[1,4,64,128]{3,2,1,0:T(8,128)(2,1)S(1)}, bf16[1,4,64,128]{3,2,1,0:T(8,128)(2,1)S(1)}, u32[]{:S(2)}, u32[]{:S(2)}) %collective-permute-start.2) | collective-permute-done | bytes 65568 | tf_op jit(solution)/shard_map/ppermute | solution.py:20
  62.1 3.9 %collective-permute-start.15 = (bf16[1,4,64,128]{3,2,1,0:T(8,128)(2,1)S(1)}, bf16[1,4,64,128]{3,2,1,0:T(8,128)(2,1)S(1)}, u32[]{:S(2)}, u32[]{:S(2)}) collective-permute-start(bf16[1,4,64,128]{3,2,1,0:T(8,128)(2,1)S(1)} %get-tuple-element.216), channel_id=1, source_target_pairs={{0,32},{32,0},{8,40},{40,8},{16,48},{48,16},{24,56},{56,24},{64,96... | collective-permute-start | bytes 196616 | tf_op jit(solution)/shard_map/ppermute | solution.py:20
  66.0 1.9 collective-permute-start.4
  68.2 4.3 %collective-permute-done.4 = bf16[1,4,64,128]{3,2,1,0:T(8,128)(2,1)S(1)} collective-permute-done((bf16[1,4,64,128]{3,2,1,0:T(8,128)(2,1)S(1)}, bf16[1,4,64,128]{3,2,1,0:T(8,128)(2,1)S(1)}, u32[]{:S(2)}, u32[]{:S(2)}) %collective-permute-start.4) | collective-permute-done | bytes 65568 | tf_op jit(solution)/shard_map/ppermute | solution.py:20
  72.9 4.5 %collective-permute-start.16 = (bf16[1,4,64,128]{3,2,1,0:T(8,128)(2,1)S(1)}, bf16[1,4,64,128]{3,2,1,0:T(8,128)(2,1)S(1)}, u32[]{:S(2)}, u32[]{:S(2)}) collective-permute-start(bf16[1,4,64,128]{3,2,1,0:T(8,128)(2,1)S(1)} %get-tuple-element.211), channel_id=1, source_target_pairs={{0,64},{64,0},{8,72},{72,8},{16,80},{80,16},{24,88},{88,24},{32,96... | collective-permute-start | bytes 196616 | tf_op jit(solution)/shard_map/ppermute | solution.py:20
  77.4 2.2 collective-permute-start.6
  79.9 5.8 %collective-permute-done.6 = bf16[1,4,64,128]{3,2,1,0:T(8,128)(2,1)S(1)} collective-permute-done((bf16[1,4,64,128]{3,2,1,0:T(8,128)(2,1)S(1)}, bf16[1,4,64,128]{3,2,1,0:T(8,128)(2,1)S(1)}, u32[]{:S(2)}, u32[]{:S(2)}) %collective-permute-start.6) | collective-permute-done | bytes 65568 | tf_op jit(solution)/shard_map/ppermute | solution.py:20
  85.9 2.9 %collective-permute-start.17 = (bf16[1,4,64,128]{3,2,1,0:T(8,128)(2,1)S(1)}, bf16[1,4,64,128]{3,2,1,0:T(8,128)(2,1)S(1)}, u32[]{:S(2)}, u32[]{:S(2)}) collective-permute-start(bf16[1,4,64,128]{3,2,1,0:T(8,128)(2,1)S(1)} %get-tuple-element.226), channel_id=1, source_target_pairs={{0,128},{128,0},{8,136},{136,8},{16,144},{144,16},{24,152},{152,24... | collective-permute-start | bytes 196616 | tf_op jit(solution)/shard_map/ppermute | solution.py:20
  88.8 6.8 %collective-permute-start.8 = (bf16[1,4,64,128]{3,2,1,0:T(8,128)(2,1)S(1)}, bf16[1,4,64,128]{3,2,1,0:T(8,128)(2,1)S(1)}, u32[]{:S(2)}, u32[]{:S(2)}) collective-permute-start(bf16[1,4,64,128]{3,2,1,0:T(8,128)(2,1)S(1)} %get-tuple-element.225), channel_id=1, source_target_pairs={{0,128},{128,0},{8,136},{136,8},{16,144},{144,16},{24,152},{152,24... | collective-permute-start | bytes 196616 | tf_op jit(solution)/shard_map/ppermute | solution.py:20
  96.4 2.2 collective-permute-done.17
  99.5 11.7 %collective-permute-start.10 = (bf16[1,4,64,128]{3,2,1,0:T(8,128)(2,1)S(1)}, bf16[1,4,64,128]{3,2,1,0:T(8,128)(2,1)S(1)}, u32[]{:S(2)}, u32[]{:S(2)}) collective-permute-start(bf16[1,4,64,128]{3,2,1,0:T(8,128)(2,1)S(1)} %get-tuple-element.213), channel_id=1, source_target_pairs={{0,256},{256,0},{8,264},{264,8},{16,272},{272,16},{24,280},{280,24... | collective-permute-start | bytes 196616 | tf_op jit(solution)/shard_map/ppermute | solution.py:20
  111.2 2.8 %collective-permute-start.18 = (bf16[1,4,64,128]{3,2,1,0:T(8,128)(2,1)S(1)}, bf16[1,4,64,128]{3,2,1,0:T(8,128)(2,1)S(1)}, u32[]{:S(2)}, u32[]{:S(2)}) collective-permute-start(bf16[1,4,64,128]{3,2,1,0:T(8,128)(2,1)S(1)} %get-tuple-element.214), channel_id=1, source_target_pairs={{0,256},{256,0},{8,264},{264,8},{16,272},{272,16},{24,280},{280,24... | collective-permute-start | bytes 196616 | tf_op jit(solution)/shard_map/ppermute | solution.py:20
  114.6 11.6 %collective-permute-done.18 = bf16[1,4,64,128]{3,2,1,0:T(8,128)(2,1)S(1)} collective-permute-done((bf16[1,4,64,128]{3,2,1,0:T(8,128)(2,1)S(1)}, bf16[1,4,64,128]{3,2,1,0:T(8,128)(2,1)S(1)}, u32[]{:S(2)}, u32[]{:S(2)}) %collective-permute-start.18) | collective-permute-done | bytes 65568 | tf_op jit(solution)/shard_map/ppermute | solution.py:20
  127.5 1.3 collective-permute-start.12
  128.8 4.2 %collective-permute-done.12 = f32[3,128]{1,0:T(4,128)S(1)} collective-permute-done((f32[3,128]{1,0:T(4,128)S(1)}, f32[3,128]{1,0:T(4,128)S(1)}, u32[]{:S(2)}, u32[]{:S(2)}) %collective-permute-start.12) | collective-permute-done | bytes 1568 | tf_op jit(solution)/shard_map/ppermute | solution.py:26
  133.3 1.1 reshape.462
  134.5 11.3 %all-to-all-start = ((bf16[64,2,2048]{2,1,0:T(2,128)(2,1)}), bf16[64,2,2048]{2,1,0:T(2,128)(2,1)S(1)}, u32[]{:S(2)}, u32[]{:S(2)}) async-start(bf16[64,2,2048]{2,1,0:T(2,128)(2,1)} %reshape.462), calls=%async_computation | async-start | bytes 1048576 | tf_op jit(solution)/shard_map/all_to_all | solution.py:37
  146.9 1.1 reduce_window_sum.43
  149.8 0.8 copy.120
  150.6 18.2 %all-to-all-done = bf16[64,2,2048]{2,1,0:T(2,128)(2,1)S(1)} async-done(((bf16[64,2,2048]{2,1,0:T(2,128)(2,1)}), bf16[64,2,2048]{2,1,0:T(2,128)(2,1)S(1)}, u32[]{:S(2)}, u32[]{:S(2)}) %all-to-all-start) | async-done | bytes 524320 | tf_op jit(solution)/shard_map/all_to_all | solution.py:37
  168.8 4.8 %all-to-all-start.3 = ((bf16[8,256,128]{1,2,0:T(8,128)(2,1)}), bf16[8,256,128]{1,2,0:T(8,128)(2,1)S(1)}, u32[]{:S(2)}, u32[]{:S(2)}) async-start(bf16[8,256,128]{1,2,0:T(8,128)(2,1)} %bitcast.241), calls=%async_computation.3 | async-start | bytes 1048576 | tf_op jit(solution)/shard_map/all_to_all | solution.py:37
  174.3 8.2 %all-to-all-done.3 = bf16[8,256,128]{1,2,0:T(8,128)(2,1)S(1)} async-done(((bf16[8,256,128]{1,2,0:T(8,128)(2,1)}), bf16[8,256,128]{1,2,0:T(8,128)(2,1)S(1)}, u32[]{:S(2)}, u32[]{:S(2)}) %all-to-all-start.3) | async-done | bytes 524320 | tf_op jit(solution)/shard_map/all_to_all | solution.py:37
  183.2 5.8 %all-to-all-start.2 = ((f32[64,1,2]{2,1,0:T(1,128)}), f32[64,1,2]{2,1,0:T(1,128)S(1)}, u32[]{:S(2)}, u32[]{:S(2)}) async-start(f32[64,1,2]{2,1,0:T(1,128)} %broadcast_in_dim.135), calls=%async_computation.2 | async-start | bytes 65536 | tf_op jit(solution)/shard_map/all_to_all | solution.py:43
  190.2 13.4 %all-to-all-done.2 = f32[64,1,2]{2,1,0:T(1,128)S(1)} async-done(((f32[64,1,2]{2,1,0:T(1,128)}), f32[64,1,2]{2,1,0:T(1,128)S(1)}, u32[]{:S(2)}, u32[]{:S(2)}) %all-to-all-start.2) | async-done | bytes 544 | tf_op jit(solution)/shard_map/all_to_all | solution.py:43
  203.6 4.6 %all-to-all-start.1 = ((f32[2,64,32]{2,0,1:T(2,128)}), f32[2,64,32]{2,0,1:T(2,128)S(1)}, u32[]{:S(2)}, u32[]{:S(2)}) async-start(f32[2,64,32]{2,0,1:T(2,128)} %copy.85), calls=%async_computation.1 | async-start | bytes 131072 | tf_op jit(solution)/shard_map/all_to_all | solution.py:298
  208.1 0.8 fusion.6
  208.9 0.7 copy.106
  210.3 0.7 copy.104
  211.1 0.7 copy.103
  212.4 0.7 reduce.17
  213.8 9.6 %all-to-all-done.1 = f32[2,64,32]{2,0,1:T(2,128)S(1)} async-done(((f32[2,64,32]{2,0,1:T(2,128)}), f32[2,64,32]{2,0,1:T(2,128)S(1)}, u32[]{:S(2)}, u32[]{:S(2)}) %all-to-all-start.1) | async-done | bytes 16416 | tf_op jit(solution)/shard_map/all_to_all | solution.py:298
  (106 shorter events, 17.5 us)
Async XLA Ops:
  0.6 6.2 %copy-start = (bf16[128,2048]{1,0:T(8,128)(2,1)S(1)}, bf16[128,2048]{1,0:T(8,128)(2,1)}, u32[]{:S(2)}) copy-start(bf16[128,2048]{1,0:T(8,128)(2,1)} %param.10) | copy-start | bytes 1572868
  0.6 0.8 copy-start.6
  0.7 6.2 %copy-start.1 = (bf16[128,2048]{1,0:T(8,128)(2,1)S(1)}, bf16[128,2048]{1,0:T(8,128)(2,1)}, u32[]{:S(2)}) copy-start(bf16[128,2048]{1,0:T(8,128)(2,1)} %param.11) | copy-start | bytes 1572868
  3.4 9.2 %collective-permute-start.1 = (bf16[1,4]{1,0:T(2,128)(2,1)S(1)}, bf16[1,4]{1,0:T(2,128)(2,1)S(1)}, u32[]{:S(2)}, u32[]{:S(2)}) collective-permute-start(bf16[1,4]{1,0:T(2,128)(2,1)S(1)} %slice.129), channel_id=1, source_target_pairs={{0,8},{8,0},{16,24},{24,16},{32,40},{40,32},{48,56},{56,48},{64,72... | collective-permute-start | bytes 32 | tf_op jit(solution)/shard_map/ppermute | solution.py:20
  7.2 37.8 %collective-permute-start.11 = (bf16[3,128]{1,0:T(4,128)(2,1)S(1)}, bf16[3,128]{1,0:T(4,128)(2,1)S(1)}, u32[]{:S(2)}, u32[]{:S(2)}) collective-permute-start(bf16[3,128]{1,0:T(4,128)(2,1)S(1)} %slice.67), channel_id=1, source_target_pairs={{0,8},{8,16},{16,24},{24,32},{32,40},{40,48},{48,56},{56,64},{64,7... | collective-permute-start | bytes 2312 | tf_op jit(solution)/shard_map/ppermute | solution.py:26
  9.7 0.7 copy-start.7
  9.7 0.8 copy-start.3
  10.5 0.8 copy-start.4
  11.4 0.8 copy-start.5
  12.6 9.9 %collective-permute-start.3 = (bf16[1,4]{1,0:T(2,128)(2,1)S(1)}, bf16[1,4]{1,0:T(2,128)(2,1)S(1)}, u32[]{:S(2)}, u32[]{:S(2)}) collective-permute-start(bf16[1,4]{1,0:T(2,128)(2,1)S(1)} %get-tuple-element.196), channel_id=1, source_target_pairs={{0,16},{16,0},{8,24},{24,8},{32,48},{48,32},{40,56},{56,40},{64,80... | collective-permute-start | bytes 32 | tf_op jit(solution)/shard_map/ppermute | solution.py:20
  17.8 0.8 copy-start.2
  18.8 28.5 %collective-permute-start = (bf16[1,4,64,128]{3,2,1,0:T(8,128)(2,1)S(1)}, bf16[1,4,64,128]{3,2,1,0:T(8,128)(2,1)S(1)}, u32[]{:S(2)}, u32[]{:S(2)}) collective-permute-start(bf16[1,4,64,128]{3,2,1,0:T(8,128)(2,1)S(1)} %convert_bitcast_fusion.1), channel_id=1, source_target_pairs={{0,8},{8,0},{16,24},{24,16},{32,40},{40,32},{48,56},{56,48},{64,72... | collective-permute-start | bytes 196616 | tf_op jit(solution)/shard_map/ppermute | solution.py:20
  22.6 5.5 %collective-permute-start.5 = (bf16[1,4]{1,0:T(2,128)(2,1)S(1)}, bf16[1,4]{1,0:T(2,128)(2,1)S(1)}, u32[]{:S(2)}, u32[]{:S(2)}) collective-permute-start(bf16[1,4]{1,0:T(2,128)(2,1)S(1)} %get-tuple-element.247), channel_id=1, source_target_pairs={{0,32},{32,0},{8,40},{40,8},{16,48},{48,16},{24,56},{56,24},{64,96... | collective-permute-start | bytes 32 | tf_op jit(solution)/shard_map/ppermute | solution.py:20
  28.1 7.8 %collective-permute-start.7 = (bf16[1,4]{1,0:T(2,128)(2,1)S(1)}, bf16[1,4]{1,0:T(2,128)(2,1)S(1)}, u32[]{:S(2)}, u32[]{:S(2)}) collective-permute-start(bf16[1,4]{1,0:T(2,128)(2,1)S(1)} %get-tuple-element.241), channel_id=1, source_target_pairs={{0,64},{64,0},{8,72},{72,8},{16,80},{80,16},{24,88},{88,24},{32,96... | collective-permute-start | bytes 32 | tf_op jit(solution)/shard_map/ppermute | solution.py:20
  35.9 11.4 %collective-permute-start.9 = (bf16[1,4]{1,0:T(2,128)(2,1)S(1)}, bf16[1,4]{1,0:T(2,128)(2,1)S(1)}, u32[]{:S(2)}, u32[]{:S(2)}) collective-permute-start(bf16[1,4]{1,0:T(2,128)(2,1)S(1)} %get-tuple-element.230), channel_id=1, source_target_pairs={{0,128},{128,0},{8,136},{136,8},{16,144},{144,16},{24,152},{152,24... | collective-permute-start | bytes 32 | tf_op jit(solution)/shard_map/ppermute | solution.py:20
  45.3 6.4 %collective-permute-start.13 = (bf16[1,4,64,128]{3,2,1,0:T(8,128)(2,1)S(1)}, bf16[1,4,64,128]{3,2,1,0:T(8,128)(2,1)S(1)}, u32[]{:S(2)}, u32[]{:S(2)}) collective-permute-start(bf16[1,4,64,128]{3,2,1,0:T(8,128)(2,1)S(1)} %convert_bitcast_fusion), channel_id=1, source_target_pairs={{0,8},{8,0},{16,24},{24,16},{32,40},{40,32},{48,56},{56,48},{64,72... | collective-permute-start | bytes 196616 | tf_op jit(solution)/shard_map/ppermute | solution.py:20
  51.9 7.7 %collective-permute-start.14 = (bf16[1,4,64,128]{3,2,1,0:T(8,128)(2,1)S(1)}, bf16[1,4,64,128]{3,2,1,0:T(8,128)(2,1)S(1)}, u32[]{:S(2)}, u32[]{:S(2)}) collective-permute-start(bf16[1,4,64,128]{3,2,1,0:T(8,128)(2,1)S(1)} %get-tuple-element.228), channel_id=1, source_target_pairs={{0,16},{16,0},{8,24},{24,8},{32,48},{48,32},{40,56},{56,40},{64,80... | collective-permute-start | bytes 196616 | tf_op jit(solution)/shard_map/ppermute | solution.py:20
  54.2 7.7 %collective-permute-start.2 = (bf16[1,4,64,128]{3,2,1,0:T(8,128)(2,1)S(1)}, bf16[1,4,64,128]{3,2,1,0:T(8,128)(2,1)S(1)}, u32[]{:S(2)}, u32[]{:S(2)}) collective-permute-start(bf16[1,4,64,128]{3,2,1,0:T(8,128)(2,1)S(1)} %get-tuple-element.227), channel_id=1, source_target_pairs={{0,16},{16,0},{8,24},{24,8},{32,48},{48,32},{40,56},{56,40},{64,80... | collective-permute-start | bytes 196616 | tf_op jit(solution)/shard_map/ppermute | solution.py:20
  62.1 6.2 %collective-permute-start.15 = (bf16[1,4,64,128]{3,2,1,0:T(8,128)(2,1)S(1)}, bf16[1,4,64,128]{3,2,1,0:T(8,128)(2,1)S(1)}, u32[]{:S(2)}, u32[]{:S(2)}) collective-permute-start(bf16[1,4,64,128]{3,2,1,0:T(8,128)(2,1)S(1)} %get-tuple-element.216), channel_id=1, source_target_pairs={{0,32},{32,0},{8,40},{40,8},{16,48},{48,16},{24,56},{56,24},{64,96... | collective-permute-start | bytes 196616 | tf_op jit(solution)/shard_map/ppermute | solution.py:20
  66.0 6.5 %collective-permute-start.4 = (bf16[1,4,64,128]{3,2,1,0:T(8,128)(2,1)S(1)}, bf16[1,4,64,128]{3,2,1,0:T(8,128)(2,1)S(1)}, u32[]{:S(2)}, u32[]{:S(2)}) collective-permute-start(bf16[1,4,64,128]{3,2,1,0:T(8,128)(2,1)S(1)} %get-tuple-element.215), channel_id=1, source_target_pairs={{0,32},{32,0},{8,40},{40,8},{16,48},{48,16},{24,56},{56,24},{64,96... | collective-permute-start | bytes 196616 | tf_op jit(solution)/shard_map/ppermute | solution.py:20
  72.9 7.1 %collective-permute-start.16 = (bf16[1,4,64,128]{3,2,1,0:T(8,128)(2,1)S(1)}, bf16[1,4,64,128]{3,2,1,0:T(8,128)(2,1)S(1)}, u32[]{:S(2)}, u32[]{:S(2)}) collective-permute-start(bf16[1,4,64,128]{3,2,1,0:T(8,128)(2,1)S(1)} %get-tuple-element.211), channel_id=1, source_target_pairs={{0,64},{64,0},{8,72},{72,8},{16,80},{80,16},{24,88},{88,24},{32,96... | collective-permute-start | bytes 196616 | tf_op jit(solution)/shard_map/ppermute | solution.py:20
  77.4 8.3 %collective-permute-start.6 = (bf16[1,4,64,128]{3,2,1,0:T(8,128)(2,1)S(1)}, bf16[1,4,64,128]{3,2,1,0:T(8,128)(2,1)S(1)}, u32[]{:S(2)}, u32[]{:S(2)}) collective-permute-start(bf16[1,4,64,128]{3,2,1,0:T(8,128)(2,1)S(1)} %get-tuple-element.168), channel_id=1, source_target_pairs={{0,64},{64,0},{8,72},{72,8},{16,80},{80,16},{24,88},{88,24},{32,96... | collective-permute-start | bytes 196616 | tf_op jit(solution)/shard_map/ppermute | solution.py:20
  85.9 12.7 %collective-permute-start.17 = (bf16[1,4,64,128]{3,2,1,0:T(8,128)(2,1)S(1)}, bf16[1,4,64,128]{3,2,1,0:T(8,128)(2,1)S(1)}, u32[]{:S(2)}, u32[]{:S(2)}) collective-permute-start(bf16[1,4,64,128]{3,2,1,0:T(8,128)(2,1)S(1)} %get-tuple-element.226), channel_id=1, source_target_pairs={{0,128},{128,0},{8,136},{136,8},{16,144},{144,16},{24,152},{152,24... | collective-permute-start | bytes 196616 | tf_op jit(solution)/shard_map/ppermute | solution.py:20
  88.8 10.5 %collective-permute-start.8 = (bf16[1,4,64,128]{3,2,1,0:T(8,128)(2,1)S(1)}, bf16[1,4,64,128]{3,2,1,0:T(8,128)(2,1)S(1)}, u32[]{:S(2)}, u32[]{:S(2)}) collective-permute-start(bf16[1,4,64,128]{3,2,1,0:T(8,128)(2,1)S(1)} %get-tuple-element.225), channel_id=1, source_target_pairs={{0,128},{128,0},{8,136},{136,8},{16,144},{144,16},{24,152},{152,24... | collective-permute-start | bytes 196616 | tf_op jit(solution)/shard_map/ppermute | solution.py:20
  99.5 15.1 %collective-permute-start.10 = (bf16[1,4,64,128]{3,2,1,0:T(8,128)(2,1)S(1)}, bf16[1,4,64,128]{3,2,1,0:T(8,128)(2,1)S(1)}, u32[]{:S(2)}, u32[]{:S(2)}) collective-permute-start(bf16[1,4,64,128]{3,2,1,0:T(8,128)(2,1)S(1)} %get-tuple-element.213), channel_id=1, source_target_pairs={{0,256},{256,0},{8,264},{264,8},{16,272},{272,16},{24,280},{280,24... | collective-permute-start | bytes 196616 | tf_op jit(solution)/shard_map/ppermute | solution.py:20
  111.2 15.0 %collective-permute-start.18 = (bf16[1,4,64,128]{3,2,1,0:T(8,128)(2,1)S(1)}, bf16[1,4,64,128]{3,2,1,0:T(8,128)(2,1)S(1)}, u32[]{:S(2)}, u32[]{:S(2)}) collective-permute-start(bf16[1,4,64,128]{3,2,1,0:T(8,128)(2,1)S(1)} %get-tuple-element.214), channel_id=1, source_target_pairs={{0,256},{256,0},{8,264},{264,8},{16,272},{272,16},{24,280},{280,24... | collective-permute-start | bytes 196616 | tf_op jit(solution)/shard_map/ppermute | solution.py:20
  127.5 5.5 %collective-permute-start.12 = (f32[3,128]{1,0:T(4,128)S(1)}, f32[3,128]{1,0:T(4,128)S(1)}, u32[]{:S(2)}, u32[]{:S(2)}) collective-permute-start(f32[3,128]{1,0:T(4,128)S(1)} %slice.72), channel_id=1, source_target_pairs={{8,0},{16,8},{24,16},{32,24},{40,32},{48,40},{56,48},{64,56},{72,6... | collective-permute-start | bytes 4616 | tf_op jit(solution)/shard_map/ppermute | solution.py:26
  134.5 34.4 %all-to-all-start = ((bf16[64,2,2048]{2,1,0:T(2,128)(2,1)}), bf16[64,2,2048]{2,1,0:T(2,128)(2,1)S(1)}, u32[]{:S(2)}, u32[]{:S(2)}) async-start(bf16[64,2,2048]{2,1,0:T(2,128)(2,1)} %reshape.462), calls=%async_computation | async-start | bytes 1048576 | tf_op jit(solution)/shard_map/all_to_all | solution.py:37
  168.8 13.7 %all-to-all-start.3 = ((bf16[8,256,128]{1,2,0:T(8,128)(2,1)}), bf16[8,256,128]{1,2,0:T(8,128)(2,1)S(1)}, u32[]{:S(2)}, u32[]{:S(2)}) async-start(bf16[8,256,128]{1,2,0:T(8,128)(2,1)} %bitcast.241), calls=%async_computation.3 | async-start | bytes 1048576 | tf_op jit(solution)/shard_map/all_to_all | solution.py:37
  183.2 20.4 %all-to-all-start.2 = ((f32[64,1,2]{2,1,0:T(1,128)}), f32[64,1,2]{2,1,0:T(1,128)S(1)}, u32[]{:S(2)}, u32[]{:S(2)}) async-start(f32[64,1,2]{2,1,0:T(1,128)} %broadcast_in_dim.135), calls=%async_computation.2 | async-start | bytes 65536 | tf_op jit(solution)/shard_map/all_to_all | solution.py:43
  203.6 19.8 %all-to-all-start.1 = ((f32[2,64,32]{2,0,1:T(2,128)}), f32[2,64,32]{2,0,1:T(2,128)S(1)}, u32[]{:S(2)}, u32[]{:S(2)}) async-start(f32[2,64,32]{2,0,1:T(2,128)} %copy.85), calls=%async_computation.1 | async-start | bytes 131072 | tf_op jit(solution)/shard_map/all_to_all | solution.py:298
where the time goes:
time: 225 us; the launch traced here: 224 us
  starting transfers between devices  108 us (48%)
  waiting for transfers between devices  89 us (40%)
  local copies, waits for them, and re-layouts  14.3 us (6%)
  other arithmetic  5.72 us (3%)
  matrix products  5.72 us (3%)
    ppermute x17, starting transfers between devices, from_partner(): return lax.ppermute(block, axis, route)  77.7 us
    ppermute x17, waiting for transfers between devices, from_partner(): return lax.ppermute(block, axis, route)  35.4 us
    all_to_all x2, waiting for transfers between devices, summed_on_arrival(): parts = lax.all_to_all(cut_along(shard, dim, peers), axis, 0, 0, tiled=True)  26.5 us
    all_to_all x2, starting transfers between devices, summed_on_arrival(): parts = lax.all_to_all(cut_along(shard, dim, peers), axis, 0, 0, tiled=True)  16.2 us
    all_to_all x1, waiting for transfers between devices, sent_to_all(): return lax.all_to_all(copies, axis, split_axis=0, concat_axis=0, tiled=True)  13.4 us
    all_to_all x1, waiting for transfers between devices, per_device(): lax.all_to_all(summed, 'sp', split_axis=1, concat_axis=0, tiled=True)  9.59 us
    unnamed x25, local copies, waits for them, and re-layouts  7.54 us
    all_to_all x1, starting transfers between devices, sent_to_all(): return lax.all_to_all(copies, axis, split_axis=0, concat_axis=0, tiled=True)  5.83 us
  transfers between devices with their start and end apart: 23, of which 17 were waited for; matrix products, arithmetic and copies ran while one was open for 7% of the time, Pallas kernels for 0%

commit v1 on v0

v1 whole, which is shorter than its diff:
```python
import functools

import jax
import jax.numpy as jnp
from jax import lax
from jax.experimental import pallas as pl
from jax.experimental.pallas import tpu as pltpu
from jax.sharding import Mesh
from jax.sharding import PartitionSpec as P

TOK = 128
STATE = 128
HEAD = 64
R = 4
HP = R * HEAD
Y = 4
NS = STATE // Y
PAD = 8
HIGH = lax.Precision.HIGHEST
F32 = jnp.float32
BF16 = jnp.bfloat16
PALLAS = True
ZY = ("z", "y")


def dot(a, b, ca=1, cb=0, precision=None):
    return lax.dot_general(
        a, b, (((ca,), (cb,)), ((), ())), preferred_element_type=F32, precision=precision
    )


def roll(a, shift):
    size = a.shape[1]
    if PALLAS:
        return pltpu.roll(a, shift % size, 1)
    return jnp.roll(a, shift, axis=1)


def local(fn, outs, *args, flops=10**7):
    single = not isinstance(outs, (list, tuple))
    shapes = [outs] if single else list(outs)
    if not PALLAS:
        res = fn(*args)
        res = [res] if single else list(res)
        for r, s in zip(res, shapes):
            assert r.shape == s.shape and r.dtype == s.dtype, (fn, r, s)
        return res[0] if single else res

    def kernel(*refs):
        ins, dst = refs[: len(args)], refs[len(args) :]
        res = fn(*[r[...] for r in ins])
        res = [res] if single else res
        for ref, val in zip(dst, res):
            ref[...] = val

    vm = pl.BlockSpec(memory_space=pltpu.VMEM)
    res = pl.pallas_call(
        kernel,
        out_shape=shapes,
        in_specs=[vm] * len(args),
        out_specs=[vm] * len(shapes),
        name=fn.__name__,
        cost_estimate=pl.CostEstimate(flops=flops, bytes_accessed=10**6, transcendentals=0),
    )(*args)
    return res[0] if single else res


def sds(shape, dtype):
    return jax.ShapeDtypeStruct(shape, dtype)


def iota2(shape, dim):
    return lax.broadcasted_iota(jnp.int32, shape, dim)


def expand(a):
    return jnp.concatenate(
        [jnp.broadcast_to(a[:, h : h + 1], (a.shape[0], HEAD)) for h in range(R)], axis=1
    )


def split3(a):
    hi = a.astype(BF16)
    rest = a - hi.astype(F32)
    mid = rest.astype(BF16)
    low = (rest - mid.astype(F32)).astype(BF16)
    return hi, mid, low


def joined(parts, first):
    return (
        parts[:, first].astype(F32)
        + parts[:, first + 1].astype(F32)
        + parts[:, first + 2].astype(F32)
    )


def decays(tpre, aexp, jump):
    step = jnp.log(1.0 + jnp.exp(tpre))
    rate = jnp.exp(aexp)
    la = jump - rate * step
    tri = (iota2((TOK, TOK), 0) >= iota2((TOK, TOK), 1)).astype(F32)
    cum = dot(tri, la, precision=HIGH)
    return step, rate, la, cum


def sigmoid(v):
    return 1.0 / (1.0 + jnp.exp(-v))


def bwd_local(tpre, aexp, jump, gate, adj, q):
    step, rate, la, cum = decays(tpre, aexp, jump)
    g = gate.astype(F32)
    dy = adj.astype(F32) * g * sigmoid(g)
    dye = (dy * expand(jnp.exp(cum))).astype(BF16)
    lg = dot(q, dye, 0, 0).astype(BF16)
    hi, mid, low = split3(expand(cum[TOK - 1 :]))
    tail = jnp.concatenate([hi, mid, low, jnp.zeros((PAD - 3, HP), BF16)], axis=0)
    return jnp.stack([jnp.concatenate([lg[NS * i : NS * (i + 1)], tail], axis=0) for i in range(Y)])


def masks_of(cum, cum_t, h):
    causal = iota2((TOK, TOK), 0) >= iota2((TOK, TOK), 1)
    return jnp.exp(jnp.where(causal, cum[:, h : h + 1] - cum_t[h : h + 1, :], -1e30))


def fwd_local(tpre, aexp, jump, gate, adj, q, v, x, w, rim, taps_t):
    step, rate, la, cum = decays(tpre, aexp, jump)
    upper = (iota2((TOK, TOK), 0) <= iota2((TOK, TOK), 1)).astype(F32)
    cum_t = dot(la, upper, 0, 0, HIGH)
    g = gate.astype(F32)
    dy = (adj.astype(F32) * g * sigmoid(g)).astype(BF16)
    u = v.astype(F32) * expand(step)
    ud = (u * expand(jnp.exp(cum[TOK - 1 :] - cum))).astype(BF16)
    u = u.astype(BF16)
    dc = jnp.zeros((TOK, TOK), F32)
    for h in range(R):
        at = slice(HEAD * h, HEAD * (h + 1))
        dc = dc + masks_of(cum, cum_t, h) * dot(dy[:, at], u[:, at], 1, 1)
    dki = dot(q, dc.astype(BF16), 0, 0)
    proj = dot(w, x, 1, 1).astype(BF16).astype(F32)
    rim_proj = dot(w, rim, 1, 1).astype(BF16)
    place = (iota2((PAD, TOK), 1) == iota2((PAD, TOK), 0) + (TOK - PAD)).astype(BF16)
    rim_full = dot(rim_proj, place)
    lane = iota2((STATE, TOK), 1)
    conv = taps_t[:, 3:4] * proj
    for d in range(1, 4):
        conv = conv + taps_t[:, 3 - d : 4 - d] * roll(
            jnp.where(lane >= TOK - d, rim_full, proj), d
        )
    sig = sigmoid(conv)
    keys = (conv * sig).astype(BF16)
    slope = sig * (1.0 + conv * (1.0 - sig))
    ls = dot(keys, ud).astype(BF16)
    pair = jnp.concatenate([dki.astype(BF16), slope.astype(BF16)], axis=1)
    chunks = [rim[:, HP * i : HP * (i + 1)] for i in range(rim.shape[1] // HP)]
    shared = jnp.concatenate([ud] + chunks, axis=0)
    mid = jnp.stack(
        [
            jnp.concatenate(
                [shared, ls[NS * i : NS * (i + 1)], pair[NS * i : NS * (i + 1)]], axis=0
            )
            for i in range(Y)
        ]
    )
    return mid, keys


def bwd_group(got):
    tau = joined(got, NS)
    acc = got[Y - 1, :NS].astype(F32)
    for j in range(Y - 2, -1, -1):
        acc = got[j, :NS].astype(F32) + jnp.exp(tau[j : j + 1]) * acc
    hi, mid, low = split3(jnp.sum(tau, axis=0, keepdims=True))
    return jnp.concatenate(
        [acc.astype(BF16), hi, mid, low, jnp.zeros((PAD - 3, HP), BF16)], axis=0
    )


def fwd_group(got, mid):
    tau = joined(got, NS)
    at = slice(TOK + 8 * PAD, TOK + 8 * PAD + NS)
    acc = mid[0, at].astype(F32)
    for j in range(1, Y):
        acc = mid[j, at].astype(F32) + jnp.exp(tau[j : j + 1]) * acc
    return acc.astype(BF16)


def chain_sums(far):
    count = far.shape[0]
    tau = joined(far, NS)
    tri = (iota2((count, count), 0) >= iota2((count, count), 1)).astype(F32)
    upto = dot(tri, tau, precision=HIGH)
    return tau, upto


def weighted(weights, far):
    acc = weights[0:1] * far[0, :NS].astype(F32)
    for i in range(1, far.shape[0]):
        acc = acc + weights[i : i + 1] * far[i, :NS].astype(F32)
    return acc


def bwd_apply(far, got, mid, xg, taps_own, zrow):
    count = far.shape[0]
    tau, upto = chain_sums(far)
    row = iota2((count, HP), 0)
    mine = jnp.sum(jnp.where(row == zrow, upto, 0.0), axis=0, keepdims=True)
    weights = jnp.exp(jnp.where(row > zrow, upto - tau - mine, -1e30))
    state = weighted(weights, far)
    tau_j = joined(got, NS)
    ends = [None] * Y
    for j in range(Y - 1, -1, -1):
        ends[j] = state.astype(BF16)
        if j:
            state = got[j, :NS].astype(F32) + jnp.exp(tau_j[j : j + 1]) * state
    own = TOK + 8 * PAD + NS
    cg = []
    for j in range(Y):
        dk = dot(ends[j], mid[j, :TOK], 1, 1) + mid[j, own : own + NS, :TOK].astype(F32)
        cg.append(dk * mid[j, own : own + NS, TOK:].astype(F32))
    cg = jnp.concatenate(cg, axis=1)
    size = Y * TOK
    lane = iota2((NS, size), 1)
    main = taps_own[:, 3:4] * cg
    over = jnp.zeros_like(main)
    for d in range(1, 4):
        moved = taps_own[:, 3 - d : 4 - d] * roll(cg, -d)
        main = main + jnp.where(lane < size - d, moved, 0.0)
        over = over + jnp.where(lane >= size - d, moved, 0.0)
    rims = jnp.concatenate(
        [mid[0, TOK + PAD * i : TOK + PAD * (i + 1)] for i in range(8)], axis=1
    )
    over = over[:, size - TOK :]
    zero = jnp.zeros((TOK - PAD, rims.shape[1]), BF16)
    dw = dot(main.astype(BF16), xg) + dot(over.astype(BF16), jnp.concatenate([zero, rims], axis=0))
    width = dw.shape[1] // count
    dw = jnp.stack([dw[:, width * i : width * (i + 1)] for i in range(count)]).astype(BF16)
    return dw, jnp.stack(ends), main, over


def fwd_apply(far, bfar, got, mid, ends, zrow):
    count = far.shape[0]
    tau, upto = chain_sums(bfar)
    row = iota2((count, HP), 0)
    before = jnp.sum(jnp.where(row == zrow, upto - tau, 0.0), axis=0, keepdims=True)
    weights = jnp.exp(jnp.where(row < zrow, before - upto, -1e30))
    state = weighted(weights, far)
    tau_j = joined(got, NS)
    at = slice(TOK + 8 * PAD, TOK + 8 * PAD + NS)
    res = []
    for j in range(Y):
        res.append(jnp.concatenate([state.astype(BF16), ends[j]], axis=0))
        if j < Y - 1:
            state = mid[j, at].astype(F32) + jnp.exp(tau_j[j : j + 1]) * state
    return jnp.stack(res)


def head_sums(a):
    return jnp.concatenate(
        [jnp.sum(a[:, HEAD * h : HEAD * (h + 1)], axis=1, keepdims=True) for h in range(R)], axis=1
    )


def finish(states, tpre, aexp, jump, gate, adj, q, v, keys):
    step, rate, la, cum = decays(tpre, aexp, jump)
    upper = (iota2((TOK, TOK), 0) <= iota2((TOK, TOK), 1)).astype(F32)
    cum_t = dot(la, upper, 0, 0, HIGH)
    s_in = jnp.concatenate([states[i, :NS] for i in range(Y)], axis=0)
    g_out = jnp.concatenate([states[i, NS:] for i in range(Y)], axis=0)
    g = gate.astype(F32)
    a = adj.astype(F32)
    sig = sigmoid(g)
    dy = a * g * sig
    vw = v.astype(F32)
    stepw = expand(step)
    u = vw * stepw
    e = expand(jnp.exp(cum))
    d = expand(jnp.exp(cum[TOK - 1 :] - cum))
    dyb, ub = dy.astype(BF16), u.astype(BF16)
    scores = dot(q, keys)
    y_far = e * dot(q, s_in)
    du_far = d * dot(keys, g_out, 0, 0)
    dc = jnp.zeros((TOK, TOK), F32)
    ys, dus, diffs = [], [], []
    for h in range(R):
        at = slice(HEAD * h, HEAD * (h + 1))
        mask = masks_of(cum, cum_t, h)
        z = dot(dyb[:, at], ub[:, at], 1, 1)
        lz = mask * z
        dc = dc + lz
        m = lz * scores
        diffs.append(jnp.sum(m - m.T, axis=1, keepdims=True))
        lc = (mask * scores).astype(BF16)
        ys.append(dot(lc, ub[:, at]))
        dus.append(dot(lc, dyb[:, at], 0, 0))
    y = y_far + jnp.concatenate(ys, axis=1)
    du = du_far + jnp.concatenate(dus, axis=1)
    from_d = head_sums(u * du_far)
    dcum = jnp.concatenate(diffs, axis=1) + head_sums(dy * y_far) - from_d
    kept = jnp.sum(s_in.astype(F32) * g_out.astype(F32), axis=0, keepdims=True)
    dtot = jnp.sum(from_d, axis=0, keepdims=True) + jnp.exp(cum[TOK - 1 :]) * head_sums(kept)
    dla = dot(upper, dcum, precision=HIGH) + dtot
    dstep = head_sums(du * vw) - rate * dla
    decay_grad = dstep * sigmoid(tpre)
    value_grad = (du * stepw).astype(BF16)
    query_grad = (
        dot(dc.astype(BF16), keys, 1, 1) + dot((dy * e).astype(BF16), s_in, 1, 1)
    ).astype(BF16)
    gate_grad = (a * y * (sig * (1.0 + g * (1.0 - sig)))).astype(BF16)
    return value_grad, query_grad, decay_grad, gate_grad


def summed(parts):
    acc = parts[0].astype(F32)
    for i in range(1, parts.shape[0]):
        acc = acc + parts[i].astype(F32)
    return acc


def weight_sum(parts):
    acc = summed(parts)
    squares = jnp.sum(acc * acc, axis=1, keepdims=True)
    return acc, squares


def exchange(parts, axis):
    return lax.all_to_all(parts, axis, split_axis=0, concat_axis=0, tiled=True)


def copies(part, count):
    return jnp.broadcast_to(part[None], (count, *part.shape))


def per_device(
    block_source,
    address_weights,
    causal_filter_taps,
    payload_vectors,
    probe_vectors,
    interval_preimage,
    channel_damping_exponent,
    added_damping_jumps,
    sigmoid_argument,
    adjoint_of_result,
):
    zs = lax.axis_size("z")
    sp = zs * Y
    tp = lax.axis_size("tp")
    features = block_source.shape[1]
    zi = lax.axis_index("z")
    yi = lax.axis_index("y")
    zrow = jnp.full((1, HP), zi, jnp.int32)
    aexp = channel_damping_exponent.reshape(1, R)
    taps_t = causal_filter_taps.T
    taps_own = lax.dynamic_slice(taps_t, (yi * NS, 0), (NS, taps_t.shape[1]))
    small = (interval_preimage, aexp, added_damping_jumps, sigmoid_argument, adjoint_of_result)
    rim = lax.ppermute(block_source[TOK - PAD :], ZY, [(i, i + 1) for i in range(sp - 1)])
    rim = jnp.where(iota2((PAD, 1), 0) >= PAD - 3, rim, jnp.zeros_like(rim))
    bwd_send = local(bwd_local, sds((Y, NS + PAD, HP), BF16), *small, probe_vectors)
    got = exchange(bwd_send, "y")
    xg = exchange(copies(block_source, Y), "y").reshape(Y * TOK, features)
    rows = TOK + 8 * PAD + 2 * NS
    mid_send, keys = local(
        fwd_local,
        [sds((Y, rows, HP), BF16), sds((STATE, TOK), BF16)],
        *small,
        probe_vectors,
        payload_vectors,
        block_source,
        address_weights,
        rim,
        taps_t,
    )
    mid = exchange(mid_send, "y")
    far = exchange(copies(local(bwd_group, sds((NS + PAD, HP), BF16), got), zs), "z")
    width = features // zs
    dw_send, ends, main, over = local(
        bwd_apply,
        [
            sds((zs, NS, width), BF16),
            sds((Y, NS, HP), BF16),
            sds((NS, Y * TOK), F32),
            sds((NS, TOK), F32),
        ],
        far,
        got,
        mid,
        xg,
        taps_own,
        zrow,
    )
    dw_parts = exchange(dw_send, "z")
    fwd_far = exchange(copies(local(fwd_group, sds((NS, HP), BF16), got, mid), zs), "z")
    state_send = local(
        fwd_apply, sds((Y, 2 * NS, HP), BF16), fwd_far, far, got, mid, ends, zrow
    )
    states = exchange(state_send, "y")
    value_grad, query_grad, decay_grad, gate_grad = local(
        finish,
        [sds((TOK, HP), BF16), sds((TOK, STATE), BF16), sds((TOK, R), F32), sds((TOK, HP), BF16)],
        states,
        *small,
        probe_vectors,
        payload_vectors,
        keys,
    )
    dw, squares = local(weight_sum, [sds((NS, width), F32), sds((NS, 1), F32)], dw_parts)
    squares = jnp.broadcast_to(squares.reshape(1, NS), (sp, NS))
    row_squares = jnp.sum(exchange(squares, ZY).reshape(zs, Y * NS), axis=0)
    pieces = jnp.moveaxis(dw.reshape(NS, Y, width // Y), 1, 0)
    key_weight_grad = exchange(pieces, "y").reshape(Y * NS, width // Y)
    after = lax.ppermute(over, "z", [(i, i - 1) for i in range(1, zs)])
    tokens = jnp.moveaxis(main.reshape(NS, Y, TOK), 1, 0)
    tokens = jnp.concatenate([tokens[: Y - 1], tokens[Y - 1 :] + after[None]], axis=0)
    projected_grad = exchange(tokens.astype(BF16), "y").reshape(STATE, TOK)
    partial = dot(address_weights, projected_grad, 0, 0).astype(BF16)
    input_grad = jnp.sum(
        exchange(partial.reshape(tp, features // tp, TOK), "tp").astype(F32), axis=0
    ).astype(BF16)
    return (
        key_weight_grad,
        row_squares,
        input_grad,
        value_grad,
        query_grad,
        decay_grad,
        gate_grad,
    )


def solution(mesh):
    sp, tp = mesh.shape["sp"], mesh.shape["tp"]
    fine = Mesh(mesh.devices.reshape(sp // Y, Y, tp), ("z", "y", "tp"))
    sh = P(ZY, "tp")
    in_specs = (
        P(ZY, None),
        P("tp", None),
        P(None, "tp"),
        sh,
        sh,
        sh,
        P("tp"),
        sh,
        sh,
        sh,
    )
    out_specs = (P("tp", ZY), P("tp"), P("tp", ZY), sh, sh, sh, sh)
    return jax.shard_map(
        per_device, mesh=fine, in_specs=in_specs, out_specs=out_specs, check_vma=False
    )
```

time: 225 us -> 209 us (0.929)
  starting transfers between devices: 108 us -> 54.2 us
  blocking collectives: 0 us -> 43.7 us
  waiting for transfers between devices: 89 us -> 65.3 us
  Pallas kernels: 0 us -> 20.2 us
  matrix products: 5.72 us -> 0.32 us
  local copies, waits for them, and re-layouts: 14.3 us -> 18.6 us
    ppermute x19 -> x2, starting transfers between devices: 81.3 us -> 4.75 us  [the longest x1 3.47 us: per_device(): lax.ppermute(block_source[TOK - PAD:], ZY, [(i, i + 1) for i in range(sp...]
    all_to_all x0 -> x2, blocking collectives: none -> 43.7 us  [exchange(): return lax.all_to_all(parts, axis, split_axis=0, concat_axis=0, tiled=True)]
    ppermute x19 -> x2, waiting for transfers between devices: 39.6 us -> 3.8 us  [the longest x1 3.79 us: per_device(): after = lax.ppermute(over, 'z', [(i, i - 1) for i in range(1, zs)])]
    all_to_all x4 -> x9, starting transfers between devices: 26.6 us -> 49.4 us  [exchange(): return lax.all_to_all(parts, axis, split_axis=0, concat_axis=0, tiled=True)]
    pallas_call x0 -> x8, Pallas kernels: none -> 20.2 us  [local(): pl.pallas_call(kernel, out_shape=shapes, in_specs=[vm] * len(args), out_s...]
    all_to_all x4 -> x9, waiting for transfers between devices: 49.4 us -> 61.5 us  [exchange(): return lax.all_to_all(parts, axis, split_axis=0, concat_axis=0, tiled=True)]
    dot_general x15 -> x1, matrix products: 5.72 us -> 0.32 us  [dot(): lax.dot_general(a, b, (((ca,), (cb,)), ((), ())), preferred_element_type=...]
    broadcast_in_dim x1 -> x5, local copies, waits for them, and re-layouts: 0.63 us -> 4.99 us  [the longest x3 3.8 us: copies(): return jnp.broadcast_to(part[None], (count, *part.shape))]
  transfers between devices with their start and end apart: 23 -> 11, of which waited for: 17 -> 10; matrix products, arithmetic and copies ran while one was open for 7% -> 8% of each run, Pallas kernels for 0% -> 10%
where the time goes in v1:
time: 209 us; the launch traced here: 207 us
  waiting for transfers between devices  65.3 us (31%)
  starting transfers between devices  54.2 us (26%)
  blocking collectives  43.7 us (21%)
  Pallas kernels  20.2 us (10%)
  local copies, waits for them, and re-layouts  18.6 us (9%)
  other arithmetic  4.17 us (2%)
    all_to_all x9, waiting for transfers between devices, exchange(): return lax.all_to_all(parts, axis, split_axis=0, concat_axis=0, tiled=True)  61.5 us
    all_to_all x9, starting transfers between devices, exchange(): return lax.all_to_all(parts, axis, split_axis=0, concat_axis=0, tiled=True)  49.4 us
    all_to_all x2, blocking collectives, exchange(): return lax.all_to_all(parts, axis, split_axis=0, concat_axis=0, tiled=True)  43.7 us
    pallas_call x8, Pallas kernels, local(): pl.pallas_call(kernel, out_shape=shapes, in_specs=[vm] * len(args), out_s...  20.2 us
    unnamed x22, local copies, waits for them, and re-layouts  7.96 us
  transfers between devices with their start and end apart: 11, of which 10 were waited for; matrix products, arithmetic and copies ran while one was open for 8% of the time, Pallas kernels for 10%

profile of v1, /device:TPU:2, one launch (start us, length us, event | category | flops | bytes accessed | tf_op | source)
XLA Modules:
  0.0 207.2 jit_solution(16085873056611352175)
XLA Ops:
  0.6 0.8 slice.10
  1.4 3.5 %collective-permute-start = (bf16[8,2048]{1,0:T(8,128)(2,1)S(1)}, bf16[8,2048]{1,0:T(8,128)(2,1)S(1)}, u32[]{:S(2)}, u32[]{:S(2)}) collective-permute-start(bf16[8,2048]{1,0:T(8,128)(2,1)S(1)} %slice.10), channel_id=1, source_target_pairs={{0,8},{8,16},{16,24},{24,32},{32,40},{40,48},{48,56},{56,64},{64,7... | collective-permute-start | bytes 98312 | tf_op jit(solution)/shard_map/ppermute | solution.py:358
  4.9 1.4 copy.38.refs_0_.refs_1_
  6.3 1.4 copy.39.refs_2_.refs_3_
  7.7 2.2 %bwd_local.1 = bf16[4,40,256]{2,1,0:T(8,128)(2,1)} custom-call(f32[128,4]{1,0:T(8,128)} %copy.38.refs_0_.refs_1_, f32[1,4]{1,0:T(1,128)} %bitcast.32, f32[128,4]{1,0:T(8,128)} %copy.39.refs_2_.refs_3_, bf16[128,256]{1,0:T(8,128)(2,1)} %refs_4_.5, bf16[128,256]{1,0:T(8,128)(2,1)} %refs_5_.5, bf16[128,128]{1,0:T(8,128)(2,1)} %refs_6_.3), custom_call_target="tpu_custom_call" | custom-call | flops 10000000 | bytes 1000000 | tf_op jit(solution)/shard_map/bwd_local/pallas_call | solution.py:57
  9.9 4.3 %all-to-all-start = ((bf16[4,40,256]{2,1,0:T(8,128)(2,1)}), bf16[4,40,256]{2,1,0:T(8,128)(2,1)S(1)}, u32[]{:S(2)}, u32[]{:S(2)}) async-start(bf16[4,40,256]{2,1,0:T(8,128)(2,1)} %bwd_local.1), calls=%async_computation | async-start | bytes 163840 | tf_op jit(solution)/shard_map/all_to_all | solution.py:328
  14.2 1.4 copy.40
  15.6 0.7 broadcast_select_fusion.refs_9_
  16.3 3.4 %fwd_local.1 = (bf16[4,256,256]{2,1,0:T(8,128)(2,1)}, bf16[128,128]{1,0:T(8,128)(2,1)}) custom-call(f32[128,4]{1,0:T(8,128)} %copy.38.refs_0_.refs_1_, f32[1,4]{1,0:T(1,128)} %bitcast.33, f32[128,4]{1,0:T(8,128)} %copy.39.refs_2_.refs_3_, bf16[128,256]{1,0:T(8,128)(2,1)} %refs_4_.5, bf16[128,256]{1,0:T(8,128)(2,1)} %refs_5_.5, bf16[128,128]{1,0:T(8,128)(2,1)} %refs_6_.3, ...), custom_call_target="tpu_custom_call" | custom-call | flops 10000000 | bytes 1000000 | tf_op jit(solution)/shard_map/fwd_local/pallas_call | solution.py:57
  19.9 4.6 %all-to-all-start.2 = ((bf16[4,256,256]{2,1,0:T(8,128)(2,1)}), bf16[4,256,256]{2,1,0:T(8,128)(2,1)S(1)}, u32[]{:S(2)}, u32[]{:S(2)}) async-start(bf16[4,256,256]{2,1,0:T(8,128)(2,1)} %get-tuple-element.19), calls=%async_computation.2 | async-start | bytes 1048576 | tf_op jit(solution)/shard_map/all_to_all | solution.py:328
  24.5 1.5 bwd_group.1
  26.0 7.1 %all-to-all-done.2.refs_2_.refs_1_.refs_3_ = bf16[4,256,256]{2,1,0:T(8,128)(2,1)S(1)} async-done(((bf16[4,256,256]{2,1,0:T(8,128)(2,1)}), bf16[4,256,256]{2,1,0:T(8,128)(2,1)S(1)}, u32[]{:S(2)}, u32[]{:S(2)}) %all-to-all-start.2) | async-done | bytes 524320 | tf_op jit(solution)/shard_map/all_to_all | solution.py:328
  33.2 0.7 broadcast_in_dim.42
  33.9 33.7 %all_to_all.56.refs_0_.refs_1_ = bf16[16,40,256]{2,1,0:T(8,128)(2,1)} all-to-all(bf16[16,40,256]{2,1,0:T(8,128)(2,1)S(1)} %broadcast_in_dim.42), channel_id=1, replica_groups=mesh['z'=16,'y'=4,'tp'=8] {'z'}, dimensions={0} | all-to-all | bytes 655360 | tf_op jit(solution)/shard_map/all_to_all | solution.py:328
  67.6 1.6 broadcast_in_dim.45
  69.2 3.6 %all-to-all-start.3 = ((bf16[4,128,2048]{2,1,0:T(8,128)(2,1)}), bf16[4,128,2048]{2,1,0:T(8,128)(2,1)S(1)}, u32[]{:S(2)}, u32[]{:S(2)}) async-start(bf16[4,128,2048]{2,1,0:T(8,128)(2,1)} %broadcast_in_dim.45), calls=%async_computation.3 | async-start | bytes 4194304 | tf_op jit(solution)/shard_map/all_to_all | solution.py:328
  72.8 1.7 fwd_group.1
  74.5 17.0 %all-to-all-done.3 = bf16[4,128,2048]{2,1,0:T(8,128)(2,1)S(1)} async-done(((bf16[4,128,2048]{2,1,0:T(8,128)(2,1)}), bf16[4,128,2048]{2,1,0:T(8,128)(2,1)S(1)}, u32[]{:S(2)}, u32[]{:S(2)}) %all-to-all-start.3) | async-done | bytes 2097184 | tf_op jit(solution)/shard_map/all_to_all | solution.py:328
  91.5 1.4 broadcast_in_dim.50
  93.0 13.3 %all-to-all-start.9 = ((bf16[16,32,256]{2,1,0:T(8,128)(2,1)}), bf16[16,32,256]{2,1,0:T(8,128)(2,1)S(1)}, u32[]{:S(2)}, u32[]{:S(2)}) async-start(bf16[16,32,256]{2,1,0:T(8,128)(2,1)} %broadcast_in_dim.50), calls=%async_computation.9 | async-start | bytes 524288 | tf_op jit(solution)/shard_map/all_to_all | solution.py:328
  106.3 1.3 dynamic-slice_bitcast_fusion.refs_4_
  108.2 3.7 %bwd_apply.1 = (bf16[16,32,128]{2,1,0:T(8,128)(2,1)}, bf16[4,32,256]{2,1,0:T(8,128)(2,1)}, f32[32,512]{1,0:T(8,128)}, f32[32,128]{1,0:T(8,128)}) custom-call(bf16[16,40,256]{2,1,0:T(8,128)(2,1)} %all_to_all.56.refs_0_.refs_1_, bf16[4,40,256]{2,1,0:T(8,128)(2,1)} %copy-done.4, bf16[4,256,256]{2,1,0:T(8,128)(2,1)} %copy-done.1, bf16[512,2048]{1,0:T(8,128)(2,1)} %bitcast.26, ...), custom_call_target="tpu_custom_call" | custom-call | flops 10000000 | bytes 1000000 | tf_op jit(solution)/shard_map/bwd_apply/pallas_call | solution.py:57
  111.9 1.3 collective-permute-start.1
  113.1 0.8 bitcast_bitcast_fusion
  114.0 3.8 %collective-permute-done.1 = f32[32,128]{1,0:T(8,128)S(1)} collective-permute-done((f32[32,128]{1,0:T(8,128)}, f32[32,128]{1,0:T(8,128)S(1)}, u32[]{:S(2)}, u32[]{:S(2)}) %collective-permute-start.1) | collective-permute-done | bytes 16416 | tf_op jit(solution)/shard_map/ppermute | solution.py:413
  118.4 5.1 %all-to-all-done.9.refs_0_ = bf16[16,32,256]{2,1,0:T(8,128)(2,1)S(1)} async-done(((bf16[16,32,256]{2,1,0:T(8,128)(2,1)}), bf16[16,32,256]{2,1,0:T(8,128)(2,1)S(1)}, u32[]{:S(2)}, u32[]{:S(2)}) %all-to-all-start.9) | async-done | bytes 262176 | tf_op jit(solution)/shard_map/all_to_all | solution.py:328
  123.5 3.3 %all-to-all-start.7 = ((bf16[4,32,128]{2,1,0:T(8,128)(2,1)}), bf16[4,32,128]{2,1,0:T(8,128)(2,1)S(1)}, u32[]{:S(2)}, u32[]{:S(2)}) async-start(bf16[4,32,128]{2,1,0:T(8,128)(2,1)} %pad_maximum_fusion), calls=%async_computation.7 | async-start | bytes 65536 | tf_op jit(solution)/shard_map/all_to_all | solution.py:328
  126.8 2.1 %fwd_apply.1 = bf16[4,64,256]{2,1,0:T(8,128)(2,1)} custom-call(bf16[16,32,256]{2,1,0:T(8,128)(2,1)} %copy-done.5, bf16[16,40,256]{2,1,0:T(8,128)(2,1)} %all_to_all.56.refs_0_.refs_1_, bf16[4,40,256]{2,1,0:T(8,128)(2,1)} %copy-done.4, bf16[4,256,256]{2,1,0:T(8,128)(2,1)} %copy-done.1, bf16[4,32,256]{2,1,0:T(8,128)(2,1)} %get-tuple-element.25.refs_4_, ...), custom_call_target="tpu_custom_call" | custom-call | flops 10000000 | bytes 1000000 | tf_op jit(solution)/shard_map/fwd_apply/pallas_call | solution.py:57
  129.0 3.3 %all-to-all-done.7 = bf16[4,32,128]{2,1,0:T(8,128)(2,1)S(1)} async-done(((bf16[4,32,128]{2,1,0:T(8,128)(2,1)}), bf16[4,32,128]{2,1,0:T(8,128)(2,1)S(1)}, u32[]{:S(2)}, u32[]{:S(2)}) %all-to-all-start.7) | async-done | bytes 32800 | tf_op jit(solution)/shard_map/all_to_all | solution.py:328
  132.2 10.0 %all_to_all.57.refs_0_ = bf16[4,64,256]{2,1,0:T(8,128)(2,1)} all-to-all(bf16[4,64,256]{2,1,0:T(8,128)(2,1)} %fwd_apply.1), channel_id=1, replica_groups=mesh['z'=16,'y'=4,'tp'=8] {'y'}, dimensions={0} | all-to-all | bytes 262144 | tf_op jit(solution)/shard_map/all_to_all | solution.py:328
  142.2 6.8 %all-to-all-start.4 = ((bf16[16,32,128]{2,1,0:T(8,128)(2,1)}), bf16[16,32,128]{2,1,0:T(8,128)(2,1)S(1)}, u32[]{:S(2)}, u32[]{:S(2)}) async-start(bf16[16,32,128]{2,1,0:T(8,128)(2,1)} %get-tuple-element.20), calls=%async_computation.4 | async-start | bytes 262144 | tf_op jit(solution)/shard_map/all_to_all | solution.py:328
  149.3 0.8 copy.59
  150.2 12.0 %all-to-all-done.4.refs_0_ = bf16[16,32,128]{2,1,0:T(8,128)(2,1)S(1)} async-done(((bf16[16,32,128]{2,1,0:T(8,128)(2,1)}), bf16[16,32,128]{2,1,0:T(8,128)(2,1)S(1)}, u32[]{:S(2)}, u32[]{:S(2)}) %all-to-all-start.4) | async-done | bytes 131104 | tf_op jit(solution)/shard_map/all_to_all | solution.py:328
  162.2 4.8 %all-to-all-start.8 = ((bf16[8,256,128]{1,2,0:T(8,128)(2,1)}), bf16[8,256,128]{1,2,0:T(8,128)(2,1)S(1)}, u32[]{:S(2)}, u32[]{:S(2)}) async-start(bf16[8,256,128]{1,2,0:T(8,128)(2,1)} %bitcast.24), calls=%async_computation.8 | async-start | bytes 1048576 | tf_op jit(solution)/shard_map/all_to_all | solution.py:328
  167.0 1.6 weight_sum.1
  168.6 0.8 reshape.58
  169.4 0.7 reshape.74
  170.1 5.7 %all-to-all-done.8 = bf16[8,256,128]{1,2,0:T(8,128)(2,1)S(1)} async-done(((bf16[8,256,128]{1,2,0:T(8,128)(2,1)}), bf16[8,256,128]{1,2,0:T(8,128)(2,1)S(1)}, u32[]{:S(2)}, u32[]{:S(2)}) %all-to-all-start.8) | async-done | bytes 524320 | tf_op jit(solution)/shard_map/all_to_all | solution.py:328
  175.9 3.3 %all-to-all-start.5 = ((f32[4,1,1024]{2,1,0:T(1,128)}), f32[4,1,1024]{2,1,0:T(1,128)S(1)}, u32[]{:S(2)}, u32[]{:S(2)}) async-start(f32[4,1,1024]{2,1,0:T(1,128)} %reshape.74), calls=%async_computation.5 | async-start | bytes 32768 | tf_op jit(solution)/shard_map/all_to_all | solution.py:328
  179.1 0.8 reduce.1
  180.0 4.5 %all-to-all-done.5 = f32[4,1,1024]{2,1,0:T(1,128)S(1)} async-done(((f32[4,1,1024]{2,1,0:T(1,128)}), f32[4,1,1024]{2,1,0:T(1,128)S(1)}, u32[]{:S(2)}, u32[]{:S(2)}) %all-to-all-start.5) | async-done | bytes 16416 | tf_op jit(solution)/shard_map/all_to_all | solution.py:328
  185.1 5.5 %all-to-all-start.6 = ((f32[64,1,32]{2,1,0:T(1,128)}), f32[64,1,32]{2,1,0:T(1,128)S(1)}, u32[]{:S(2)}, u32[]{:S(2)}) async-start(f32[64,1,32]{2,1,0:T(1,128)} %broadcast_in_dim.48), calls=%async_computation.6 | async-start | bytes 65536 | tf_op jit(solution)/shard_map/all_to_all | solution.py:328
  190.6 3.9 %finish.1 = (bf16[128,256]{1,0:T(8,128)(2,1)}, bf16[128,128]{1,0:T(8,128)(2,1)}, f32[128,4]{1,0:T(8,128)}, bf16[128,256]{1,0:T(8,128)(2,1)}) custom-call(bf16[4,64,256]{2,1,0:T(8,128)(2,1)} %all_to_all.57.refs_0_, f32[128,4]{1,0:T(8,128)} %copy.38.refs_0_.refs_1_, f32[1,4]{1,0:T(1,128)} %bitcast.34, f32[128,4]{1,0:T(8,128)} %copy.39.refs_2_.refs_3_, ...), custom_call_target="tpu_custom_call" | custom-call | flops 10000000 | bytes 1000000 | tf_op jit(solution)/shard_map/finish/pallas_call | solution.py:57
  194.5 1.5 copy.52
  196.0 0.7 copy.51
  197.3 0.7 reduce.6
  198.7 6.6 %all-to-all-done.6 = f32[64,1,32]{2,1,0:T(1,128)S(1)} async-done(((f32[64,1,32]{2,1,0:T(1,128)}), f32[64,1,32]{2,1,0:T(1,128)S(1)}, u32[]{:S(2)}, u32[]{:S(2)}) %all-to-all-start.6) | async-done | bytes 8224 | tf_op jit(solution)/shard_map/all_to_all | solution.py:328
  205.9 0.7 reduce.5
  (31 shorter events, 4.9 us)
Async XLA Ops:
  1.4 14.2 %collective-permute-start = (bf16[8,2048]{1,0:T(8,128)(2,1)S(1)}, bf16[8,2048]{1,0:T(8,128)(2,1)S(1)}, u32[]{:S(2)}, u32[]{:S(2)}) collective-permute-start(bf16[8,2048]{1,0:T(8,128)(2,1)S(1)} %slice.10), channel_id=1, source_target_pairs={{0,8},{8,16},{16,24},{24,32},{32,40},{40,48},{48,56},{56,64},{64,7... | collective-permute-start | bytes 98312 | tf_op jit(solution)/shard_map/ppermute | solution.py:358
  7.7 59.9 %copy-start.2 = (bf16[128,2048]{1,0:T(8,128)(2,1)S(1)}, bf16[128,2048]{1,0:T(8,128)(2,1)}, u32[]{:S(2)}) copy-start(bf16[128,2048]{1,0:T(8,128)(2,1)} %refs_7_.2) | copy-start | bytes 1572868
  9.9 10.0 %all-to-all-start = ((bf16[4,40,256]{2,1,0:T(8,128)(2,1)}), bf16[4,40,256]{2,1,0:T(8,128)(2,1)S(1)}, u32[]{:S(2)}, u32[]{:S(2)}) async-start(bf16[4,40,256]{2,1,0:T(8,128)(2,1)} %bwd_local.1), calls=%async_computation | async-start | bytes 163840 | tf_op jit(solution)/shard_map/all_to_all | solution.py:328
  19.9 4.6 %copy-start.4 = (bf16[4,40,256]{2,1,0:T(8,128)(2,1)}, bf16[4,40,256]{2,1,0:T(8,128)(2,1)S(1)}, u32[]{:S(2)}) copy-start(bf16[4,40,256]{2,1,0:T(8,128)(2,1)S(1)} %all-to-all-done.refs_0_.refs_1_.refs_2_) | copy-start | bytes 245764
  19.9 13.2 %all-to-all-start.2 = ((bf16[4,256,256]{2,1,0:T(8,128)(2,1)}), bf16[4,256,256]{2,1,0:T(8,128)(2,1)S(1)}, u32[]{:S(2)}, u32[]{:S(2)}) async-start(bf16[4,256,256]{2,1,0:T(8,128)(2,1)} %get-tuple-element.19), calls=%async_computation.2 | async-start | bytes 1048576 | tf_op jit(solution)/shard_map/all_to_all | solution.py:328
  33.1 36.0 %copy-start.1 = (bf16[4,256,256]{2,1,0:T(8,128)(2,1)}, bf16[4,256,256]{2,1,0:T(8,128)(2,1)S(1)}, u32[]{:S(2)}) copy-start(bf16[4,256,256]{2,1,0:T(8,128)(2,1)S(1)} %all-to-all-done.2.refs_2_.refs_1_.refs_3_) | copy-start | bytes 1572868
  69.2 22.3 %all-to-all-start.3 = ((bf16[4,128,2048]{2,1,0:T(8,128)(2,1)}), bf16[4,128,2048]{2,1,0:T(8,128)(2,1)S(1)}, u32[]{:S(2)}, u32[]{:S(2)}) async-start(bf16[4,128,2048]{2,1,0:T(8,128)(2,1)} %broadcast_in_dim.45), calls=%async_computation.3 | async-start | bytes 4194304 | tf_op jit(solution)/shard_map/all_to_all | solution.py:328
  91.5 16.7 %copy-start = (bf16[4,128,2048]{2,1,0:T(8,128)(2,1)}, bf16[4,128,2048]{2,1,0:T(8,128)(2,1)S(1)}, u32[]{:S(2)}) copy-start(bf16[4,128,2048]{2,1,0:T(8,128)(2,1)S(1)} %all-to-all-done.3) | copy-start | bytes 6291460
  93.0 30.6 %all-to-all-start.9 = ((bf16[16,32,256]{2,1,0:T(8,128)(2,1)}), bf16[16,32,256]{2,1,0:T(8,128)(2,1)S(1)}, u32[]{:S(2)}, u32[]{:S(2)}) async-start(bf16[16,32,256]{2,1,0:T(8,128)(2,1)} %broadcast_in_dim.50), calls=%async_computation.9 | async-start | bytes 524288 | tf_op jit(solution)/shard_map/all_to_all | solution.py:328
  108.2 40.8 %copy-start.3 = (bf16[128,2048]{1,0:T(8,128)(2,1)S(1)}, bf16[128,2048]{1,0:T(8,128)(2,1)}, u32[]{:S(2)}) copy-start(bf16[128,2048]{1,0:T(8,128)(2,1)} %refs_8_.1) | copy-start | bytes 1572868
  111.9 5.9 %collective-permute-start.1 = (f32[32,128]{1,0:T(8,128)}, f32[32,128]{1,0:T(8,128)S(1)}, u32[]{:S(2)}, u32[]{:S(2)}) collective-permute-start(f32[32,128]{1,0:T(8,128)} %get-tuple-element.24), channel_id=1, source_target_pairs={{32,0},{64,32},{96,64},{128,96},{160,128},{192,160},{224,192},{256... | collective-permute-start | bytes 49160 | tf_op jit(solution)/shard_map/ppermute | solution.py:413
  123.5 3.3 %copy-start.5 = (bf16[16,32,256]{2,1,0:T(8,128)(2,1)}, bf16[16,32,256]{2,1,0:T(8,128)(2,1)S(1)}, u32[]{:S(2)}) copy-start(bf16[16,32,256]{2,1,0:T(8,128)(2,1)S(1)} %all-to-all-done.9.refs_0_) | copy-start | bytes 786436
  123.5 8.7 %all-to-all-start.7 = ((bf16[4,32,128]{2,1,0:T(8,128)(2,1)}), bf16[4,32,128]{2,1,0:T(8,128)(2,1)S(1)}, u32[]{:S(2)}, u32[]{:S(2)}) async-start(bf16[4,32,128]{2,1,0:T(8,128)(2,1)} %pad_maximum_fusion), calls=%async_computation.7 | async-start | bytes 65536 | tf_op jit(solution)/shard_map/all_to_all | solution.py:328
  142.2 20.0 %all-to-all-start.4 = ((bf16[16,32,128]{2,1,0:T(8,128)(2,1)}), bf16[16,32,128]{2,1,0:T(8,128)(2,1)S(1)}, u32[]{:S(2)}, u32[]{:S(2)}) async-start(bf16[16,32,128]{2,1,0:T(8,128)(2,1)} %get-tuple-element.20), calls=%async_computation.4 | async-start | bytes 262144 | tf_op jit(solution)/shard_map/all_to_all | solution.py:328
  162.2 4.8 %copy-start.6 = (bf16[16,32,128]{2,1,0:T(8,128)(2,1)}, bf16[16,32,128]{2,1,0:T(8,128)(2,1)S(1)}, u32[]{:S(2)}) copy-start(bf16[16,32,128]{2,1,0:T(8,128)(2,1)S(1)} %all-to-all-done.4.refs_0_) | copy-start | bytes 393220
  162.2 13.7 %all-to-all-start.8 = ((bf16[8,256,128]{1,2,0:T(8,128)(2,1)}), bf16[8,256,128]{1,2,0:T(8,128)(2,1)S(1)}, u32[]{:S(2)}, u32[]{:S(2)}) async-start(bf16[8,256,128]{1,2,0:T(8,128)(2,1)} %bitcast.24), calls=%async_computation.8 | async-start | bytes 1048576 | tf_op jit(solution)/shard_map/all_to_all | solution.py:328
  175.9 8.6 %all-to-all-start.5 = ((f32[4,1,1024]{2,1,0:T(1,128)}), f32[4,1,1024]{2,1,0:T(1,128)S(1)}, u32[]{:S(2)}, u32[]{:S(2)}) async-start(f32[4,1,1024]{2,1,0:T(1,128)} %reshape.74), calls=%async_computation.5 | async-start | bytes 32768 | tf_op jit(solution)/shard_map/all_to_all | solution.py:328
  185.1 20.3 %all-to-all-start.6 = ((f32[64,1,32]{2,1,0:T(1,128)}), f32[64,1,32]{2,1,0:T(1,128)S(1)}, u32[]{:S(2)}, u32[]{:S(2)}) async-start(f32[64,1,32]{2,1,0:T(1,128)} %broadcast_in_dim.48), calls=%async_computation.6 | async-start | bytes 65536 | tf_op jit(solution)/shard_map/all_to_all | solution.py:328

commit v2 on v1

v2 whole, which is shorter than its diff:
```python
import jax
import jax.numpy as jnp
from jax import lax
from jax.experimental import pallas as pl
from jax.experimental.pallas import tpu as pltpu
from jax.sharding import Mesh
from jax.sharding import PartitionSpec as P


TOK = 128
STATE = 128
HEAD = 64
R = 4
HP = R * HEAD
Y = 4
NS = STATE // Y
PAD = 8
HIGH = lax.Precision.HIGHEST
F32 = jnp.float32
BF16 = jnp.bfloat16
PALLAS = True
CORES = 2
ZY = ("z", "y")
VMEM_LIMIT = 16 * 2**20


def dot(a, b, ca=1, cb=0, precision=None):
    return lax.dot_general(
        a, b, (((ca,), (cb,)), ((), ())), preferred_element_type=F32, precision=precision
    )


def roll(a, shift):
    size = a.shape[1]
    if PALLAS:
        return pltpu.roll(a, shift % size, 1)
    return jnp.roll(a, shift, axis=1)


def local(fn, outs, *args, flops=10**7, raw=()):
    single = not isinstance(outs, (list, tuple))
    shapes = [outs] if single else list(outs)
    if not PALLAS:
        res = fn(*args)
        res = [res] if single else list(res)
        for r, s in zip(res, shapes):
            assert r.shape == s.shape and r.dtype == s.dtype, (fn, r, s)
        return res[0] if single else res

    def kernel(*refs):
        ins, dst = refs[: len(args)], refs[len(args) :]
        res = fn(*[r if i in raw else r[...] for i, r in enumerate(ins)])
        res = [res] if single else res
        for ref, val in zip(dst, res):
            ref[...] = val

    vm = pl.BlockSpec(memory_space=pltpu.VMEM)
    res = pl.pallas_call(
        kernel,
        out_shape=shapes,
        in_specs=[vm] * len(args),
        out_specs=[vm] * len(shapes),
        cost_estimate=pl.CostEstimate(flops=flops, bytes_accessed=10**6, transcendentals=0),
        compiler_params=pltpu.CompilerParams(vmem_limit_bytes=VMEM_LIMIT),
    )(*args)
    return res[0] if single else res


def sds(shape, dtype):
    return jax.ShapeDtypeStruct(shape, dtype)


def choose(parts, index):
    res = parts[0]
    for i in range(1, len(parts)):
        res = jnp.where(index == i, parts[i], res)
    return res


def to_peers(parts):
    yi = lax.axis_index("y")
    return [choose(parts, lax.rem(yi + d, Y)) for d in range(Y)]


def from_peers(parts):
    yi = lax.axis_index("y")
    return [choose(parts, lax.rem(yi + Y - j, Y)) for j in range(Y)]


def columns_at(ref, start, size):
    if PALLAS:
        return ref[:, pl.ds(pl.multiple_of(start, size), size)]
    return lax.dynamic_slice_in_dim(ref, start, size, axis=1)


def iota2(shape, dim):
    return lax.broadcasted_iota(jnp.int32, shape, dim)


def expand(a):
    return jnp.concatenate(
        [jnp.broadcast_to(a[:, h : h + 1], (a.shape[0], HEAD)) for h in range(R)], axis=1
    )


def split3(a):
    hi = a.astype(BF16)
    rest = a - hi.astype(F32)
    mid = rest.astype(BF16)
    low = (rest - mid.astype(F32)).astype(BF16)
    return hi, mid, low


def joined(parts, first):
    return (
        parts[:, first].astype(F32)
        + parts[:, first + 1].astype(F32)
        + parts[:, first + 2].astype(F32)
    )


def column(a):
    eye = (iota2((TOK, TOK), 0) == iota2((TOK, TOK), 1)).astype(F32)
    return dot(eye, a, 1, 1, HIGH)


def decays(tpre, aexp, jump):
    step = jnp.log(1.0 + jnp.exp(tpre))
    rate = jnp.exp(aexp)
    la = jump - rate * step
    tri = (iota2((TOK, TOK), 0) >= iota2((TOK, TOK), 1)).astype(F32)
    cum = dot(tri, la, 1, 1, HIGH)
    return step, rate, la, cum


def row_form(la):
    upper = (iota2((TOK, TOK), 0) <= iota2((TOK, TOK), 1)).astype(F32)
    return dot(la, upper, precision=HIGH)


def sigmoid(v):
    return 1.0 / (1.0 + jnp.exp(-v))


def bwd_local(tpre, aexp, jump, gate, adj, q):
    cum = decays(tpre, aexp, jump)[3]
    g = gate.astype(F32)
    dy = adj.astype(F32) * g * sigmoid(g)
    dye = (dy * expand(jnp.exp(cum))).astype(BF16)
    lg = dot(q, dye, 0, 0).astype(BF16)
    hi, mid, low = split3(expand(cum[TOK - 1 :]))
    tail = jnp.concatenate([hi, mid, low, jnp.zeros((PAD - 3, HP), BF16)], axis=0)
    return jnp.stack([jnp.concatenate([lg[NS * i : NS * (i + 1)], tail], axis=0) for i in range(Y)])


def masks_of(cum, cum_t, h):
    causal = iota2((TOK, TOK), 0) >= iota2((TOK, TOK), 1)
    return jnp.exp(jnp.where(causal, cum[:, h : h + 1] - cum_t[h : h + 1, :], -1e30))


def fwd_local(tpre, aexp, jump, gate, adj, q, v, x, w, rim, taps):
    step, _, la, cum = decays(tpre, aexp, jump)
    cum_t = row_form(la)
    taps_t = column(taps)
    rim = jnp.where(iota2(rim.shape, 0) >= PAD - 3, rim.astype(F32), 0.0).astype(BF16)
    g = gate.astype(F32)
    dy = (adj.astype(F32) * g * sigmoid(g)).astype(BF16)
    u = v.astype(F32) * expand(column(step))
    ud = (u * expand(jnp.exp(cum[TOK - 1 :] - cum))).astype(BF16)
    u = u.astype(BF16)
    dc = jnp.zeros((TOK, TOK), F32)
    for h in range(R):
        at = slice(HEAD * h, HEAD * (h + 1))
        dc = dc + masks_of(cum, cum_t, h) * dot(dy[:, at], u[:, at], 1, 1)
    dki = dot(q, dc.astype(BF16), 0, 0)
    proj = dot(w, x, 1, 1).astype(BF16).astype(F32)
    rim_proj = dot(w, rim, 1, 1).astype(BF16)
    place = (iota2((PAD, TOK), 1) == iota2((PAD, TOK), 0) + (TOK - PAD)).astype(BF16)
    rim_full = dot(rim_proj, place)
    lane = iota2((STATE, TOK), 1)
    conv = taps_t[:, 3:4] * proj
    for d in range(1, 4):
        conv = conv + taps_t[:, 3 - d : 4 - d] * roll(
            jnp.where(lane >= TOK - d, rim_full, proj), d
        )
    sig = sigmoid(conv)
    keys = (conv * sig).astype(BF16)
    slope = sig * (1.0 + conv * (1.0 - sig))
    ls = dot(keys, ud).astype(BF16)
    pair = jnp.concatenate([dki.astype(BF16), slope.astype(BF16)], axis=1)
    chunks = [rim[:, HP * i : HP * (i + 1)] for i in range(rim.shape[1] // HP)]
    shared = jnp.concatenate([ud] + chunks, axis=0)
    mids = [
        jnp.concatenate([shared, ls[NS * i : NS * (i + 1)], pair[NS * i : NS * (i + 1)]], axis=0)
        for i in range(Y)
    ]
    return *to_peers(mids), keys


def bwd_group(got):
    tau = joined(got, NS)
    acc = got[Y - 1, :NS].astype(F32)
    for j in range(Y - 2, -1, -1):
        acc = got[j, :NS].astype(F32) + jnp.exp(tau[j : j + 1]) * acc
    hi, mid, low = split3(jnp.sum(tau, axis=0, keepdims=True))
    part = jnp.concatenate(
        [acc.astype(BF16), hi, mid, low, jnp.zeros((PAD - 3, HP), BF16)], axis=0
    )
    return jnp.stack([part] * lax.axis_size("z"))


def fwd_group(got, mid):
    tau = joined(got, NS)
    at = slice(TOK + 8 * PAD, TOK + 8 * PAD + NS)
    acc = mid[0][at].astype(F32)
    for j in range(1, Y):
        acc = mid[j][at].astype(F32) + jnp.exp(tau[j : j + 1]) * acc
    return acc.astype(BF16)


def chain_sums(far):
    count = far.shape[0]
    tau = joined(far, NS)
    tri = (iota2((count, count), 0) >= iota2((count, count), 1)).astype(F32)
    upto = dot(tri, tau, precision=HIGH)
    return tau, upto


def weighted(weights, far):
    acc = weights[0:1] * far[0, :NS].astype(F32)
    for i in range(1, far.shape[0]):
        acc = acc + weights[i : i + 1] * far[i, :NS].astype(F32)
    return acc


def bwd_apply(far, got, m0, m1, m2, m3, x0, x1, x2, x3, taps):
    mid = from_peers([m0, m1, m2, m3])
    yi = lax.axis_index("y")
    zrow = lax.axis_index("z")
    mine = iota2((NS, STATE), 1) == iota2((NS, STATE), 0) + NS * lax.axis_index("y")
    taps_own = dot(mine.astype(F32), taps, 1, 1, HIGH)
    count = far.shape[0]
    tau, upto = chain_sums(far)
    row = iota2((count, HP), 0)
    mine = jnp.sum(jnp.where(row == zrow, upto, 0.0), axis=0, keepdims=True)
    weights = jnp.exp(jnp.where(row > zrow, upto - tau - mine, -1e30))
    state = weighted(weights, far)
    tau_j = joined(got, NS)
    ends = [None] * Y
    for j in range(Y - 1, -1, -1):
        ends[j] = state.astype(BF16)
        if j:
            state = got[j, :NS].astype(F32) + jnp.exp(tau_j[j : j + 1]) * state
    own = TOK + 8 * PAD + NS
    cg = []
    for j in range(Y):
        dk = dot(ends[j], mid[j][:TOK], 1, 1) + mid[j][own : own + NS, :TOK].astype(F32)
        cg.append(dk * mid[j][own : own + NS, TOK:].astype(F32))
    cg = jnp.concatenate(cg, axis=1)
    size = Y * TOK
    lane = iota2((NS, size), 1)
    main = taps_own[:, 3:4] * cg
    over = jnp.zeros_like(main)
    for d in range(1, 4):
        moved = taps_own[:, 3 - d : 4 - d] * roll(cg, -d)
        main = main + jnp.where(lane < size - d, moved, 0.0)
        over = over + jnp.where(lane >= size - d, moved, 0.0)
    rims = jnp.concatenate(
        [mid[0][TOK + PAD * i : TOK + PAD * (i + 1)] for i in range(8)], axis=1
    )
    over = over[:, size - TOK :]
    zero = jnp.zeros((TOK - PAD, rims.shape[1]), BF16)
    dw = dot(over.astype(BF16), jnp.concatenate([zero, rims], axis=0))
    pg = main.astype(BF16)
    pg = [pg[:, TOK * i : TOK * (i + 1)] for i in range(Y)]
    for d, part in enumerate((x0, x1, x2, x3)):
        dw = dw + dot(choose(pg, lax.rem(yi + Y - d, Y)), part)
    width = dw.shape[1] // count
    dw = dw.astype(BF16)
    fwd = fwd_group(got, mid)
    send = jnp.stack(
        [
            jnp.concatenate([dw[:, width * i : width * (i + 1)], fwd], axis=1)
            for i in range(count)
        ]
    )
    return send, jnp.stack(ends), main, over


def fwd_apply(near, bfar, got, m0, m1, m2, m3, ends):
    mid = from_peers([m0, m1, m2, m3])
    far = near[:, :, near.shape[2] - HP :]
    zrow = lax.axis_index("z")
    count = far.shape[0]
    tau, upto = chain_sums(bfar)
    row = iota2((count, HP), 0)
    before = jnp.sum(jnp.where(row == zrow, upto - tau, 0.0), axis=0, keepdims=True)
    weights = jnp.exp(jnp.where(row < zrow, before - upto, -1e30))
    state = weighted(weights, far)
    tau_j = joined(got, NS)
    at = slice(TOK + 8 * PAD, TOK + 8 * PAD + NS)
    res = []
    for j in range(Y):
        res.append(jnp.concatenate([state.astype(BF16), ends[j]], axis=0))
        if j < Y - 1:
            state = mid[j][at].astype(F32) + jnp.exp(tau_j[j : j + 1]) * state
    return to_peers(res)


def finish(p0, p1, p2, p3, tpre, aexp, jump, gate, adj, q, v, keys):
    step, rate, la, cum = decays(tpre, aexp, jump)
    cum_t = row_form(la)
    states = from_peers([p0, p1, p2, p3])
    s_in = jnp.concatenate([part[:NS] for part in states], axis=0)
    g_out = jnp.concatenate([part[NS:] for part in states], axis=0)
    g = gate.astype(F32)
    a = adj.astype(F32)
    sig = sigmoid(g)
    dy = a * g * sig
    vw = v.astype(F32)
    stepw = expand(column(step))
    u = vw * stepw
    e = expand(jnp.exp(cum))
    d = expand(jnp.exp(cum[TOK - 1 :] - cum))
    dyb, ub = dy.astype(BF16), u.astype(BF16)
    scores = dot(q, keys)
    y_far = e * dot(q, s_in)
    du_far = d * dot(keys, g_out, 0, 0)
    dc = jnp.zeros((TOK, TOK), F32)
    ys, dus, diffs = [], [], []
    for h in range(R):
        at = slice(HEAD * h, HEAD * (h + 1))
        mask = masks_of(cum, cum_t, h)
        z = dot(dyb[:, at], ub[:, at], 1, 1)
        lz = mask * z
        dc = dc + lz
        m = lz * scores
        diffs.append(jnp.sum(m.T - m, axis=0, keepdims=True))
        lc = (mask * scores).astype(BF16)
        ys.append(dot(lc, ub[:, at]))
        dus.append(dot(lc, dyb[:, at], 0, 0))
    y = y_far + jnp.concatenate(ys, axis=1)
    du = du_far + jnp.concatenate(dus, axis=1)
    pick = (iota2((R, HP), 1) // HEAD == iota2((R, HP), 0)).astype(F32)
    from_d = dot(pick, u * du_far, 1, 1, HIGH)
    dcum = jnp.concatenate(diffs, axis=0) + dot(pick, dy * y_far, 1, 1, HIGH) - from_d
    kept = jnp.sum(s_in.astype(F32) * g_out.astype(F32), axis=0, keepdims=True)
    kept = kept * expand(jnp.exp(cum[TOK - 1 :]))
    dtot = jnp.sum(from_d, axis=1, keepdims=True) + jnp.sum(pick * kept, axis=1, keepdims=True)
    later = (iota2((TOK, TOK), 0) >= iota2((TOK, TOK), 1)).astype(F32)
    dla = dot(dcum, later, precision=HIGH) + dtot
    dstep = dot(pick, du * vw, 1, 1, HIGH) - rate * dla
    decay_grad = dstep * sigmoid(tpre)
    value_grad = (du * stepw).astype(BF16)
    query_grad = (
        dot(dc.astype(BF16), keys, 1, 1) + dot((dy * e).astype(BF16), s_in, 1, 1)
    ).astype(BF16)
    gate_grad = (a * y * (sig * (1.0 + g * (1.0 - sig)))).astype(BF16)
    return value_grad, query_grad, decay_grad, gate_grad


def summed(parts):
    acc = parts[0].astype(F32)
    for i in range(1, parts.shape[0]):
        acc = acc + parts[i].astype(F32)
    return acc


def weight_sum(near):
    acc = summed(near[:, :, : near.shape[2] - HP])
    count = lax.axis_size("z") * Y
    place = iota2((NS, STATE), 1) == iota2((NS, STATE), 0) + NS * lax.axis_index("y")
    placed = dot(acc, place.astype(F32), 0, 0, HIGH)
    width = placed.shape[0] // Y
    pieces = to_peers([placed[width * i : width * (i + 1)] for i in range(Y)])
    squares = jnp.sum(placed * placed, axis=0, keepdims=True)
    return *pieces, jnp.broadcast_to(squares[None], (count, 1, STATE))


def own_tokens(main, after):
    last = Y * TOK - TOK
    whole = jnp.concatenate([main[:, :last], main[:, last:] + after], axis=1).astype(BF16)
    return to_peers([whole[:, TOK * i : TOK * (i + 1)] for i in range(Y)])


def partial_input(w, p0, p1, p2, p3):
    grad = jnp.concatenate(from_peers([p0, p1, p2, p3]), axis=0)
    count = lax.axis_size("tp")
    chips = count // CORES
    width = w.shape[1] // count
    place = lax.axis_index("tp")
    core = lax.rem(place, CORES)
    chip = lax.div(place, CORES)
    res = []
    for side in range(CORES):
        owner = lax.rem(core + side, CORES)
        blocks = []
        for d in range(chips):
            rank = lax.rem(chip + d, chips) * CORES + owner
            blocks.append(dot(columns_at(w, rank * width, width), grad, 0, 0).astype(BF16))
        res.append(jnp.stack(blocks))
    return res


def core_sum(mine, other):
    return [
        (mine[i].astype(F32) + other[i].astype(F32)).astype(BF16) for i in range(mine.shape[0])
    ]


def piece_sum(*parts):
    return summed(jnp.stack(parts))


def input_sum(*parts):
    acc = parts[0].astype(F32)
    for part in parts[1:]:
        acc = acc + part.astype(F32)
    return acc.astype(BF16)


def piece_sum(*parts):
    acc = parts[0]
    for part in parts[1:]:
        acc = acc + part
    return acc


def square_sum(parts):
    return jnp.sum(parts[:, 0, :], axis=0, keepdims=True)


def exchange(parts, axis):
    return lax.all_to_all(parts, axis, split_axis=0, concat_axis=0, tiled=True)


def around(parts, axis, step):
    count = lax.axis_size(axis)
    ring = count // step
    got = [parts[0]]
    for d in range(1, ring):
        route = [(i, (i + d * step) % count) for i in range(count)]
        got.append(lax.ppermute(parts[d], axis, route))
    return got


def per_device(
    block_source,
    address_weights,
    causal_filter_taps,
    payload_vectors,
    probe_vectors,
    interval_preimage,
    channel_damping_exponent,
    added_damping_jumps,
    sigmoid_argument,
    adjoint_of_result,
):
    return step(
        block_source,
        address_weights,
        causal_filter_taps,
        payload_vectors,
        probe_vectors,
        interval_preimage.T,
        channel_damping_exponent.reshape(R, 1),
        added_damping_jumps.T,
        sigmoid_argument,
        adjoint_of_result,
    )


def step(x, w, taps, v, q, tpre, aexp, jump, gate, adj):
    zs = lax.axis_size("z")
    sp = zs * Y
    tp = lax.axis_size("tp")
    features = x.shape[1]
    width = features // zs
    small = (tpre, aexp, jump, gate, adj)
    bwd_send = local(bwd_local, sds((Y, NS + PAD, HP), BF16), *small, q)
    got = exchange(bwd_send, "y")
    rim = lax.ppermute(x[TOK - PAD :], ZY, [(i, i + 1) for i in range(sp - 1)])
    xs = around([x] * Y, "y", 1)
    rows = TOK + 8 * PAD + 2 * NS
    *mids, keys = local(
        fwd_local,
        [sds((rows, HP), BF16)] * Y + [sds((STATE, TOK), BF16)],
        *small,
        q,
        v,
        x,
        w,
        rim,
        taps,
    )
    mids = around(mids, "y", 1)
    bwd_totals = local(bwd_group, sds((zs, NS + PAD, HP), BF16), got)
    far = exchange(bwd_totals, "z")
    near_send, ends, main, over = local(
        bwd_apply,
        [
            sds((zs, NS, width + HP), BF16),
            sds((Y, NS, HP), BF16),
            sds((NS, Y * TOK), F32),
            sds((NS, TOK), F32),
        ],
        far,
        got,
        *mids,
        *xs,
        taps,
    )
    near = exchange(near_send, "z")
    after = lax.ppermute(over, "z", [(i, i - 1) for i in range(1, zs)])
    tokens = local(own_tokens, [sds((NS, TOK), BF16)] * Y, main, after)
    tokens = around(tokens, "y", 1)
    chips = tp // CORES
    share = (features // tp, TOK)
    sides = local(partial_input, [sds((chips, *share), BF16)] * CORES, w, *tokens, raw=(0,))
    swap = [(i, i ^ 1) for i in range(tp)]
    other = lax.ppermute(sides[-1], "tp", swap) if CORES > 1 else None
    *pieces, squares = local(
        weight_sum, [sds((width // Y, STATE), F32)] * Y + [sds((sp, 1, STATE), F32)], near
    )
    squares = exchange(squares, ZY)
    states = local(fwd_apply, [sds((2 * NS, HP), BF16)] * Y, near, far, got, *mids, ends)
    states = around(states, "y", 1)
    if CORES > 1:
        shares = local(core_sum, [sds(share, BF16)] * chips, sides[0], other)
    else:
        shares = [sides[0][i] for i in range(chips)]
    shares = around(shares, "tp", CORES)
    pieces = around(pieces, "y", 1)
    value_grad, query_grad, decay_grad, gate_grad = local(
        finish,
        [sds((TOK, HP), BF16), sds((TOK, STATE), BF16), sds((R, TOK), F32), sds((TOK, HP), BF16)],
        *states,
        *small,
        q,
        v,
        keys,
    )
    input_grad = local(input_sum, sds(share, BF16), *shares)
    key_weight_grad = local(piece_sum, sds((width // Y, STATE), F32), *pieces).T
    row_squares = local(square_sum, sds((1, STATE), F32), squares).reshape(STATE)
    return (
        key_weight_grad,
        row_squares,
        input_grad,
        value_grad,
        query_grad,
        decay_grad.T,
        gate_grad,
    )


def solution(mesh):
    sp, tp = mesh.shape["sp"], mesh.shape["tp"]
    fine = Mesh(mesh.devices.reshape(sp // Y, Y, tp), ("z", "y", "tp"))
    sh = P(ZY, "tp")
    in_specs = (
        P(ZY, None),
        P("tp", None),
        P(None, "tp"),
        sh,
        sh,
        sh,
        P("tp"),
        sh,
        sh,
        sh,
    )
    out_specs = (P("tp", ZY), P("tp"), P("tp", ZY), sh, sh, sh, sh)
    return jax.shard_map(
        per_device, mesh=fine, in_specs=in_specs, out_specs=out_specs, check_vma=False
    )
```

time: 209 us -> 180 us (0.86)
  the two profiles are of different devices: /device:TPU:2 before, /device:TPU:24 now
where the time goes in v2:
time: 180 us; the launch traced here: 179 us
  starting transfers between devices  107 us (59%)
  waiting for transfers between devices  39 us (22%)
  blocking collectives  11.7 us (6%)
  local copies, waits for them, and re-layouts  10.1 us (6%)
  Pallas kernels  9.67 us (5%)
    ppermute x18, starting transfers between devices, around(): got.append(lax.ppermute(parts[d], axis, route))  59.9 us
    all_to_all x3, starting transfers between devices, exchange(): return lax.all_to_all(parts, axis, split_axis=0, concat_axis=0, tiled=True)  38.8 us
    ppermute x1, waiting for transfers between devices, step(): after = lax.ppermute(over, 'z', [(i, i - 1) for i in range(1, zs)])  14.9 us
    ppermute x18, waiting for transfers between devices, around(): got.append(lax.ppermute(parts[d], axis, route))  12.6 us
    all_to_all x1, blocking collectives, exchange(): return lax.all_to_all(parts, axis, split_axis=0, concat_axis=0, tiled=True)  11.7 us
    ppermute x1, waiting for transfers between devices, step(): rim = lax.ppermute(x[TOK - PAD:], ZY, [(i, i + 1) for i in range(sp - 1)])  11.4 us
    unnamed x76, local copies, waits for them, and re-layouts  9.98 us
    pallas_call x13, Pallas kernels, local(): pl.pallas_call(kernel, out_shape=shapes, in_specs=[vm] * len(args), out_s...  9.67 us
  transfers between devices with their start and end apart: 24, of which 7 were waited for; matrix products, arithmetic and copies ran while one was open for 0% of the time, Pallas kernels for 4%

profile of v2, /device:TPU:24, one launch (start us, length us, event | category | flops | bytes accessed | tf_op | source)
XLA Modules:
  0.0 179.0 jit_solution(7491952553516646820)
XLA Ops:
  0.6 0.6 copy-done.37
  2.1 0.8 copy-done.2
  2.9 0.8 copy-done.4
  3.8 0.8 copy-done.16
  5.1 11.7 %all_to_all.20.refs_0_.refs_1_.refs_2_ = bf16[4,40,256]{2,1,0:T(8,128)(2,1)S(1)} all-to-all(bf16[4,40,256]{2,1,0:T(8,128)(2,1)S(1)} %shard_map.153), channel_id=1, replica_groups=mesh['z'=16,'y'=4,'tp'=8] {'y'}, dimensions={0} | all-to-all | bytes 163840 | tf_op jit(solution)/shard_map/all_to_all | solution.py:434
  16.9 0.8 shard_map.154
  17.7 11.9 %all-to-all-start.1 = ((bf16[16,40,256]{2,1,0:T(8,128)(2,1)}), bf16[16,40,256]{2,1,0:T(8,128)(2,1)S(1)}, u32[]{:S(2)}, u32[]{:S(2)}) async-start(bf16[16,40,256]{2,1,0:T(8,128)(2,1)} %shard_map.154), calls=%async_computation.1 | async-start | bytes 655360 | tf_op jit(solution)/shard_map/all_to_all | solution.py:434
  29.6 4.1 %collective-permute-start.5 = (bf16[128,2048]{1,0:T(8,128)(2,1)S(1)}, bf16[128,2048]{1,0:T(8,128)(2,1)S(1)}, u32[]{:S(2)}, u32[]{:S(2)}) collective-permute-start(bf16[128,2048]{1,0:T(8,128)(2,1)S(1)} %copy-done), channel_id=1, source_target_pairs={{0,16},{8,24},{16,0},{24,8},{1,17},{9,25},{17,1},{25,9},{2,18},{10... | collective-permute-start | bytes 1572872 | tf_op jit(solution)/shard_map/ppermute | solution.py:443
  33.7 2.9 %collective-permute-start.4 = (bf16[128,2048]{1,0:T(8,128)(2,1)S(1)}, bf16[128,2048]{1,0:T(8,128)(2,1)S(1)}, u32[]{:S(2)}, u32[]{:S(2)}) collective-permute-start(bf16[128,2048]{1,0:T(8,128)(2,1)S(1)} %copy-done), channel_id=1, source_target_pairs={{0,8},{8,16},{16,24},{24,0},{1,9},{9,17},{17,25},{25,1},{2,10},{10... | collective-permute-start | bytes 1572872 | tf_op jit(solution)/shard_map/ppermute | solution.py:443
  36.5 3.0 %collective-permute-start.6 = (bf16[128,2048]{1,0:T(8,128)(2,1)S(1)}, bf16[128,2048]{1,0:T(8,128)(2,1)S(1)}, u32[]{:S(2)}, u32[]{:S(2)}) collective-permute-start(bf16[128,2048]{1,0:T(8,128)(2,1)S(1)} %copy-done), channel_id=1, source_target_pairs={{0,24},{8,0},{16,8},{24,16},{1,25},{9,1},{17,9},{25,17},{2,26},{10... | collective-permute-start | bytes 1572872 | tf_op jit(solution)/shard_map/ppermute | solution.py:443
  39.5 5.4 %collective-permute-start = (bf16[8,2048]{1,0:T(8,128)(2,1)S(1)}, bf16[8,2048]{1,0:T(8,128)(2,1)S(1)}, u32[]{:S(2)}, u32[]{:S(2)}) collective-permute-start(bf16[8,2048]{1,0:T(8,128)(2,1)S(1)} %slice.3), channel_id=1, source_target_pairs={{0,8},{8,16},{16,24},{24,32},{32,40},{40,48},{48,56},{56,64},{64,7... | collective-permute-start | bytes 98312 | tf_op jit(solution)/shard_map/ppermute | solution.py:482
  45.0 11.4 %collective-permute-done.refs_9_ = bf16[8,2048]{1,0:T(8,128)(2,1)S(1)} collective-permute-done((bf16[8,2048]{1,0:T(8,128)(2,1)S(1)}, bf16[8,2048]{1,0:T(8,128)(2,1)S(1)}, u32[]{:S(2)}, u32[]{:S(2)}) %collective-permute-start) | collective-permute-done | bytes 32800 | tf_op jit(solution)/shard_map/ppermute | solution.py:482
  56.5 1.6 shard_map.155
  58.7 1.9 %collective-permute-start.1 = (bf16[256,256]{1,0:T(8,128)(2,1)S(1)}, bf16[256,256]{1,0:T(8,128)(2,1)S(1)}, u32[]{:S(2)}, u32[]{:S(2)}) collective-permute-start(bf16[256,256]{1,0:T(8,128)(2,1)S(1)} %get-tuple-element.40), channel_id=1, source_target_pairs={{0,8},{8,16},{16,24},{24,0},{1,9},{9,17},{17,25},{25,1},{2,10},{10... | collective-permute-start | bytes 393224 | tf_op jit(solution)/shard_map/ppermute | solution.py:443
  60.6 4.9 %collective-permute-start.2 = (bf16[256,256]{1,0:T(8,128)(2,1)S(1)}, bf16[256,256]{1,0:T(8,128)(2,1)S(1)}, u32[]{:S(2)}, u32[]{:S(2)}) collective-permute-start(bf16[256,256]{1,0:T(8,128)(2,1)S(1)} %get-tuple-element.41), channel_id=1, source_target_pairs={{0,16},{8,24},{16,0},{24,8},{1,17},{9,25},{17,1},{25,9},{2,18},{10... | collective-permute-start | bytes 393224 | tf_op jit(solution)/shard_map/ppermute | solution.py:443
  65.5 0.9 collective-permute-done.1.refs_3_.refs_4_
  66.3 2.4 %collective-permute-start.3 = (bf16[256,256]{1,0:T(8,128)(2,1)S(1)}, bf16[256,256]{1,0:T(8,128)(2,1)S(1)}, u32[]{:S(2)}, u32[]{:S(2)}) collective-permute-start(bf16[256,256]{1,0:T(8,128)(2,1)S(1)} %get-tuple-element.42), channel_id=1, source_target_pairs={{0,24},{8,0},{16,8},{24,16},{1,25},{9,1},{17,9},{25,17},{2,26},{10... | collective-permute-start | bytes 393224 | tf_op jit(solution)/shard_map/ppermute | solution.py:443
  68.9 5.5 %collective-permute-done.3.refs_5_.refs_6_ = bf16[256,256]{1,0:T(8,128)(2,1)S(1)} collective-permute-done((bf16[256,256]{1,0:T(8,128)(2,1)S(1)}, bf16[256,256]{1,0:T(8,128)(2,1)S(1)}, u32[]{:S(2)}, u32[]{:S(2)}) %collective-permute-start.3) | collective-permute-done | bytes 131104 | tf_op jit(solution)/shard_map/ppermute | solution.py:443
  74.4 0.6 copy-done.12
  75.1 0.9 copy-done.13
  76.0 0.7 copy-done.34
  76.7 1.0 shard_map.156
  77.7 0.8 copy-done.15
  78.4 0.6 copy-done.21
  79.1 0.6 copy-done.23
  80.3 11.9 %all-to-all-start.2 = ((bf16[16,32,384]{2,1,0:T(8,128)(2,1)}), bf16[16,32,384]{2,1,0:T(8,128)(2,1)S(1)}, u32[]{:S(2)}, u32[]{:S(2)}) async-start(bf16[16,32,384]{2,1,0:T(8,128)(2,1)} %copy-done.15), calls=%async_computation.2 | async-start | bytes 786432 | tf_op jit(solution)/shard_map/all_to_all | solution.py:434
  92.2 1.3 collective-permute-start.10
  93.5 14.9 %collective-permute-done.10.refs_1_ = f32[32,128]{1,0:T(8,128)S(1)} collective-permute-done((f32[32,128]{1,0:T(8,128)S(1)}, f32[32,128]{1,0:T(8,128)S(1)}, u32[]{:S(2)}, u32[]{:S(2)}) %collective-permute-start.10) | collective-permute-done | bytes 16416 | tf_op jit(solution)/shard_map/ppermute | solution.py:514
  108.5 1.9 %collective-permute-start.11 = (bf16[32,128]{1,0:T(8,128)(2,1)S(1)}, bf16[32,128]{1,0:T(8,128)(2,1)S(1)}, u32[]{:S(2)}, u32[]{:S(2)}) collective-permute-start(bf16[32,128]{1,0:T(8,128)(2,1)S(1)} %get-tuple-element.52), channel_id=1, source_target_pairs={{0,8},{8,16},{16,24},{24,0},{1,9},{9,17},{17,25},{25,1},{2,10},{10... | collective-permute-start | bytes 24584 | tf_op jit(solution)/shard_map/ppermute | solution.py:443
  110.4 4.3 %collective-permute-start.12 = (bf16[32,128]{1,0:T(8,128)(2,1)S(1)}, bf16[32,128]{1,0:T(8,128)(2,1)S(1)}, u32[]{:S(2)}, u32[]{:S(2)}) collective-permute-start(bf16[32,128]{1,0:T(8,128)(2,1)S(1)} %get-tuple-element.53), channel_id=1, source_target_pairs={{0,16},{8,24},{16,0},{24,8},{1,17},{9,25},{17,1},{25,9},{2,18},{10... | collective-permute-start | bytes 24584 | tf_op jit(solution)/shard_map/ppermute | solution.py:443
  114.7 3.3 %collective-permute-start.13 = (bf16[32,128]{1,0:T(8,128)(2,1)S(1)}, bf16[32,128]{1,0:T(8,128)(2,1)S(1)}, u32[]{:S(2)}, u32[]{:S(2)}) collective-permute-start(bf16[32,128]{1,0:T(8,128)(2,1)S(1)} %get-tuple-element.54), channel_id=1, source_target_pairs={{0,24},{8,0},{16,8},{24,16},{1,25},{9,1},{17,9},{25,17},{2,26},{10... | collective-permute-start | bytes 24584 | tf_op jit(solution)/shard_map/ppermute | solution.py:443
  118.1 3.4 %collective-permute-done.13.refs_4_ = bf16[32,128]{1,0:T(8,128)(2,1)S(1)} collective-permute-done((bf16[32,128]{1,0:T(8,128)(2,1)S(1)}, bf16[32,128]{1,0:T(8,128)(2,1)S(1)}, u32[]{:S(2)}, u32[]{:S(2)}) %collective-permute-start.13) | collective-permute-done | bytes 8224 | tf_op jit(solution)/shard_map/ppermute | solution.py:443
  121.8 1.9 %collective-permute-start.14 = (bf16[4,256,128]{2,1,0:T(8,128)(2,1)S(1)}, bf16[4,256,128]{2,1,0:T(8,128)(2,1)S(1)}, u32[]{:S(2)}, u32[]{:S(2)}) collective-permute-start(bf16[4,256,128]{2,1,0:T(8,128)(2,1)S(1)} %get-tuple-element.56), channel_id=1, source_target_pairs={{0,1},{1,0},{2,3},{3,2},{4,5},{5,4},{6,7},{7,6},{8,9},{9,8},{10,11... | collective-permute-start | bytes 786440 | tf_op jit(solution)/shard_map/ppermute | solution.py:521
  123.8 0.9 shard_map.157
  124.7 15.0 %all-to-all-start.3 = ((f32[64,1,128]{2,1,0:T(1,128)}), f32[64,1,128]{2,1,0:T(1,128)S(1)}, u32[]{:S(2)}, u32[]{:S(2)}) async-start(f32[64,1,128]{2,1,0:T(1,128)} %get-tuple-element.48), calls=%async_computation.3 | async-start | bytes 65536 | tf_op jit(solution)/shard_map/all_to_all | solution.py:434
  139.9 3.5 %collective-permute-start.15 = (bf16[256,128]{1,0:T(8,128)(2,1)S(1)}, bf16[256,128]{1,0:T(8,128)(2,1)S(1)}, u32[]{:S(2)}, u32[]{:S(2)}) collective-permute-start(bf16[256,128]{1,0:T(8,128)(2,1)S(1)} %get-tuple-element.58), channel_id=1, source_target_pairs={{0,2},{1,3},{2,4},{3,5},{4,6},{5,7},{6,0},{7,1},{8,10},{9,11},{10,... | collective-permute-start | bytes 196616 | tf_op jit(solution)/shard_map/ppermute | solution.py:443
  143.4 4.6 %collective-permute-start.16 = (bf16[256,128]{1,0:T(8,128)(2,1)S(1)}, bf16[256,128]{1,0:T(8,128)(2,1)S(1)}, u32[]{:S(2)}, u32[]{:S(2)}) collective-permute-start(bf16[256,128]{1,0:T(8,128)(2,1)S(1)} %get-tuple-element.59), channel_id=1, source_target_pairs={{0,4},{1,5},{2,6},{3,7},{4,0},{5,1},{6,2},{7,3},{8,12},{9,13},{10,... | collective-permute-start | bytes 196616 | tf_op jit(solution)/shard_map/ppermute | solution.py:443
  148.0 3.3 %collective-permute-start.17 = (bf16[256,128]{1,0:T(8,128)(2,1)S(1)}, bf16[256,128]{1,0:T(8,128)(2,1)S(1)}, u32[]{:S(2)}, u32[]{:S(2)}) collective-permute-start(bf16[256,128]{1,0:T(8,128)(2,1)S(1)} %get-tuple-element.60), channel_id=1, source_target_pairs={{0,6},{1,7},{2,0},{3,1},{4,2},{5,3},{6,4},{7,5},{8,14},{9,15},{10,... | collective-permute-start | bytes 196616 | tf_op jit(solution)/shard_map/ppermute | solution.py:443
  151.4 2.4 %collective-permute-start.7 = (f32[32,128]{1,0:T(8,128)S(1)}, f32[32,128]{1,0:T(8,128)S(1)}, u32[]{:S(2)}, u32[]{:S(2)}) collective-permute-start(f32[32,128]{1,0:T(8,128)S(1)} %get-tuple-element.45), channel_id=1, source_target_pairs={{0,8},{8,16},{16,24},{24,0},{1,9},{9,17},{17,25},{25,1},{2,10},{10... | collective-permute-start | bytes 49160 | tf_op jit(solution)/shard_map/ppermute | solution.py:443
  154.1 3.5 %collective-permute-start.18 = (bf16[64,256]{1,0:T(8,128)(2,1)S(1)}, bf16[64,256]{1,0:T(8,128)(2,1)S(1)}, u32[]{:S(2)}, u32[]{:S(2)}) collective-permute-start(bf16[64,256]{1,0:T(8,128)(2,1)S(1)} %get-tuple-element.63), channel_id=1, source_target_pairs={{0,8},{8,16},{16,24},{24,0},{1,9},{9,17},{17,25},{25,1},{2,10},{10... | collective-permute-start | bytes 98312 | tf_op jit(solution)/shard_map/ppermute | solution.py:443
  157.6 4.0 %collective-permute-start.19 = (bf16[64,256]{1,0:T(8,128)(2,1)S(1)}, bf16[64,256]{1,0:T(8,128)(2,1)S(1)}, u32[]{:S(2)}, u32[]{:S(2)}) collective-permute-start(bf16[64,256]{1,0:T(8,128)(2,1)S(1)} %get-tuple-element.64), channel_id=1, source_target_pairs={{0,16},{8,24},{16,0},{24,8},{1,17},{9,25},{17,1},{25,9},{2,18},{10... | collective-permute-start | bytes 98312 | tf_op jit(solution)/shard_map/ppermute | solution.py:443
  161.6 2.2 %collective-permute-start.20 = (bf16[64,256]{1,0:T(8,128)(2,1)S(1)}, bf16[64,256]{1,0:T(8,128)(2,1)S(1)}, u32[]{:S(2)}, u32[]{:S(2)}) collective-permute-start(bf16[64,256]{1,0:T(8,128)(2,1)S(1)} %get-tuple-element.65), channel_id=1, source_target_pairs={{0,24},{8,0},{16,8},{24,16},{1,25},{9,1},{17,9},{25,17},{2,26},{10... | collective-permute-start | bytes 98312 | tf_op jit(solution)/shard_map/ppermute | solution.py:443
  163.8 4.2 %collective-permute-start.8 = (f32[32,128]{1,0:T(8,128)S(1)}, f32[32,128]{1,0:T(8,128)S(1)}, u32[]{:S(2)}, u32[]{:S(2)}) collective-permute-start(f32[32,128]{1,0:T(8,128)S(1)} %get-tuple-element.46), channel_id=1, source_target_pairs={{0,16},{8,24},{16,0},{24,8},{1,17},{9,25},{17,1},{25,9},{2,18},{10... | collective-permute-start | bytes 49160 | tf_op jit(solution)/shard_map/ppermute | solution.py:443
  168.0 3.5 %collective-permute-start.9 = (f32[32,128]{1,0:T(8,128)S(1)}, f32[32,128]{1,0:T(8,128)S(1)}, u32[]{:S(2)}, u32[]{:S(2)}) collective-permute-start(f32[32,128]{1,0:T(8,128)S(1)} %get-tuple-element.47), channel_id=1, source_target_pairs={{0,24},{8,0},{16,8},{24,16},{1,25},{9,1},{17,9},{25,17},{2,26},{10... | collective-permute-start | bytes 49160 | tf_op jit(solution)/shard_map/ppermute | solution.py:443
  171.5 0.7 shard_map.163
  172.1 2.7 %collective-permute-done.9.refs_3_ = f32[32,128]{1,0:T(8,128)S(1)} collective-permute-done((f32[32,128]{1,0:T(8,128)S(1)}, f32[32,128]{1,0:T(8,128)S(1)}, u32[]{:S(2)}, u32[]{:S(2)}) %collective-permute-start.9) | collective-permute-done | bytes 16416 | tf_op jit(solution)/shard_map/ppermute | solution.py:443
  174.8 0.6 shard_map.158
  176.1 2.3 %shard_map.165 = (bf16[128,256]{1,0:T(8,128)(2,1)}, bf16[128,128]{1,0:T(8,128)(2,1)}, f32[4,128]{1,0:T(4,128)}, bf16[128,256]{1,0:T(8,128)(2,1)}) custom-call(bf16[64,256]{1,0:T(8,128)(2,1)S(1)} %get-tuple-element.62.refs_0_, bf16[64,256]{1,0:T(8,128)(2,1)S(1)} %collective-permute-done.18.refs_1_, bf16[64,256]{1,0:T(8,128)(2,1)S(1)} %collective-permute-done.19.refs_2_, ...), custom_call_target="tpu_custom_call" | custom-call | flops 10000000 | bytes 1000000 | tf_op jit(solution)/shard_map/pallas_call | solution.py:58
  (92 shorter events, 4.8 us)
Async XLA Ops:
  1.4 55.0 %copy-start.25 = (f32[4,1]{1,0:T(4,128)}, f32[4,1]{1,0:T(4,128)S(1)}, u32[]{:S(2)}) copy-start(f32[4,1]{1,0:T(4,128)S(1)} %copy.17.refs_1_.refs_5_) | copy-start | bytes 52
  2.1 0.8 copy-start.2
  2.9 0.8 copy-start.4
  5.1 51.3 %copy-start.5 = (bf16[128,256]{1,0:T(8,128)(2,1)S(1)}, bf16[128,256]{1,0:T(8,128)(2,1)}, u32[]{:S(2)}) copy-start(bf16[128,256]{1,0:T(8,128)(2,1)} %refs_8_.3) | copy-start | bytes 196612
  5.1 51.3 %copy-start.17 = (bf16[128,128]{1,0:T(8,128)(2,1)S(1)}, bf16[128,128]{1,0:T(8,128)(2,1)}, u32[]{:S(2)}) copy-start(bf16[128,128]{1,0:T(8,128)(2,1)} %refs_9_.1) | copy-start | bytes 98308
  5.1 51.3 %copy-start.19 = (bf16[128,256]{1,0:T(8,128)(2,1)S(1)}, bf16[128,256]{1,0:T(8,128)(2,1)}, u32[]{:S(2)}) copy-start(bf16[128,256]{1,0:T(8,128)(2,1)} %refs_10_.5) | copy-start | bytes 196612
  16.8 12.7 %copy-start = (bf16[128,2048]{1,0:T(8,128)(2,1)S(1)}, bf16[128,2048]{1,0:T(8,128)(2,1)}, u32[]{:S(2)}) copy-start(bf16[128,2048]{1,0:T(8,128)(2,1)} %refs_6_.3) | copy-start | bytes 1572868
  16.9 39.6 %copy-start.1 = (bf16[128,2048]{1,0:T(8,128)(2,1)S(1)}, bf16[128,2048]{1,0:T(8,128)(2,1)}, u32[]{:S(2)}) copy-start(bf16[128,2048]{1,0:T(8,128)(2,1)} %refs_0_.1) | copy-start | bytes 1572868
  17.6 38.8 %copy-start.33 = (f32[4,128]{1,0:T(4,128)S(1)}, f32[4,128]{1,0:T(4,128)}, u32[]{:S(2)}) copy-start(f32[4,128]{1,0:T(4,128)} %refs_10_.4) | copy-start | bytes 6148
  17.7 57.4 %all-to-all-start.1 = ((bf16[16,40,256]{2,1,0:T(8,128)(2,1)}), bf16[16,40,256]{2,1,0:T(8,128)(2,1)S(1)}, u32[]{:S(2)}, u32[]{:S(2)}) async-start(bf16[16,40,256]{2,1,0:T(8,128)(2,1)} %shard_map.154), calls=%async_computation.1 | async-start | bytes 655360 | tf_op jit(solution)/shard_map/all_to_all | solution.py:434
  29.6 26.9 %copy-start.3 = (bf16[128,256]{1,0:T(8,128)(2,1)S(1)}, bf16[128,256]{1,0:T(8,128)(2,1)}, u32[]{:S(2)}) copy-start(bf16[128,256]{1,0:T(8,128)(2,1)} %refs_7_.3) | copy-start | bytes 196612
  29.6 45.5 %collective-permute-start.5 = (bf16[128,2048]{1,0:T(8,128)(2,1)S(1)}, bf16[128,2048]{1,0:T(8,128)(2,1)S(1)}, u32[]{:S(2)}, u32[]{:S(2)}) collective-permute-start(bf16[128,2048]{1,0:T(8,128)(2,1)S(1)} %copy-done), channel_id=1, source_target_pairs={{0,16},{8,24},{16,0},{24,8},{1,17},{9,25},{17,1},{25,9},{2,18},{10... | collective-permute-start | bytes 1572872 | tf_op jit(solution)/shard_map/ppermute | solution.py:443
  33.7 41.4 %collective-permute-start.4 = (bf16[128,2048]{1,0:T(8,128)(2,1)S(1)}, bf16[128,2048]{1,0:T(8,128)(2,1)S(1)}, u32[]{:S(2)}, u32[]{:S(2)}) collective-permute-start(bf16[128,2048]{1,0:T(8,128)(2,1)S(1)} %copy-done), channel_id=1, source_target_pairs={{0,8},{8,16},{16,24},{24,0},{1,9},{9,17},{17,25},{25,1},{2,10},{10... | collective-permute-start | bytes 1572872 | tf_op jit(solution)/shard_map/ppermute | solution.py:443
  36.5 38.5 %collective-permute-start.6 = (bf16[128,2048]{1,0:T(8,128)(2,1)S(1)}, bf16[128,2048]{1,0:T(8,128)(2,1)S(1)}, u32[]{:S(2)}, u32[]{:S(2)}) collective-permute-start(bf16[128,2048]{1,0:T(8,128)(2,1)S(1)} %copy-done), channel_id=1, source_target_pairs={{0,24},{8,0},{16,8},{24,16},{1,25},{9,1},{17,9},{25,17},{2,26},{10... | collective-permute-start | bytes 1572872 | tf_op jit(solution)/shard_map/ppermute | solution.py:443
  39.5 16.9 %collective-permute-start = (bf16[8,2048]{1,0:T(8,128)(2,1)S(1)}, bf16[8,2048]{1,0:T(8,128)(2,1)S(1)}, u32[]{:S(2)}, u32[]{:S(2)}) collective-permute-start(bf16[8,2048]{1,0:T(8,128)(2,1)S(1)} %slice.3), channel_id=1, source_target_pairs={{0,8},{8,16},{16,24},{24,32},{32,40},{40,48},{48,56},{56,64},{64,7... | collective-permute-start | bytes 98312 | tf_op jit(solution)/shard_map/ppermute | solution.py:482
  58.7 19.0 %copy-start.6 = (bf16[256,256]{1,0:T(8,128)(2,1)}, bf16[256,256]{1,0:T(8,128)(2,1)S(1)}, u32[]{:S(2)}) copy-start(bf16[256,256]{1,0:T(8,128)(2,1)S(1)} %get-tuple-element.39.refs_2_.refs_3_) | copy-start | bytes 393220
  58.7 7.7 %collective-permute-start.1 = (bf16[256,256]{1,0:T(8,128)(2,1)S(1)}, bf16[256,256]{1,0:T(8,128)(2,1)S(1)}, u32[]{:S(2)}, u32[]{:S(2)}) collective-permute-start(bf16[256,256]{1,0:T(8,128)(2,1)S(1)} %get-tuple-element.40), channel_id=1, source_target_pairs={{0,8},{8,16},{16,24},{24,0},{1,9},{9,17},{17,25},{25,1},{2,10},{10... | collective-permute-start | bytes 393224 | tf_op jit(solution)/shard_map/ppermute | solution.py:443
  60.6 8.4 %collective-permute-start.2 = (bf16[256,256]{1,0:T(8,128)(2,1)S(1)}, bf16[256,256]{1,0:T(8,128)(2,1)S(1)}, u32[]{:S(2)}, u32[]{:S(2)}) collective-permute-start(bf16[256,256]{1,0:T(8,128)(2,1)S(1)} %get-tuple-element.41), channel_id=1, source_target_pairs={{0,16},{8,24},{16,0},{24,8},{1,17},{9,25},{17,1},{25,9},{2,18},{10... | collective-permute-start | bytes 393224 | tf_op jit(solution)/shard_map/ppermute | solution.py:443
  66.3 11.3 %copy-start.8 = (bf16[256,256]{1,0:T(8,128)(2,1)}, bf16[256,256]{1,0:T(8,128)(2,1)S(1)}, u32[]{:S(2)}) copy-start(bf16[256,256]{1,0:T(8,128)(2,1)S(1)} %collective-permute-done.1.refs_3_.refs_4_) | copy-start | bytes 393220
  66.3 8.1 %collective-permute-start.3 = (bf16[256,256]{1,0:T(8,128)(2,1)S(1)}, bf16[256,256]{1,0:T(8,128)(2,1)S(1)}, u32[]{:S(2)}, u32[]{:S(2)}) collective-permute-start(bf16[256,256]{1,0:T(8,128)(2,1)S(1)} %get-tuple-element.42), channel_id=1, source_target_pairs={{0,24},{8,0},{16,8},{24,16},{1,25},{9,1},{17,9},{25,17},{2,26},{10... | collective-permute-start | bytes 393224 | tf_op jit(solution)/shard_map/ppermute | solution.py:443
  68.9 8.7 %copy-start.10 = (bf16[256,256]{1,0:T(8,128)(2,1)}, bf16[256,256]{1,0:T(8,128)(2,1)S(1)}, u32[]{:S(2)}) copy-start(bf16[256,256]{1,0:T(8,128)(2,1)S(1)} %collective-permute-done.2.refs_4_.refs_5_) | copy-start | bytes 393220
  75.1 0.9 copy-start.13
  80.3 11.9 %copy-start.36 = (f32[32,128]{1,0:T(8,128)S(1)}, f32[32,128]{1,0:T(8,128)}, u32[]{:S(2)}) copy-start(f32[32,128]{1,0:T(8,128)} %copy-done.35) | copy-start | bytes 49156
  80.3 28.1 %copy-start.24 = (f32[32,512]{1,0:T(8,128)S(1)}, f32[32,512]{1,0:T(8,128)}, u32[]{:S(2)}) copy-start(f32[32,512]{1,0:T(8,128)} %copy-done.23) | copy-start | bytes 196612
  80.3 43.5 %all-to-all-start.2 = ((bf16[16,32,384]{2,1,0:T(8,128)(2,1)}), bf16[16,32,384]{2,1,0:T(8,128)(2,1)S(1)}, u32[]{:S(2)}, u32[]{:S(2)}) async-start(bf16[16,32,384]{2,1,0:T(8,128)(2,1)} %copy-done.15), calls=%async_computation.2 | async-start | bytes 786432 | tf_op jit(solution)/shard_map/all_to_all | solution.py:434
  92.2 16.2 %collective-permute-start.10 = (f32[32,128]{1,0:T(8,128)S(1)}, f32[32,128]{1,0:T(8,128)S(1)}, u32[]{:S(2)}, u32[]{:S(2)}) collective-permute-start(f32[32,128]{1,0:T(8,128)S(1)} %copy-done.36), channel_id=1, source_target_pairs={{32,0},{64,32},{96,64},{128,96},{160,128},{192,160},{224,192},{256... | collective-permute-start | bytes 49160 | tf_op jit(solution)/shard_map/ppermute | solution.py:514
  108.5 9.6 %collective-permute-start.11 = (bf16[32,128]{1,0:T(8,128)(2,1)S(1)}, bf16[32,128]{1,0:T(8,128)(2,1)S(1)}, u32[]{:S(2)}, u32[]{:S(2)}) collective-permute-start(bf16[32,128]{1,0:T(8,128)(2,1)S(1)} %get-tuple-element.52), channel_id=1, source_target_pairs={{0,8},{8,16},{16,24},{24,0},{1,9},{9,17},{17,25},{25,1},{2,10},{10... | collective-permute-start | bytes 24584 | tf_op jit(solution)/shard_map/ppermute | solution.py:443
  110.4 7.7 %collective-permute-start.12 = (bf16[32,128]{1,0:T(8,128)(2,1)S(1)}, bf16[32,128]{1,0:T(8,128)(2,1)S(1)}, u32[]{:S(2)}, u32[]{:S(2)}) collective-permute-start(bf16[32,128]{1,0:T(8,128)(2,1)S(1)} %get-tuple-element.53), channel_id=1, source_target_pairs={{0,16},{8,24},{16,0},{24,8},{1,17},{9,25},{17,1},{25,9},{2,18},{10... | collective-permute-start | bytes 24584 | tf_op jit(solution)/shard_map/ppermute | solution.py:443
  114.7 6.8 %collective-permute-start.13 = (bf16[32,128]{1,0:T(8,128)(2,1)S(1)}, bf16[32,128]{1,0:T(8,128)(2,1)S(1)}, u32[]{:S(2)}, u32[]{:S(2)}) collective-permute-start(bf16[32,128]{1,0:T(8,128)(2,1)S(1)} %get-tuple-element.54), channel_id=1, source_target_pairs={{0,24},{8,0},{16,8},{24,16},{1,25},{9,1},{17,9},{25,17},{2,26},{10... | collective-permute-start | bytes 24584 | tf_op jit(solution)/shard_map/ppermute | solution.py:443
  121.8 17.9 %collective-permute-start.14 = (bf16[4,256,128]{2,1,0:T(8,128)(2,1)S(1)}, bf16[4,256,128]{2,1,0:T(8,128)(2,1)S(1)}, u32[]{:S(2)}, u32[]{:S(2)}) collective-permute-start(bf16[4,256,128]{2,1,0:T(8,128)(2,1)S(1)} %get-tuple-element.56), channel_id=1, source_target_pairs={{0,1},{1,0},{2,3},{3,2},{4,5},{5,4},{6,7},{7,6},{8,9},{9,8},{10,11... | collective-permute-start | bytes 786440 | tf_op jit(solution)/shard_map/ppermute | solution.py:521
  124.7 29.1 %copy-start.22 = (bf16[4,32,256]{2,1,0:T(8,128)(2,1)S(1)}, bf16[4,32,256]{2,1,0:T(8,128)(2,1)}, u32[]{:S(2)}) copy-start(bf16[4,32,256]{2,1,0:T(8,128)(2,1)} %copy-done.21) | copy-start | bytes 196612
  124.7 53.7 %all-to-all-start.3 = ((f32[64,1,128]{2,1,0:T(1,128)}), f32[64,1,128]{2,1,0:T(1,128)S(1)}, u32[]{:S(2)}, u32[]{:S(2)}) async-start(f32[64,1,128]{2,1,0:T(1,128)} %get-tuple-element.48), calls=%async_computation.3 | async-start | bytes 65536 | tf_op jit(solution)/shard_map/all_to_all | solution.py:434
  139.7 14.0 %copy-start.7 = (bf16[256,256]{1,0:T(8,128)(2,1)S(1)}, bf16[256,256]{1,0:T(8,128)(2,1)}, u32[]{:S(2)}) copy-start(bf16[256,256]{1,0:T(8,128)(2,1)} %copy-done.6) | copy-start | bytes 393220
  139.8 14.0 %copy-start.9 = (bf16[256,256]{1,0:T(8,128)(2,1)S(1)}, bf16[256,256]{1,0:T(8,128)(2,1)}, u32[]{:S(2)}) copy-start(bf16[256,256]{1,0:T(8,128)(2,1)} %copy-done.8) | copy-start | bytes 393220
  139.8 14.0 %copy-start.11 = (bf16[256,256]{1,0:T(8,128)(2,1)S(1)}, bf16[256,256]{1,0:T(8,128)(2,1)}, u32[]{:S(2)}) copy-start(bf16[256,256]{1,0:T(8,128)(2,1)} %copy-done.10) | copy-start | bytes 393220
  139.8 14.0 %copy-start.14 = (bf16[256,256]{1,0:T(8,128)(2,1)S(1)}, bf16[256,256]{1,0:T(8,128)(2,1)}, u32[]{:S(2)}) copy-start(bf16[256,256]{1,0:T(8,128)(2,1)} %copy-done.12) | copy-start | bytes 393220
  139.9 17.7 %collective-permute-start.15 = (bf16[256,128]{1,0:T(8,128)(2,1)S(1)}, bf16[256,128]{1,0:T(8,128)(2,1)S(1)}, u32[]{:S(2)}, u32[]{:S(2)}) collective-permute-start(bf16[256,128]{1,0:T(8,128)(2,1)S(1)} %get-tuple-element.58), channel_id=1, source_target_pairs={{0,2},{1,3},{2,4},{3,5},{4,6},{5,7},{6,0},{7,1},{8,10},{9,11},{10,... | collective-permute-start | bytes 196616 | tf_op jit(solution)/shard_map/ppermute | solution.py:443
  143.4 18.2 %collective-permute-start.16 = (bf16[256,128]{1,0:T(8,128)(2,1)S(1)}, bf16[256,128]{1,0:T(8,128)(2,1)S(1)}, u32[]{:S(2)}, u32[]{:S(2)}) collective-permute-start(bf16[256,128]{1,0:T(8,128)(2,1)S(1)} %get-tuple-element.59), channel_id=1, source_target_pairs={{0,4},{1,5},{2,6},{3,7},{4,0},{5,1},{6,2},{7,3},{8,12},{9,13},{10,... | collective-permute-start | bytes 196616 | tf_op jit(solution)/shard_map/ppermute | solution.py:443
  148.0 15.7 %collective-permute-start.17 = (bf16[256,128]{1,0:T(8,128)(2,1)S(1)}, bf16[256,128]{1,0:T(8,128)(2,1)S(1)}, u32[]{:S(2)}, u32[]{:S(2)}) collective-permute-start(bf16[256,128]{1,0:T(8,128)(2,1)S(1)} %get-tuple-element.60), channel_id=1, source_target_pairs={{0,6},{1,7},{2,0},{3,1},{4,2},{5,3},{6,4},{7,5},{8,14},{9,15},{10,... | collective-permute-start | bytes 196616 | tf_op jit(solution)/shard_map/ppermute | solution.py:443
  151.4 16.6 %collective-permute-start.7 = (f32[32,128]{1,0:T(8,128)S(1)}, f32[32,128]{1,0:T(8,128)S(1)}, u32[]{:S(2)}, u32[]{:S(2)}) collective-permute-start(f32[32,128]{1,0:T(8,128)S(1)} %get-tuple-element.45), channel_id=1, source_target_pairs={{0,8},{8,16},{16,24},{24,0},{1,9},{9,17},{17,25},{25,1},{2,10},{10... | collective-permute-start | bytes 49160 | tf_op jit(solution)/shard_map/ppermute | solution.py:443
  154.1 21.3 %collective-permute-start.18 = (bf16[64,256]{1,0:T(8,128)(2,1)S(1)}, bf16[64,256]{1,0:T(8,128)(2,1)S(1)}, u32[]{:S(2)}, u32[]{:S(2)}) collective-permute-start(bf16[64,256]{1,0:T(8,128)(2,1)S(1)} %get-tuple-element.63), channel_id=1, source_target_pairs={{0,8},{8,16},{16,24},{24,0},{1,9},{9,17},{17,25},{25,1},{2,10},{10... | collective-permute-start | bytes 98312 | tf_op jit(solution)/shard_map/ppermute | solution.py:443
  157.6 17.8 %collective-permute-start.19 = (bf16[64,256]{1,0:T(8,128)(2,1)S(1)}, bf16[64,256]{1,0:T(8,128)(2,1)S(1)}, u32[]{:S(2)}, u32[]{:S(2)}) collective-permute-start(bf16[64,256]{1,0:T(8,128)(2,1)S(1)} %get-tuple-element.64), channel_id=1, source_target_pairs={{0,16},{8,24},{16,0},{24,8},{1,17},{9,25},{17,1},{25,9},{2,18},{10... | collective-permute-start | bytes 98312 | tf_op jit(solution)/shard_map/ppermute | solution.py:443
  161.6 13.9 %collective-permute-start.20 = (bf16[64,256]{1,0:T(8,128)(2,1)S(1)}, bf16[64,256]{1,0:T(8,128)(2,1)S(1)}, u32[]{:S(2)}, u32[]{:S(2)}) collective-permute-start(bf16[64,256]{1,0:T(8,128)(2,1)S(1)} %get-tuple-element.65), channel_id=1, source_target_pairs={{0,24},{8,0},{16,8},{24,16},{1,25},{9,1},{17,9},{25,17},{2,26},{10... | collective-permute-start | bytes 98312 | tf_op jit(solution)/shard_map/ppermute | solution.py:443
  163.8 8.4 %collective-permute-start.8 = (f32[32,128]{1,0:T(8,128)S(1)}, f32[32,128]{1,0:T(8,128)S(1)}, u32[]{:S(2)}, u32[]{:S(2)}) collective-permute-start(f32[32,128]{1,0:T(8,128)S(1)} %get-tuple-element.46), channel_id=1, source_target_pairs={{0,16},{8,24},{16,0},{24,8},{1,17},{9,25},{17,1},{25,9},{2,18},{10... | collective-permute-start | bytes 49160 | tf_op jit(solution)/shard_map/ppermute | solution.py:443
  168.0 6.8 %collective-permute-start.9 = (f32[32,128]{1,0:T(8,128)S(1)}, f32[32,128]{1,0:T(8,128)S(1)}, u32[]{:S(2)}, u32[]{:S(2)}) collective-permute-start(f32[32,128]{1,0:T(8,128)S(1)} %get-tuple-element.47), channel_id=1, source_target_pairs={{0,24},{8,0},{16,8},{24,16},{1,25},{9,1},{17,9},{25,17},{2,26},{10... | collective-permute-start | bytes 49160 | tf_op jit(solution)/shard_map/ppermute | solution.py:443
  171.4 4.0 %copy-start.20 = (bf16[128,256]{1,0:T(8,128)(2,1)S(1)}, bf16[128,256]{1,0:T(8,128)(2,1)}, u32[]{:S(2)}) copy-start(bf16[128,256]{1,0:T(8,128)(2,1)} %refs_10_.5) | copy-start | bytes 196612
  174.8 0.8 copy-start.30
  174.8 0.8 copy-start.32
  (14 other events, 9.6 us)

commit v3 on v2

--- a/solution.py
+++ b/solution.py
@@ -19,9 +19,9 @@
 F32 = jnp.float32
 BF16 = jnp.bfloat16
 PALLAS = True
-CORES = 2
 ZY = ("z", "y")
 VMEM_LIMIT = 16 * 2**20
+BIG = 60 * 1024 * 2**10
 
 
 def dot(a, b, ca=1, cb=0, precision=None):
@@ -37,7 +37,7 @@
     return jnp.roll(a, shift, axis=1)
 
 
-def local(fn, outs, *args, flops=10**7, raw=()):
+def local(fn, outs, *args, flops=10**7, raw=(), vmem=VMEM_LIMIT):
     single = not isinstance(outs, (list, tuple))
     shapes = [outs] if single else list(outs)
     if not PALLAS:
@@ -61,7 +61,7 @@
         in_specs=[vm] * len(args),
         out_specs=[vm] * len(shapes),
         cost_estimate=pl.CostEstimate(flops=flops, bytes_accessed=10**6, transcendentals=0),
-        compiler_params=pltpu.CompilerParams(vmem_limit_bytes=VMEM_LIMIT),
+        compiler_params=pltpu.CompilerParams(vmem_limit_bytes=vmem),
     )(*args)
     return res[0] if single else res
 
@@ -85,6 +85,11 @@
 def from_peers(parts):
     yi = lax.axis_index("y")
     return [choose(parts, lax.rem(yi + Y - j, Y)) for j in range(Y)]
+
+
+def by_mask(parts):
+    yi = lax.axis_index("y")
+    return [choose(parts, jnp.bitwise_xor(yi, j)) for j in range(Y)]
 
 
 def columns_at(ref, start, size):
@@ -126,7 +131,8 @@
 
 def decays(tpre, aexp, jump):
     step = jnp.log(1.0 + jnp.exp(tpre))
-    rate = jnp.exp(aexp)
+    same = iota2((R, R), 0) == iota2((R, R), 1)
+    rate = jnp.sum(jnp.where(same, jnp.exp(aexp), 0.0), axis=1, keepdims=True)
     la = jump - rate * step
     tri = (iota2((TOK, TOK), 0) >= iota2((TOK, TOK), 1)).astype(F32)
     cum = dot(tri, la, 1, 1, HIGH)
@@ -142,14 +148,17 @@
     return 1.0 / (1.0 + jnp.exp(-v))
 
 
-def bwd_local(tpre, aexp, jump, gate, adj, q):
-    cum = decays(tpre, aexp, jump)[3]
+def bwd_local(tpre, aexp, jump, gate, adj, q, v):
+    step, _, _, cum = decays(tpre, aexp, jump)
     g = gate.astype(F32)
     dy = adj.astype(F32) * g * sigmoid(g)
     dye = (dy * expand(jnp.exp(cum))).astype(BF16)
     lg = dot(q, dye, 0, 0).astype(BF16)
+    ud = v.astype(F32) * expand(column(step) * jnp.exp(cum[TOK - 1 :] - cum))
     hi, mid, low = split3(expand(cum[TOK - 1 :]))
-    tail = jnp.concatenate([hi, mid, low, jnp.zeros((PAD - 3, HP), BF16)], axis=0)
+    tail = jnp.concatenate(
+        [hi, mid, low, jnp.zeros((PAD - 3, HP), BF16), ud.astype(BF16)], axis=0
+    )
     return jnp.stack([jnp.concatenate([lg[NS * i : NS * (i + 1)], tail], axis=0) for i in range(Y)])
 
 
@@ -188,12 +197,35 @@
     slope = sig * (1.0 + conv * (1.0 - sig))
     ls = dot(keys, ud).astype(BF16)
     pair = jnp.concatenate([dki.astype(BF16), slope.astype(BF16)], axis=1)
-    chunks = [rim[:, HP * i : HP * (i + 1)] for i in range(rim.shape[1] // HP)]
-    shared = jnp.concatenate([ud] + chunks, axis=0)
-    mids = [
-        jnp.concatenate([shared, ls[NS * i : NS * (i + 1)], pair[NS * i : NS * (i + 1)]], axis=0)
-        for i in range(Y)
-    ]
+    eye = (iota2((TOK, TOK), 0) == iota2((TOK, TOK), 1)).astype(BF16)
+    xt = dot(x, eye, 0, 0).astype(BF16)
+    small_eye = (iota2((PAD, PAD), 0) == iota2((PAD, PAD), 1)).astype(BF16)
+    rt = dot(rim, small_eye, 0, 0).astype(BF16)
+    width = Y * NS
+    blocks = x.shape[1] // width
+
+    def features_of(a, i):
+        return jnp.concatenate(
+            [a[width * b + NS * i : width * b + NS * (i + 1)] for b in range(blocks)], axis=0
+        )
+
+    mids = []
+    for i in range(Y):
+        xs = features_of(xt, i)
+        rs = dot(small_eye, features_of(rt, i), 1, 1).astype(BF16)
+        half = xs.shape[0] // 2
+        mids.append(
+            jnp.concatenate(
+                [
+                    pair,
+                    ls[NS * i : NS * (i + 1)],
+                    jnp.concatenate([xs[:half], xs[half:]], axis=1),
+                    rs[:, :half],
+                    rs[:, half:],
+                ],
+                axis=0,
+            )
+        )
     return *to_peers(mids), keys
 
 
@@ -211,7 +243,7 @@
 
 def fwd_group(got, mid):
     tau = joined(got, NS)
-    at = slice(TOK + 8 * PAD, TOK + 8 * PAD + NS)
+    at = slice(TOK, TOK + NS)
     acc = mid[0][at].astype(F32)
     for j in range(1, Y):
         acc = mid[j][at].astype(F32) + jnp.exp(tau[j : j + 1]) * acc
@@ -233,13 +265,9 @@
     return acc
 
 
-def bwd_apply(far, got, m0, m1, m2, m3, x0, x1, x2, x3, taps):
-    mid = from_peers([m0, m1, m2, m3])
-    yi = lax.axis_index("y")
+def bwd_far(far, got):
+    count = far.shape[0]
     zrow = lax.axis_index("z")
-    mine = iota2((NS, STATE), 1) == iota2((NS, STATE), 0) + NS * lax.axis_index("y")
-    taps_own = dot(mine.astype(F32), taps, 1, 1, HIGH)
-    count = far.shape[0]
     tau, upto = chain_sums(far)
     row = iota2((count, HP), 0)
     mine = jnp.sum(jnp.where(row == zrow, upto, 0.0), axis=0, keepdims=True)
@@ -251,43 +279,55 @@
         ends[j] = state.astype(BF16)
         if j:
             state = got[j, :NS].astype(F32) + jnp.exp(tau_j[j : j + 1]) * state
-    own = TOK + 8 * PAD + NS
-    cg = []
-    for j in range(Y):
-        dk = dot(ends[j], mid[j][:TOK], 1, 1) + mid[j][own : own + NS, :TOK].astype(F32)
-        cg.append(dk * mid[j][own : own + NS, TOK:].astype(F32))
-    cg = jnp.concatenate(cg, axis=1)
+    dk = [dot(ends[j], got[j, NS + PAD :], 1, 1).astype(BF16) for j in range(Y)]
+    halves = [jnp.concatenate(dk[i : i + 2], axis=1) for i in range(0, Y, 2)]
+    return jnp.stack([jnp.concatenate([*halves, ends[j]], axis=0) for j in range(Y)])
+
+
+def key_grads(near, got, m0, m1, m2, m3, taps):
+    mid = from_peers([m0, m1, m2, m3])
+    yi = lax.axis_index("y")
+    taps_t = column(taps)
+    dk = jnp.concatenate(
+        [
+            jnp.concatenate([near[i, :NS], near[i, NS : 2 * NS]], axis=1).astype(F32)
+            for i in range(Y)
+        ],
+        axis=0,
+    )
+    dki = jnp.concatenate([part[:STATE, :TOK] for part in mid], axis=1).astype(F32)
+    slope = jnp.concatenate([part[:STATE, TOK:] for part in mid], axis=1).astype(F32)
+    cg = (dk + dki) * slope
     size = Y * TOK
-    lane = iota2((NS, size), 1)
-    main = taps_own[:, 3:4] * cg
+    lane = iota2((STATE, size), 1)
+    main = taps_t[:, 3:4] * cg
     over = jnp.zeros_like(main)
     for d in range(1, 4):
-        moved = taps_own[:, 3 - d : 4 - d] * roll(cg, -d)
+        moved = taps_t[:, 3 - d : 4 - d] * roll(cg, -d)
         main = main + jnp.where(lane < size - d, moved, 0.0)
         over = over + jnp.where(lane >= size - d, moved, 0.0)
-    rims = jnp.concatenate(
-        [mid[0][TOK + PAD * i : TOK + PAD * (i + 1)] for i in range(8)], axis=1
-    )
     over = over[:, size - TOK :]
-    zero = jnp.zeros((TOK - PAD, rims.shape[1]), BF16)
-    dw = dot(over.astype(BF16), jnp.concatenate([zero, rims], axis=0))
     pg = main.astype(BF16)
-    pg = [pg[:, TOK * i : TOK * (i + 1)] for i in range(Y)]
-    for d, part in enumerate((x0, x1, x2, x3)):
-        dw = dw + dot(choose(pg, lax.rem(yi + Y - d, Y)), part)
-    width = dw.shape[1] // count
+    first = TOK + NS
+    last = mid[0].shape[0] - 2 * PAD
+    rims = jnp.concatenate([mid[0][last : last + PAD], mid[0][last + PAD :]], axis=1)
+    dw = dot(rims, over[:, TOK - PAD :].astype(BF16), 0, 1)
+    for j in range(Y):
+        xs = jnp.concatenate([mid[j][first:last, :TOK], mid[j][first:last, TOK:]], axis=0)
+        dw = dw + dot(xs, pg[:, TOK * j : TOK * (j + 1)], 1, 1)
     dw = dw.astype(BF16)
     fwd = fwd_group(got, mid)
     send = jnp.stack(
         [
-            jnp.concatenate([dw[:, width * i : width * (i + 1)], fwd], axis=1)
-            for i in range(count)
+            jnp.concatenate([dw[NS * i : NS * (i + 1)], fwd], axis=1)
+            for i in range(dw.shape[0] // NS)
         ]
     )
-    return send, jnp.stack(ends), main, over
-
-
-def fwd_apply(near, bfar, got, m0, m1, m2, m3, ends):
+    own = choose([main[:, TOK * j : TOK * (j + 1)] for j in range(Y)], yi)
+    return send, own, over
+
+
+def fwd_apply(near, bfar, got, m0, m1, m2, m3):
     mid = from_peers([m0, m1, m2, m3])
     far = near[:, :, near.shape[2] - HP :]
     zrow = lax.axis_index("z")
@@ -298,21 +338,21 @@
     weights = jnp.exp(jnp.where(row < zrow, before - upto, -1e30))
     state = weighted(weights, far)
     tau_j = joined(got, NS)
-    at = slice(TOK + 8 * PAD, TOK + 8 * PAD + NS)
+    at = slice(TOK, TOK + NS)
     res = []
     for j in range(Y):
-        res.append(jnp.concatenate([state.astype(BF16), ends[j]], axis=0))
+        res.append(state.astype(BF16))
         if j < Y - 1:
             state = mid[j][at].astype(F32) + jnp.exp(tau_j[j : j + 1]) * state
-    return to_peers(res)
-
-
-def finish(p0, p1, p2, p3, tpre, aexp, jump, gate, adj, q, v, keys):
+    mine, one, two, three = by_mask(res)
+    return mine, jnp.concatenate([one, two], axis=0), three
+
+
+def finish(mine, first, second, near, tpre, aexp, jump, gate, adj, q, v, keys):
     step, rate, la, cum = decays(tpre, aexp, jump)
     cum_t = row_form(la)
-    states = from_peers([p0, p1, p2, p3])
-    s_in = jnp.concatenate([part[:NS] for part in states], axis=0)
-    g_out = jnp.concatenate([part[NS:] for part in states], axis=0)
+    s_in = jnp.concatenate(by_mask([mine, first[:NS], second[NS:], second[:NS]]), axis=0)
+    g_out = jnp.concatenate([near[i, 2 * NS :] for i in range(Y)], axis=0)
     g = gate.astype(F32)
     a = adj.astype(F32)
     sig = sigmoid(g)
@@ -367,63 +407,39 @@
 
 
 def weight_sum(near):
-    acc = summed(near[:, :, : near.shape[2] - HP])
+    acc = summed(near[:, :, :STATE])
     count = lax.axis_size("z") * Y
-    place = iota2((NS, STATE), 1) == iota2((NS, STATE), 0) + NS * lax.axis_index("y")
-    placed = dot(acc, place.astype(F32), 0, 0, HIGH)
-    width = placed.shape[0] // Y
-    pieces = to_peers([placed[width * i : width * (i + 1)] for i in range(Y)])
-    squares = jnp.sum(placed * placed, axis=0, keepdims=True)
-    return *pieces, jnp.broadcast_to(squares[None], (count, 1, STATE))
-
-
-def own_tokens(main, after):
-    last = Y * TOK - TOK
-    whole = jnp.concatenate([main[:, :last], main[:, last:] + after], axis=1).astype(BF16)
-    return to_peers([whole[:, TOK * i : TOK * (i + 1)] for i in range(Y)])
-
-
-def partial_input(w, p0, p1, p2, p3):
-    grad = jnp.concatenate(from_peers([p0, p1, p2, p3]), axis=0)
-    count = lax.axis_size("tp")
-    chips = count // CORES
-    width = w.shape[1] // count
+    squares = jnp.sum(acc * acc, axis=0, keepdims=True)
+    return acc, jnp.broadcast_to(squares[None], (count, 1, STATE))
+
+
+def partial_input(w, own, after):
+    edge = lax.axis_index("y") == Y - 1
+    grad = (own + jnp.where(edge, after, 0.0)).astype(BF16)
     place = lax.axis_index("tp")
-    core = lax.rem(place, CORES)
-    chip = lax.div(place, CORES)
+    width = w.shape[1] // lax.axis_size("tp")
+    core = lax.rem(place, 2)
+    chip = lax.div(place, 2)
+    near = jnp.bitwise_xor(chip, 1)
+    chips = (chip, 3 - chip, near, 3 - near)
     res = []
-    for side in range(CORES):
-        owner = lax.rem(core + side, CORES)
+    for owner in (core, 1 - core):
         blocks = []
-        for d in range(chips):
-            rank = lax.rem(chip + d, chips) * CORES + owner
+        for other in chips:
+            rank = other * 2 + owner
             blocks.append(dot(columns_at(w, rank * width, width), grad, 0, 0).astype(BF16))
         res.append(jnp.stack(blocks))
     return res
 
 
-def core_sum(mine, other):
-    return [
-        (mine[i].astype(F32) + other[i].astype(F32)).astype(BF16) for i in range(mine.shape[0])
-    ]
-
-
-def piece_sum(*parts):
-    return summed(jnp.stack(parts))
-
-
-def input_sum(*parts):
-    acc = parts[0].astype(F32)
-    for part in parts[1:]:
-        acc = acc + part.astype(F32)
-    return acc.astype(BF16)
-
-
-def piece_sum(*parts):
-    acc = parts[0]
-    for part in parts[1:]:
-        acc = acc + part
-    return acc
+def half_sum(mine, other):
+    size = mine.shape[0] // 2
+    total = (mine.astype(F32) + other.astype(F32)).astype(BF16)
+    return total[:size], total[size:]
+
+
+def last_sum(mine, other):
+    return (mine[0].astype(F32) + other[0].astype(F32)).astype(BF16)
 
 
 def square_sum(parts):
@@ -463,7 +479,7 @@
         payload_vectors,
         probe_vectors,
         interval_preimage.T,
-        channel_damping_exponent.reshape(R, 1),
+        channel_damping_exponent.reshape(1, R),
         added_damping_jumps.T,
         sigmoid_argument,
         adjoint_of_result,
@@ -475,13 +491,11 @@
     sp = zs * Y
     tp = lax.axis_size("tp")
     features = x.shape[1]
-    width = features // zs
     small = (tpre, aexp, jump, gate, adj)
-    bwd_send = local(bwd_local, sds((Y, NS + PAD, HP), BF16), *small, q)
+    bwd_send = local(bwd_local, sds((Y, NS + PAD + TOK, HP), BF16), *small, q, v, vmem=BIG)
     got = exchange(bwd_send, "y")
     rim = lax.ppermute(x[TOK - PAD :], ZY, [(i, i + 1) for i in range(sp - 1)])
-    xs = around([x] * Y, "y", 1)
-    rows = TOK + 8 * PAD + 2 * NS
+    rows = TOK + NS + features // Y // 2 + 2 * PAD
     *mids, keys = local(
         fwd_local,
         [sds((rows, HP), BF16)] * Y + [sds((STATE, TOK), BF16)],
@@ -496,55 +510,56 @@
     mids = around(mids, "y", 1)
     bwd_totals = local(bwd_group, sds((zs, NS + PAD, HP), BF16), got)
     far = exchange(bwd_totals, "z")
-    near_send, ends, main, over = local(
-        bwd_apply,
-        [
-            sds((zs, NS, width + HP), BF16),
-            sds((Y, NS, HP), BF16),
-            sds((NS, Y * TOK), F32),
-            sds((NS, TOK), F32),
-        ],
+    ends = local(bwd_far, sds((Y, 3 * NS, HP), BF16), far, got)
+    ends = exchange(ends, "y")
+    send, own, over = local(
+        key_grads,
+        [sds((zs, NS, STATE + HP), BF16), sds((STATE, TOK), F32), sds((STATE, TOK), F32)],
+        ends,
+        got,
+        *mids,
+        taps,
+    )
+    near = exchange(send, "z")
+    after = lax.ppermute(over, "z", [(i, i - 1) for i in range(1, zs)])
+    weight_t, squares = local(
+        weight_sum, [sds((NS, STATE), F32), sds((sp, 1, STATE), F32)], near
+    )
+    squares = exchange(squares, ZY)
+    mine, first, second = local(
+        fwd_apply,
+        [sds((NS, HP), BF16), sds((2 * NS, HP), BF16), sds((NS, HP), BF16)],
+        near,
         far,
         got,
         *mids,
-        *xs,
-        taps,
-    )
-    near = exchange(near_send, "z")
-    after = lax.ppermute(over, "z", [(i, i - 1) for i in range(1, zs)])
-    tokens = local(own_tokens, [sds((NS, TOK), BF16)] * Y, main, after)
-    tokens = around(tokens, "y", 1)
-    chips = tp // CORES
+    )
+    first = lax.ppermute(first, "y", [(i, i ^ 1) for i in range(Y)])
+    second = jnp.concatenate([second, first[NS:]], axis=0)
+    second = lax.ppermute(second, "y", [(i, i ^ 3) for i in range(Y)])
     share = (features // tp, TOK)
-    sides = local(partial_input, [sds((chips, *share), BF16)] * CORES, w, *tokens, raw=(0,))
-    swap = [(i, i ^ 1) for i in range(tp)]
-    other = lax.ppermute(sides[-1], "tp", swap) if CORES > 1 else None
-    *pieces, squares = local(
-        weight_sum, [sds((width // Y, STATE), F32)] * Y + [sds((sp, 1, STATE), F32)], near
-    )
-    squares = exchange(squares, ZY)
-    states = local(fwd_apply, [sds((2 * NS, HP), BF16)] * Y, near, far, got, *mids, ends)
-    states = around(states, "y", 1)
-    if CORES > 1:
-        shares = local(core_sum, [sds(share, BF16)] * chips, sides[0], other)
-    else:
-        shares = [sides[0][i] for i in range(chips)]
-    shares = around(shares, "tp", CORES)
-    pieces = around(pieces, "y", 1)
+    keep, give = local(partial_input, [sds((4, *share), BF16)] * 2, w, own, after, raw=(0,))
+    give = lax.ppermute(give, "tp", [(i, i ^ 1) for i in range(tp)])
+    keep, give = local(half_sum, [sds((2, *share), BF16)] * 2, keep, give)
+    give = lax.ppermute(give, "tp", [(i, i ^ 2) for i in range(tp)])
+    keep, give = local(half_sum, [sds((1, *share), BF16)] * 2, keep, give)
+    give = lax.ppermute(give, "tp", [(i, i ^ 6) for i in range(tp)])
+    input_grad = local(last_sum, sds(share, BF16), keep, give)
     value_grad, query_grad, decay_grad, gate_grad = local(
         finish,
         [sds((TOK, HP), BF16), sds((TOK, STATE), BF16), sds((R, TOK), F32), sds((TOK, HP), BF16)],
-        *states,
+        mine,
+        first,
+        second,
+        ends,
         *small,
         q,
         v,
         keys,
     )
-    input_grad = local(input_sum, sds(share, BF16), *shares)
-    key_weight_grad = local(piece_sum, sds((width // Y, STATE), F32), *pieces).T
     row_squares = local(square_sum, sds((1, STATE), F32), squares).reshape(STATE)
     return (
-        key_weight_grad,
+        weight_t.T,
         row_squares,
         input_grad,
         value_grad,

time: 180 us -> 146 us (0.81)
  the two profiles are of different devices: /device:TPU:24 before, /device:TPU:8 now
where the time goes in v3:
time: 146 us; the launch traced here: 145 us
  starting transfers between devices  82.8 us (57%)
  waiting for transfers between devices  33.6 us (23%)
  blocking collectives  14.9 us (10%)
  Pallas kernels  13 us (9%)
    all_to_all x4, starting transfers between devices, exchange(): return lax.all_to_all(parts, axis, split_axis=0, concat_axis=0, tiled=True)  47.1 us
    ppermute x1, waiting for transfers between devices, step(): after = lax.ppermute(over, 'z', [(i, i - 1) for i in range(1, zs)])  15.9 us
    ppermute x3, starting transfers between devices, around(): got.append(lax.ppermute(parts[d], axis, route))  15.5 us
    all_to_all x1, blocking collectives, exchange(): return lax.all_to_all(parts, axis, split_axis=0, concat_axis=0, tiled=True)  14.9 us
    pallas_call x13, Pallas kernels, local(): pl.pallas_call(kernel, out_shape=shapes, in_specs=[vm] * len(args), out_s...  13 us
    all_to_all x4, waiting for transfers between devices, exchange(): return lax.all_to_all(parts, axis, split_axis=0, concat_axis=0, tiled=True)  10.4 us
    ppermute x1, starting transfers between devices, step(): give = lax.ppermute(give, 'tp', [(i, i ^ 6) for i in range(tp)])  4.65 us
    ppermute x1, waiting for transfers between devices, step(): rim = lax.ppermute(x[TOK - PAD:], ZY, [(i, i + 1) for i in range(sp - 1)])  3.55 us
  transfers between devices with their start and end apart: 14, of which 7 were waited for; matrix products, arithmetic and copies ran while one was open for 0% of the time, Pallas kernels for 5%

profile of v3, /device:TPU:8, one launch (start us, length us, event | category | flops | bytes accessed | tf_op | source)
XLA Modules:
  0.0 145.3 jit_solution(14689343914838486453)
XLA Ops:
  0.6 2.6 %shard_map.153 = bf16[4,168,256]{2,1,0:T(8,128)(2,1)} custom-call(f32[4,128]{1,0:T(4,128)} %bitcast.6, f32[1,4]{1,0:T(1,128)} %bitcast.12, f32[4,128]{1,0:T(4,128)} %bitcast.9, bf16[128,256]{1,0:T(8,128)(2,1)} %refs_7_.3, bf16[128,256]{1,0:T(8,128)(2,1)} %refs_8_.3, bf16[128,128]{1,0:T(8,128)(2,1)} %refs_9_.1, bf16[128,256]{1,0:T(8,128)(2,1)} %refs_10_.3), custom_call_target="tpu_custom_call" | custom-call | flops 10000000 | bytes 1000000 | tf_op jit(solution)/shard_map/pallas_call | solution.py:58
  3.2 14.9 %all_to_all.25.refs_0_.refs_1_.refs_2_ = bf16[4,168,256]{2,1,0:T(8,128)(2,1)S(1)} all-to-all(bf16[4,168,256]{2,1,0:T(8,128)(2,1)} %shard_map.153), channel_id=1, replica_groups=mesh['z'=16,'y'=4,'tp'=8] {'y'}, dimensions={0} | all-to-all | bytes 688128 | tf_op jit(solution)/shard_map/all_to_all | solution.py:450
  18.1 0.0 copy-start.8
  18.1 0.0 copy-start.9
  18.1 0.8 shard_map.154
  18.9 11.4 %all-to-all-start.1 = ((bf16[16,40,256]{2,1,0:T(8,128)(2,1)}), bf16[16,40,256]{2,1,0:T(8,128)(2,1)S(1)}, u32[]{:S(2)}, u32[]{:S(2)}) async-start(bf16[16,40,256]{2,1,0:T(8,128)(2,1)} %shard_map.154), calls=%async_computation.1 | async-start | bytes 655360 | tf_op jit(solution)/shard_map/all_to_all | solution.py:450
  30.4 0.0 copy-done.1
  30.4 0.0 copy-start.2
  30.4 2.3 %collective-permute-start = (bf16[8,2048]{1,0:T(8,128)(2,1)S(1)}, bf16[8,2048]{1,0:T(8,128)(2,1)S(1)}, u32[]{:S(2)}, u32[]{:S(2)}) collective-permute-start(bf16[8,2048]{1,0:T(8,128)(2,1)S(1)} %slice.6), channel_id=1, source_target_pairs={{0,8},{8,16},{16,24},{24,32},{32,40},{40,48},{48,56},{56,64},{64,7... | collective-permute-start | bytes 98312 | tf_op jit(solution)/shard_map/ppermute | solution.py:497
  32.7 3.5 %collective-permute-done.refs_9_ = bf16[8,2048]{1,0:T(8,128)(2,1)S(1)} collective-permute-done((bf16[8,2048]{1,0:T(8,128)(2,1)S(1)}, bf16[8,2048]{1,0:T(8,128)(2,1)S(1)}, u32[]{:S(2)}, u32[]{:S(2)}) %collective-permute-start) | collective-permute-done | bytes 32800 | tf_op jit(solution)/shard_map/ppermute | solution.py:497
  36.2 0.0 copy-done.5
  36.2 0.0 copy-done.6
  36.2 0.0 copy-done.7
  36.3 2.1 %shard_map.156 = (bf16[432,256]{1,0:T(8,128)(2,1)S(1)}, bf16[432,256]{1,0:T(8,128)(2,1)S(1)}, bf16[432,256]{1,0:T(8,128)(2,1)S(1)}, bf16[432,256]{1,0:T(8,128)(2,1)S(1)}, bf16[128,128]{1,0:T(8,128)(2,1)S(1)}) custom-call(f32[4,128]{1,0:T(4,128)S(1)} %bitcast.7, f32[1,4]{1,0:T(1,128)S(1)} %bitcast.13, f32[4,128]{1,0:T(4,128)S(1)} %bitcast.10, ...), custom_call_target="tpu_custom_call" | custom-call | flops 10000000 | bytes 1000000 | tf_op jit(solution)/shard_map/pallas_call | solution.py:58
  38.4 2.3 %collective-permute-start.1 = (bf16[432,256]{1,0:T(8,128)(2,1)S(1)}, bf16[432,256]{1,0:T(8,128)(2,1)S(1)}, u32[]{:S(2)}, u32[]{:S(2)}) collective-permute-start(bf16[432,256]{1,0:T(8,128)(2,1)S(1)} %get-tuple-element.31), channel_id=1, source_target_pairs={{0,8},{8,16},{16,24},{24,0},{1,9},{9,17},{17,25},{25,1},{2,10},{10... | collective-permute-start | bytes 663560 | tf_op jit(solution)/shard_map/ppermute | solution.py:459
  40.6 8.7 %collective-permute-start.2 = (bf16[432,256]{1,0:T(8,128)(2,1)S(1)}, bf16[432,256]{1,0:T(8,128)(2,1)S(1)}, u32[]{:S(2)}, u32[]{:S(2)}) collective-permute-start(bf16[432,256]{1,0:T(8,128)(2,1)S(1)} %get-tuple-element.32), channel_id=1, source_target_pairs={{0,16},{8,24},{16,0},{24,8},{1,17},{9,25},{17,1},{25,9},{2,18},{10... | collective-permute-start | bytes 663560 | tf_op jit(solution)/shard_map/ppermute | solution.py:459
  49.3 4.5 %collective-permute-start.3 = (bf16[432,256]{1,0:T(8,128)(2,1)S(1)}, bf16[432,256]{1,0:T(8,128)(2,1)S(1)}, u32[]{:S(2)}, u32[]{:S(2)}) collective-permute-start(bf16[432,256]{1,0:T(8,128)(2,1)S(1)} %get-tuple-element.33), channel_id=1, source_target_pairs={{0,24},{8,0},{16,8},{24,16},{1,25},{9,1},{17,9},{25,17},{2,26},{10... | collective-permute-start | bytes 663560 | tf_op jit(solution)/shard_map/ppermute | solution.py:459
  53.9 0.0 all-to-all-done.1.refs_0_.refs_1_
  53.9 1.1 shard_map.155
  54.9 3.4 %all-to-all-start.2 = ((bf16[4,96,256]{2,1,0:T(8,128)(2,1)}), bf16[4,96,256]{2,1,0:T(8,128)(2,1)S(1)}, u32[]{:S(2)}, u32[]{:S(2)}) async-start(bf16[4,96,256]{2,1,0:T(8,128)(2,1)} %shard_map.155), calls=%async_computation.2 | async-start | bytes 393216 | tf_op jit(solution)/shard_map/all_to_all | solution.py:450
  58.3 0.0 collective-permute-done.1.refs_3_.refs_4_
  58.3 0.0 collective-permute-done.2.refs_4_.refs_5_
  58.3 0.0 collective-permute-done.3.refs_5_.refs_6_
  58.3 4.8 %all-to-all-done.2.refs_0_.refs_3_ = bf16[4,96,256]{2,1,0:T(8,128)(2,1)S(1)} async-done(((bf16[4,96,256]{2,1,0:T(8,128)(2,1)}), bf16[4,96,256]{2,1,0:T(8,128)(2,1)S(1)}, u32[]{:S(2)}, u32[]{:S(2)}) %all-to-all-start.2) | async-done | bytes 196640 | tf_op jit(solution)/shard_map/all_to_all | solution.py:450
  63.2 1.6 %shard_map.157 = (bf16[16,32,384]{2,1,0:T(8,128)(2,1)}, f32[128,128]{1,0:T(8,128)S(1)}, f32[128,128]{1,0:T(8,128)S(1)}) custom-call(bf16[4,96,256]{2,1,0:T(8,128)(2,1)S(1)} %all-to-all-done.2.refs_0_.refs_3_, bf16[4,168,256]{2,1,0:T(8,128)(2,1)S(1)} %all_to_all.25.refs_0_.refs_1_.refs_2_, bf16[432,256]{1,0:T(8,128)(2,1)S(1)} %get-tuple-element.30.refs_2_.refs_3_, ...), custom_call_target="tpu_custom_call" | custom-call | flops 10000000 | bytes 1000000 | tf_op jit(solution)/shard_map/pallas_call | solution.py:58
  64.8 17.1 %all-to-all-start.3 = ((bf16[16,32,384]{2,1,0:T(8,128)(2,1)}), bf16[16,32,384]{2,1,0:T(8,128)(2,1)S(1)}, u32[]{:S(2)}, u32[]{:S(2)}) async-start(bf16[16,32,384]{2,1,0:T(8,128)(2,1)} %get-tuple-element.34), calls=%async_computation.3 | async-start | bytes 786432 | tf_op jit(solution)/shard_map/all_to_all | solution.py:450
  81.9 1.3 collective-permute-start.4
  83.2 15.9 %collective-permute-done.4.refs_2_ = f32[128,128]{1,0:T(8,128)S(1)} collective-permute-done((f32[128,128]{1,0:T(8,128)S(1)}, f32[128,128]{1,0:T(8,128)S(1)}, u32[]{:S(2)}, u32[]{:S(2)}) %collective-permute-start.4) | collective-permute-done | bytes 65568 | tf_op jit(solution)/shard_map/ppermute | solution.py:524
  99.1 0.3 shard_map.160
  99.4 1.9 %collective-permute-start.5 = (bf16[4,256,128]{2,1,0:T(8,128)(2,1)S(1)}, bf16[4,256,128]{2,1,0:T(8,128)(2,1)S(1)}, u32[]{:S(2)}, u32[]{:S(2)}) collective-permute-start(bf16[4,256,128]{2,1,0:T(8,128)(2,1)S(1)} %get-tuple-element.40), channel_id=1, source_target_pairs={{0,1},{1,0},{2,3},{3,2},{4,5},{5,4},{6,7},{7,6},{8,9},{9,8},{10,11... | collective-permute-start | bytes 786440 | tf_op jit(solution)/shard_map/ppermute | solution.py:542
  101.3 1.5 %collective-permute-done.5.refs_1_ = bf16[4,256,128]{2,1,0:T(8,128)(2,1)S(1)} collective-permute-done((bf16[4,256,128]{2,1,0:T(8,128)(2,1)S(1)}, bf16[4,256,128]{2,1,0:T(8,128)(2,1)S(1)}, u32[]{:S(2)}, u32[]{:S(2)}) %collective-permute-start.5) | collective-permute-done | bytes 262176 | tf_op jit(solution)/shard_map/ppermute | solution.py:542
  102.8 0.1 shard_map.161
  102.9 3.4 %collective-permute-start.6 = (bf16[2,256,128]{2,1,0:T(8,128)(2,1)S(1)}, bf16[2,256,128]{2,1,0:T(8,128)(2,1)S(1)}, u32[]{:S(2)}, u32[]{:S(2)}) collective-permute-start(bf16[2,256,128]{2,1,0:T(8,128)(2,1)S(1)} %get-tuple-element.42), channel_id=1, source_target_pairs={{0,2},{1,3},{2,0},{3,1},{4,6},{5,7},{6,4},{7,5},{8,10},{9,11},{10,... | collective-permute-start | bytes 393224 | tf_op jit(solution)/shard_map/ppermute | solution.py:544
  106.3 0.0 all-to-all-done.3.refs_0_
  106.3 0.3 shard_map.164
  106.6 3.2 %collective-permute-start.8 = (bf16[64,256]{1,0:T(8,128)(2,1)S(1)}, bf16[64,256]{1,0:T(8,128)(2,1)S(1)}, u32[]{:S(2)}, u32[]{:S(2)}) collective-permute-start(bf16[64,256]{1,0:T(8,128)(2,1)S(1)} %get-tuple-element.46), channel_id=1, source_target_pairs={{0,8},{8,0},{16,24},{24,16},{1,9},{9,1},{17,25},{25,17},{2,10},{10... | collective-permute-start | bytes 98312 | tf_op jit(solution)/shard_map/ppermute | solution.py:537
  109.9 0.5 collective-permute-done.6.refs_1_
  110.4 4.7 %collective-permute-start.7 = (bf16[1,256,128]{2,1,0:T(8,128)(2,1)S(1)}, bf16[1,256,128]{2,1,0:T(8,128)(2,1)S(1)}, u32[]{:S(2)}, u32[]{:S(2)}) collective-permute-start(bf16[1,256,128]{2,1,0:T(8,128)(2,1)S(1)} %get-tuple-element.44), channel_id=1, source_target_pairs={{0,6},{1,7},{2,4},{3,5},{4,2},{5,3},{6,0},{7,1},{8,14},{9,15},{10,... | collective-permute-start | bytes 196616 | tf_op jit(solution)/shard_map/ppermute | solution.py:546
  115.0 0.7 shard_map.158
  115.7 15.3 %all-to-all-start.4 = ((f32[64,1,128]{2,1,0:T(1,128)}), f32[64,1,128]{2,1,0:T(1,128)S(1)}, u32[]{:S(2)}, u32[]{:S(2)}) async-start(f32[64,1,128]{2,1,0:T(1,128)} %get-tuple-element.36), calls=%async_computation.4 | async-start | bytes 65536 | tf_op jit(solution)/shard_map/all_to_all | solution.py:450
  131.0 0.0 collective-permute-done.8.refs_1_
  131.0 3.4 %collective-permute-start.9 = (bf16[64,256]{1,0:T(8,128)(2,1)S(1)}, bf16[64,256]{1,0:T(8,128)(2,1)S(1)}, u32[]{:S(2)}, u32[]{:S(2)}) collective-permute-start(bf16[64,256]{1,0:T(8,128)(2,1)S(1)} %pad_maximum_fusion), channel_id=1, source_target_pairs={{0,24},{8,16},{16,8},{24,0},{1,25},{9,17},{17,9},{25,1},{2,26},{10... | collective-permute-start | bytes 98312 | tf_op jit(solution)/shard_map/ppermute | solution.py:539
  134.4 0.0 collective-permute-done.7.refs_1_
  134.4 0.6 shard_map.163
  135.0 1.8 %collective-permute-done.9.refs_2_ = bf16[64,256]{1,0:T(8,128)(2,1)S(1)} collective-permute-done((bf16[64,256]{1,0:T(8,128)(2,1)S(1)}, bf16[64,256]{1,0:T(8,128)(2,1)S(1)}, u32[]{:S(2)}, u32[]{:S(2)}) %collective-permute-start.9) | collective-permute-done | bytes 32800 | tf_op jit(solution)/shard_map/ppermute | solution.py:539
  136.8 2.3 %shard_map.165 = (bf16[128,256]{1,0:T(8,128)(2,1)}, bf16[128,128]{1,0:T(8,128)(2,1)}, f32[4,128]{1,0:T(4,128)}, bf16[128,256]{1,0:T(8,128)(2,1)}) custom-call(bf16[32,256]{1,0:T(8,128)(2,1)S(1)} %get-tuple-element.45.refs_0_, bf16[64,256]{1,0:T(8,128)(2,1)S(1)} %collective-permute-done.8.refs_1_, bf16[64,256]{1,0:T(8,128)(2,1)S(1)} %collective-permute-done.9.refs_2_, ...), custom_call_target="tpu_custom_call" | custom-call | flops 10000000 | bytes 1000000 | tf_op jit(solution)/shard_map/pallas_call | solution.py:58
  139.1 5.6 %all-to-all-done.4.refs_0_ = f32[64,1,128]{2,1,0:T(1,128)S(1)} async-done(((f32[64,1,128]{2,1,0:T(1,128)}), f32[64,1,128]{2,1,0:T(1,128)S(1)}, u32[]{:S(2)}, u32[]{:S(2)}) %all-to-all-start.4) | async-done | bytes 32800 | tf_op jit(solution)/shard_map/all_to_all | solution.py:450
  144.7 0.5 shard_map.159
  (17 shorter events, 0.1 us)
Async XLA Ops:
  18.1 12.3 %copy-start.1 = (bf16[128,2048]{1,0:T(8,128)(2,1)S(1)}, bf16[128,2048]{1,0:T(8,128)(2,1)}, u32[]{:S(2)}) copy-start(bf16[128,2048]{1,0:T(8,128)(2,1)} %refs_7_.2) | copy-start | bytes 1572868
  18.1 18.1 %copy-start.5 = (bf16[128,128]{1,0:T(8,128)(2,1)S(1)}, bf16[128,128]{1,0:T(8,128)(2,1)}, u32[]{:S(2)}) copy-start(bf16[128,128]{1,0:T(8,128)(2,1)} %refs_9_.1) | copy-start | bytes 98308
  18.1 18.1 %copy-start.6 = (f32[128,4]{0,1:T(4,128)S(1)}, f32[128,4]{0,1:T(4,128)}, u32[]{:S(2)}) copy-start(f32[128,4]{0,1:T(4,128)} %param.15) | copy-start | bytes 6148
  18.1 18.1 %copy-start.7 = (f32[128,4]{0,1:T(4,128)S(1)}, f32[128,4]{0,1:T(4,128)}, u32[]{:S(2)}) copy-start(f32[128,4]{0,1:T(4,128)} %param.17) | copy-start | bytes 6148
  18.1 18.1 %copy-start.8 = (f32[4,128]{1,0:T(4,128)S(1)}, f32[4,128]{1,0:T(4,128)}, u32[]{:S(2)}) copy-start(f32[4,128]{1,0:T(4,128)} %refs_6_.5) | copy-start | bytes 6148
  18.1 18.1 %copy-start.9 = (f32[4]{0:T(128)S(1)}, f32[4]{0:T(128)}, u32[]{:S(2)}) copy-start(f32[4]{0:T(128)} %param.16) | copy-start | bytes 52
  18.9 17.3 %copy-start = (bf16[128,2048]{1,0:T(8,128)(2,1)S(1)}, bf16[128,2048]{1,0:T(8,128)(2,1)}, u32[]{:S(2)}) copy-start(bf16[128,2048]{1,0:T(8,128)(2,1)} %refs_0_.1) | copy-start | bytes 1572868
  18.9 17.3 %copy-start.3 = (bf16[128,256]{1,0:T(8,128)(2,1)S(1)}, bf16[128,256]{1,0:T(8,128)(2,1)}, u32[]{:S(2)}) copy-start(bf16[128,256]{1,0:T(8,128)(2,1)} %refs_8_.3) | copy-start | bytes 196612
  18.9 17.4 %copy-start.4 = (bf16[128,256]{1,0:T(8,128)(2,1)S(1)}, bf16[128,256]{1,0:T(8,128)(2,1)}, u32[]{:S(2)}) copy-start(bf16[128,256]{1,0:T(8,128)(2,1)} %refs_10_.3) | copy-start | bytes 196612
  18.9 34.9 %all-to-all-start.1 = ((bf16[16,40,256]{2,1,0:T(8,128)(2,1)}), bf16[16,40,256]{2,1,0:T(8,128)(2,1)S(1)}, u32[]{:S(2)}, u32[]{:S(2)}) async-start(bf16[16,40,256]{2,1,0:T(8,128)(2,1)} %shard_map.154), calls=%async_computation.1 | async-start | bytes 655360 | tf_op jit(solution)/shard_map/all_to_all | solution.py:450
  30.4 5.9 %copy-start.2 = (bf16[128,256]{1,0:T(8,128)(2,1)S(1)}, bf16[128,256]{1,0:T(8,128)(2,1)}, u32[]{:S(2)}) copy-start(bf16[128,256]{1,0:T(8,128)(2,1)} %refs_7_.3) | copy-start | bytes 196612
  30.4 5.8 %collective-permute-start = (bf16[8,2048]{1,0:T(8,128)(2,1)S(1)}, bf16[8,2048]{1,0:T(8,128)(2,1)S(1)}, u32[]{:S(2)}, u32[]{:S(2)}) collective-permute-start(bf16[8,2048]{1,0:T(8,128)(2,1)S(1)} %slice.6), channel_id=1, source_target_pairs={{0,8},{8,16},{16,24},{24,32},{32,40},{40,48},{48,56},{56,64},{64,7... | collective-permute-start | bytes 98312 | tf_op jit(solution)/shard_map/ppermute | solution.py:497
  38.4 19.9 %collective-permute-start.1 = (bf16[432,256]{1,0:T(8,128)(2,1)S(1)}, bf16[432,256]{1,0:T(8,128)(2,1)S(1)}, u32[]{:S(2)}, u32[]{:S(2)}) collective-permute-start(bf16[432,256]{1,0:T(8,128)(2,1)S(1)} %get-tuple-element.31), channel_id=1, source_target_pairs={{0,8},{8,16},{16,24},{24,0},{1,9},{9,17},{17,25},{25,1},{2,10},{10... | collective-permute-start | bytes 663560 | tf_op jit(solution)/shard_map/ppermute | solution.py:459
  40.6 17.7 %collective-permute-start.2 = (bf16[432,256]{1,0:T(8,128)(2,1)S(1)}, bf16[432,256]{1,0:T(8,128)(2,1)S(1)}, u32[]{:S(2)}, u32[]{:S(2)}) collective-permute-start(bf16[432,256]{1,0:T(8,128)(2,1)S(1)} %get-tuple-element.32), channel_id=1, source_target_pairs={{0,16},{8,24},{16,0},{24,8},{1,17},{9,25},{17,1},{25,9},{2,18},{10... | collective-permute-start | bytes 663560 | tf_op jit(solution)/shard_map/ppermute | solution.py:459
  49.3 9.0 %collective-permute-start.3 = (bf16[432,256]{1,0:T(8,128)(2,1)S(1)}, bf16[432,256]{1,0:T(8,128)(2,1)S(1)}, u32[]{:S(2)}, u32[]{:S(2)}) collective-permute-start(bf16[432,256]{1,0:T(8,128)(2,1)S(1)} %get-tuple-element.33), channel_id=1, source_target_pairs={{0,24},{8,0},{16,8},{24,16},{1,25},{9,1},{17,9},{25,17},{2,26},{10... | collective-permute-start | bytes 663560 | tf_op jit(solution)/shard_map/ppermute | solution.py:459
  54.9 8.2 %all-to-all-start.2 = ((bf16[4,96,256]{2,1,0:T(8,128)(2,1)}), bf16[4,96,256]{2,1,0:T(8,128)(2,1)S(1)}, u32[]{:S(2)}, u32[]{:S(2)}) async-start(bf16[4,96,256]{2,1,0:T(8,128)(2,1)} %shard_map.155), calls=%async_computation.2 | async-start | bytes 393216 | tf_op jit(solution)/shard_map/all_to_all | solution.py:450
  64.8 41.6 %all-to-all-start.3 = ((bf16[16,32,384]{2,1,0:T(8,128)(2,1)}), bf16[16,32,384]{2,1,0:T(8,128)(2,1)S(1)}, u32[]{:S(2)}, u32[]{:S(2)}) async-start(bf16[16,32,384]{2,1,0:T(8,128)(2,1)} %get-tuple-element.34), calls=%async_computation.3 | async-start | bytes 786432 | tf_op jit(solution)/shard_map/all_to_all | solution.py:450
  81.9 17.2 %collective-permute-start.4 = (f32[128,128]{1,0:T(8,128)S(1)}, f32[128,128]{1,0:T(8,128)S(1)}, u32[]{:S(2)}, u32[]{:S(2)}) collective-permute-start(f32[128,128]{1,0:T(8,128)S(1)} %get-tuple-element.38), channel_id=1, source_target_pairs={{32,0},{64,32},{96,64},{128,96},{160,128},{192,160},{224,192},{256... | collective-permute-start | bytes 196616 | tf_op jit(solution)/shard_map/ppermute | solution.py:524
  99.4 3.4 %collective-permute-start.5 = (bf16[4,256,128]{2,1,0:T(8,128)(2,1)S(1)}, bf16[4,256,128]{2,1,0:T(8,128)(2,1)S(1)}, u32[]{:S(2)}, u32[]{:S(2)}) collective-permute-start(bf16[4,256,128]{2,1,0:T(8,128)(2,1)S(1)} %get-tuple-element.40), channel_id=1, source_target_pairs={{0,1},{1,0},{2,3},{3,2},{4,5},{5,4},{6,7},{7,6},{8,9},{9,8},{10,11... | collective-permute-start | bytes 786440 | tf_op jit(solution)/shard_map/ppermute | solution.py:542
  102.9 7.4 %collective-permute-start.6 = (bf16[2,256,128]{2,1,0:T(8,128)(2,1)S(1)}, bf16[2,256,128]{2,1,0:T(8,128)(2,1)S(1)}, u32[]{:S(2)}, u32[]{:S(2)}) collective-permute-start(bf16[2,256,128]{2,1,0:T(8,128)(2,1)S(1)} %get-tuple-element.42), channel_id=1, source_target_pairs={{0,2},{1,3},{2,0},{3,1},{4,6},{5,7},{6,4},{7,5},{8,10},{9,11},{10,... | collective-permute-start | bytes 393224 | tf_op jit(solution)/shard_map/ppermute | solution.py:544
  106.6 24.4 %collective-permute-start.8 = (bf16[64,256]{1,0:T(8,128)(2,1)S(1)}, bf16[64,256]{1,0:T(8,128)(2,1)S(1)}, u32[]{:S(2)}, u32[]{:S(2)}) collective-permute-start(bf16[64,256]{1,0:T(8,128)(2,1)S(1)} %get-tuple-element.46), channel_id=1, source_target_pairs={{0,8},{8,0},{16,24},{24,16},{1,9},{9,1},{17,25},{25,17},{2,10},{10... | collective-permute-start | bytes 98312 | tf_op jit(solution)/shard_map/ppermute | solution.py:537
  110.4 24.0 %collective-permute-start.7 = (bf16[1,256,128]{2,1,0:T(8,128)(2,1)S(1)}, bf16[1,256,128]{2,1,0:T(8,128)(2,1)S(1)}, u32[]{:S(2)}, u32[]{:S(2)}) collective-permute-start(bf16[1,256,128]{2,1,0:T(8,128)(2,1)S(1)} %get-tuple-element.44), channel_id=1, source_target_pairs={{0,6},{1,7},{2,4},{3,5},{4,2},{5,3},{6,0},{7,1},{8,14},{9,15},{10,... | collective-permute-start | bytes 196616 | tf_op jit(solution)/shard_map/ppermute | solution.py:546
  115.7 29.1 %all-to-all-start.4 = ((f32[64,1,128]{2,1,0:T(1,128)}), f32[64,1,128]{2,1,0:T(1,128)S(1)}, u32[]{:S(2)}, u32[]{:S(2)}) async-start(f32[64,1,128]{2,1,0:T(1,128)} %get-tuple-element.36), calls=%async_computation.4 | async-start | bytes 65536 | tf_op jit(solution)/shard_map/all_to_all | solution.py:450
  131.0 5.8 %collective-permute-start.9 = (bf16[64,256]{1,0:T(8,128)(2,1)S(1)}, bf16[64,256]{1,0:T(8,128)(2,1)S(1)}, u32[]{:S(2)}, u32[]{:S(2)}) collective-permute-start(bf16[64,256]{1,0:T(8,128)(2,1)S(1)} %pad_maximum_fusion), channel_id=1, source_target_pairs={{0,24},{8,16},{16,8},{24,0},{1,25},{9,17},{17,9},{25,1},{2,26},{10... | collective-permute-start | bytes 98312 | tf_op jit(solution)/shard_map/ppermute | solution.py:539

commit v4 on v3

--- a/solution.py
+++ b/solution.py
@@ -85,11 +85,6 @@
 def from_peers(parts):
     yi = lax.axis_index("y")
     return [choose(parts, lax.rem(yi + Y - j, Y)) for j in range(Y)]
-
-
-def by_mask(parts):
-    yi = lax.axis_index("y")
-    return [choose(parts, jnp.bitwise_xor(yi, j)) for j in range(Y)]
 
 
 def columns_at(ref, start, size):
@@ -265,7 +260,8 @@
     return acc
 
 
-def bwd_far(far, got):
+def bwd_far(far, got, m0, m1, m2, m3):
+    mid = from_peers([m0, m1, m2, m3])
     count = far.shape[0]
     zrow = lax.axis_index("z")
     tau, upto = chain_sums(far)
@@ -281,7 +277,17 @@
             state = got[j, :NS].astype(F32) + jnp.exp(tau_j[j : j + 1]) * state
     dk = [dot(ends[j], got[j, NS + PAD :], 1, 1).astype(BF16) for j in range(Y)]
     halves = [jnp.concatenate(dk[i : i + 2], axis=1) for i in range(0, Y, 2)]
-    return jnp.stack([jnp.concatenate([*halves, ends[j]], axis=0) for j in range(Y)])
+    begins = [jnp.zeros((NS, HP), F32)]
+    for j in range(Y - 1):
+        begins.append(
+            mid[j][TOK : TOK + NS].astype(F32) + jnp.exp(tau_j[j : j + 1]) * begins[j]
+        )
+    return jnp.stack(
+        [
+            jnp.concatenate([*halves, ends[j], begins[j].astype(BF16)], axis=0)
+            for j in range(Y)
+        ]
+    )
 
 
 def key_grads(near, got, m0, m1, m2, m3, taps):
@@ -317,42 +323,33 @@
         dw = dw + dot(xs, pg[:, TOK * j : TOK * (j + 1)], 1, 1)
     dw = dw.astype(BF16)
     fwd = fwd_group(got, mid)
+    count = dw.shape[0] // NS
+    each = NS // count
+    row, col = iota2((PAD * count, NS), 0), iota2((PAD * count, NS), 1)
+    part = lax.rem(row, PAD)
+    target = lax.div(row, PAD) * each + lax.rem(part, each)
+    tail = jnp.zeros((PAD * count, STATE), F32)
+    for half in range(2):
+        pick = (col == target) & (lax.div(part, each) == half)
+        tail = tail + dot(pick.astype(BF16), fwd[:, STATE * half : STATE * (half + 1)])
+    tail = tail.astype(BF16)
     send = jnp.stack(
         [
-            jnp.concatenate([dw[NS * i : NS * (i + 1)], fwd], axis=1)
-            for i in range(dw.shape[0] // NS)
+            jnp.concatenate(
+                [dw[NS * i : NS * (i + 1)], tail[PAD * i : PAD * (i + 1)]], axis=0
+            )
+            for i in range(count)
         ]
     )
     own = choose([main[:, TOK * j : TOK * (j + 1)] for j in range(Y)], yi)
-    return send, own, over
-
-
-def fwd_apply(near, bfar, got, m0, m1, m2, m3):
-    mid = from_peers([m0, m1, m2, m3])
-    far = near[:, :, near.shape[2] - HP :]
-    zrow = lax.axis_index("z")
-    count = far.shape[0]
-    tau, upto = chain_sums(bfar)
-    row = iota2((count, HP), 0)
-    before = jnp.sum(jnp.where(row == zrow, upto - tau, 0.0), axis=0, keepdims=True)
-    weights = jnp.exp(jnp.where(row < zrow, before - upto, -1e30))
-    state = weighted(weights, far)
-    tau_j = joined(got, NS)
-    at = slice(TOK, TOK + NS)
-    res = []
-    for j in range(Y):
-        res.append(state.astype(BF16))
-        if j < Y - 1:
-            state = mid[j][at].astype(F32) + jnp.exp(tau_j[j : j + 1]) * state
-    mine, one, two, three = by_mask(res)
-    return mine, jnp.concatenate([one, two], axis=0), three
-
-
-def finish(mine, first, second, near, tpre, aexp, jump, gate, adj, q, v, keys):
+    eye = (iota2((PAD, PAD), 0) == iota2((PAD, PAD), 1)).astype(F32)
+    return send, own, dot(eye, over[:, TOK - PAD :], 1, 1, HIGH)
+
+
+def finish_near(near, got, tpre, aexp, jump, gate, adj, q, v, keys):
     step, rate, la, cum = decays(tpre, aexp, jump)
     cum_t = row_form(la)
-    s_in = jnp.concatenate(by_mask([mine, first[:NS], second[NS:], second[:NS]]), axis=0)
-    g_out = jnp.concatenate([near[i, 2 * NS :] for i in range(Y)], axis=0)
+    g_out = jnp.concatenate([near[i, 2 * NS : 3 * NS] for i in range(Y)], axis=0)
     g = gate.astype(F32)
     a = adj.astype(F32)
     sig = sigmoid(g)
@@ -364,7 +361,6 @@
     d = expand(jnp.exp(cum[TOK - 1 :] - cum))
     dyb, ub = dy.astype(BF16), u.astype(BF16)
     scores = dot(q, keys)
-    y_far = e * dot(q, s_in)
     du_far = d * dot(keys, g_out, 0, 0)
     dc = jnp.zeros((TOK, TOK), F32)
     ys, dus, diffs = [], [], []
@@ -379,24 +375,67 @@
         lc = (mask * scores).astype(BF16)
         ys.append(dot(lc, ub[:, at]))
         dus.append(dot(lc, dyb[:, at], 0, 0))
-    y = y_far + jnp.concatenate(ys, axis=1)
+    y = jnp.concatenate(ys, axis=1)
     du = du_far + jnp.concatenate(dus, axis=1)
-    pick = (iota2((R, HP), 1) // HEAD == iota2((R, HP), 0)).astype(F32)
+    pick = head_pick()
     from_d = dot(pick, u * du_far, 1, 1, HIGH)
-    dcum = jnp.concatenate(diffs, axis=0) + dot(pick, dy * y_far, 1, 1, HIGH) - from_d
-    kept = jnp.sum(s_in.astype(F32) * g_out.astype(F32), axis=0, keepdims=True)
-    kept = kept * expand(jnp.exp(cum[TOK - 1 :]))
-    dtot = jnp.sum(from_d, axis=1, keepdims=True) + jnp.sum(pick * kept, axis=1, keepdims=True)
-    later = (iota2((TOK, TOK), 0) >= iota2((TOK, TOK), 1)).astype(F32)
-    dla = dot(dcum, later, precision=HIGH) + dtot
+    dcum = jnp.concatenate(diffs, axis=0) - from_d
+    dtot = jnp.sum(from_d, axis=1, keepdims=True)
+    gain = sigmoid(tpre)
+    dla = dot(dcum, later_mask(), precision=HIGH) + dtot
     dstep = dot(pick, du * vw, 1, 1, HIGH) - rate * dla
-    decay_grad = dstep * sigmoid(tpre)
-    value_grad = (du * stepw).astype(BF16)
-    query_grad = (
-        dot(dc.astype(BF16), keys, 1, 1) + dot((dy * e).astype(BF16), s_in, 1, 1)
-    ).astype(BF16)
-    gate_grad = (a * y * (sig * (1.0 + g * (1.0 - sig)))).astype(BF16)
-    return value_grad, query_grad, decay_grad, gate_grad
+    tau = joined(got, NS)
+    yi = lax.axis_index("y")
+    since = jnp.sum(jnp.where(iota2((Y, HP), 0) < yi, tau, 0.0), axis=0, keepdims=True)
+    return (
+        (du * stepw).astype(BF16),
+        dot(dc.astype(BF16), keys, 1, 1),
+        dstep * gain,
+        rate * gain,
+        y,
+        a * (sig * (1.0 + g * (1.0 - sig))),
+        e,
+        (dy * e).astype(BF16),
+        jnp.exp(since),
+        expand(jnp.exp(cum[TOK - 1 :])),
+    )
+
+
+def head_pick():
+    return (lax.div(iota2((R, HP), 1), HEAD) == iota2((R, HP), 0)).astype(F32)
+
+
+def later_mask():
+    return (iota2((TOK, TOK), 0) >= iota2((TOK, TOK), 1)).astype(F32)
+
+
+def finish_far(got, near, q, dq_in, dstep, coef, y_in, slope, e, dye, since, total):
+    flat = got.reshape(got.shape[0] * PAD, STATE)
+    rows = flat.shape[0]
+    each = NS // lax.axis_size("z")
+    n, col = iota2((STATE, rows), 0), iota2((STATE, rows), 1)
+    inner = lax.rem(n, NS)
+    source = lax.div(inner, each) * Y + lax.div(n, NS)
+    place = source * PAD + lax.rem(inner, each)
+    s_in = jnp.concatenate(
+        [dot((col == place + each * half).astype(BF16), flat) for half in range(2)], axis=1
+    )
+    within = lax.rem(iota2((PAD, rows), 1), PAD)
+    chosen = ((within >= 4) & (within < 7)).astype(BF16)
+    squares = dot(chosen, flat)[:1]
+    begin = jnp.concatenate([near[i, 3 * NS :] for i in range(Y)], axis=0).astype(F32)
+    s_in = (s_in * since + begin).astype(BF16)
+    g_out = jnp.concatenate([near[i, 2 * NS : 3 * NS] for i in range(Y)], axis=0)
+    read = dot(q, s_in)
+    gate_grad = (slope * (y_in + e * read)).astype(BF16)
+    query_grad = (dq_in + dot(dye, s_in, 1, 1)).astype(BF16)
+    pick = head_pick()
+    from_e = dot(pick, dye.astype(F32) * read, 1, 1, HIGH)
+    kept = jnp.sum(s_in.astype(F32) * g_out.astype(F32), axis=0, keepdims=True) * total
+    extra = dot(from_e, later_mask(), precision=HIGH) + jnp.sum(
+        pick * kept, axis=1, keepdims=True
+    )
+    return squares, query_grad, dstep - coef * extra, gate_grad
 
 
 def summed(parts):
@@ -406,16 +445,30 @@
     return acc
 
 
-def weight_sum(near):
-    acc = summed(near[:, :, :STATE])
-    count = lax.axis_size("z") * Y
-    squares = jnp.sum(acc * acc, axis=0, keepdims=True)
-    return acc, jnp.broadcast_to(squares[None], (count, 1, STATE))
+def weight_sum(near, far):
+    acc = summed(near[:, :NS])
+    squares = split3(jnp.sum(acc * acc, axis=0, keepdims=True))
+    count = near.shape[0]
+    each = NS // count
+    tau = jnp.exp(joined(far, NS))
+    row = iota2((PAD, STATE), 0)
+    marks = jnp.zeros((PAD, STATE), F32)
+    for i, part in enumerate(squares):
+        marks = jnp.where(row == 4 + i, part.astype(F32), marks)
+    state = jnp.zeros((PAD, STATE), F32)
+    blocks = []
+    for i in range(count):
+        blocks += [(state + marks).astype(BF16)] * Y
+        decay = jnp.where(row < each, tau[i : i + 1, :STATE], tau[i : i + 1, STATE:])
+        state = decay * state + near[i, NS:].astype(F32)
+    return acc, jnp.stack(blocks)
 
 
 def partial_input(w, own, after):
     edge = lax.axis_index("y") == Y - 1
-    grad = (own + jnp.where(edge, after, 0.0)).astype(BF16)
+    spot = iota2((PAD, TOK), 1) == iota2((PAD, TOK), 0) + (TOK - PAD)
+    spread = dot(after, spot.astype(F32), 0, 0, HIGH)
+    grad = (own + jnp.where(edge, spread, 0.0)).astype(BF16)
     place = lax.axis_index("tp")
     width = w.shape[1] // lax.axis_size("tp")
     core = lax.rem(place, 2)
@@ -440,10 +493,6 @@
 
 def last_sum(mine, other):
     return (mine[0].astype(F32) + other[0].astype(F32)).astype(BF16)
-
-
-def square_sum(parts):
-    return jnp.sum(parts[:, 0, :], axis=0, keepdims=True)
 
 
 def exchange(parts, axis):
@@ -510,11 +559,11 @@
     mids = around(mids, "y", 1)
     bwd_totals = local(bwd_group, sds((zs, NS + PAD, HP), BF16), got)
     far = exchange(bwd_totals, "z")
-    ends = local(bwd_far, sds((Y, 3 * NS, HP), BF16), far, got)
+    ends = local(bwd_far, sds((Y, 4 * NS, HP), BF16), far, got, *mids)
     ends = exchange(ends, "y")
     send, own, over = local(
         key_grads,
-        [sds((zs, NS, STATE + HP), BF16), sds((STATE, TOK), F32), sds((STATE, TOK), F32)],
+        [sds((zs, NS + PAD, STATE), BF16), sds((STATE, TOK), F32), sds((PAD, STATE), F32)],
         ends,
         got,
         *mids,
@@ -522,21 +571,32 @@
     )
     near = exchange(send, "z")
     after = lax.ppermute(over, "z", [(i, i - 1) for i in range(1, zs)])
+    wide = sds((TOK, HP), F32)
+    value_grad, dq_in, dstep, coef, y_in, slope, e, dye, since, total = local(
+        finish_near,
+        [
+            sds((TOK, HP), BF16),
+            sds((TOK, STATE), F32),
+            sds((R, TOK), F32),
+            sds((R, TOK), F32),
+            wide,
+            wide,
+            wide,
+            sds((TOK, HP), BF16),
+            sds((1, HP), F32),
+            sds((1, HP), F32),
+        ],
+        ends,
+        got,
+        *small,
+        q,
+        v,
+        keys,
+    )
     weight_t, squares = local(
-        weight_sum, [sds((NS, STATE), F32), sds((sp, 1, STATE), F32)], near
+        weight_sum, [sds((NS, STATE), F32), sds((sp, PAD, STATE), BF16)], near, far
     )
     squares = exchange(squares, ZY)
-    mine, first, second = local(
-        fwd_apply,
-        [sds((NS, HP), BF16), sds((2 * NS, HP), BF16), sds((NS, HP), BF16)],
-        near,
-        far,
-        got,
-        *mids,
-    )
-    first = lax.ppermute(first, "y", [(i, i ^ 1) for i in range(Y)])
-    second = jnp.concatenate([second, first[NS:]], axis=0)
-    second = lax.ppermute(second, "y", [(i, i ^ 3) for i in range(Y)])
     share = (features // tp, TOK)
     keep, give = local(partial_input, [sds((4, *share), BF16)] * 2, w, own, after, raw=(0,))
     give = lax.ppermute(give, "tp", [(i, i ^ 1) for i in range(tp)])
@@ -545,22 +605,30 @@
     keep, give = local(half_sum, [sds((1, *share), BF16)] * 2, keep, give)
     give = lax.ppermute(give, "tp", [(i, i ^ 6) for i in range(tp)])
     input_grad = local(last_sum, sds(share, BF16), keep, give)
-    value_grad, query_grad, decay_grad, gate_grad = local(
-        finish,
-        [sds((TOK, HP), BF16), sds((TOK, STATE), BF16), sds((R, TOK), F32), sds((TOK, HP), BF16)],
-        mine,
-        first,
-        second,
+    row_squares, query_grad, decay_grad, gate_grad = local(
+        finish_far,
+        [
+            sds((1, STATE), F32),
+            sds((TOK, STATE), BF16),
+            sds((R, TOK), F32),
+            sds((TOK, HP), BF16),
+        ],
+        squares,
         ends,
-        *small,
         q,
-        v,
-        keys,
-    )
-    row_squares = local(square_sum, sds((1, STATE), F32), squares).reshape(STATE)
+        dq_in,
+        dstep,
+        coef,
+        y_in,
+        slope,
+        e,
+        dye,
+        since,
+        total,
+    )
     return (
         weight_t.T,
-        row_squares,
+        row_squares.reshape(STATE),
         input_grad,
         value_grad,
         query_grad,

time: 146 us -> 137 us (0.938)
  the two profiles are of different devices: /device:TPU:8 before, /device:TPU:6 now
where the time goes in v4:
time: 137 us; the launch traced here: 136 us
  blocking collectives  54.5 us (40%)
  starting transfers between devices  47.2 us (34%)
  waiting for transfers between devices  21 us (15%)
  Pallas kernels  12.2 us (9%)
    all_to_all x3, blocking collectives, exchange(): return lax.all_to_all(parts, axis, split_axis=0, concat_axis=0, tiled=True)  54.5 us
    all_to_all x2, starting transfers between devices, exchange(): return lax.all_to_all(parts, axis, split_axis=0, concat_axis=0, tiled=True)  20.6 us
    ppermute x3, starting transfers between devices, around(): got.append(lax.ppermute(parts[d], axis, route))  15.8 us
    pallas_call x12, Pallas kernels, local(): pl.pallas_call(kernel, out_shape=shapes, in_specs=[vm] * len(args), out_s...  12.2 us
    ppermute x3, waiting for transfers between devices, around(): got.append(lax.ppermute(parts[d], axis, route))  5.89 us
    ppermute x1, waiting for transfers between devices, step(): give = lax.ppermute(give, 'tp', [(i, i ^ 2) for i in range(tp)])  4.68 us
    ppermute x1, waiting for transfers between devices, step(): after = lax.ppermute(over, 'z', [(i, i - 1) for i in range(1, zs)])  4.34 us
    ppermute x1, waiting for transfers between devices, step(): give = lax.ppermute(give, 'tp', [(i, i ^ 6) for i in range(tp)])  3.04 us
  transfers between devices with their start and end apart: 10, of which 7 were waited for; matrix products, arithmetic and copies ran while one was open for 0% of the time, Pallas kernels for 4%

profile of v4, /device:TPU:6, one launch (start us, length us, event | category | flops | bytes accessed | tf_op | source)
XLA Modules:
  0.0 135.9 jit_solution(4553571772572223218)
XLA Ops:
  0.6 2.6 %shard_map.153 = bf16[4,168,256]{2,1,0:T(8,128)(2,1)} custom-call(f32[4,128]{1,0:T(4,128)} %bitcast.6, f32[1,4]{1,0:T(1,128)} %bitcast.12, f32[4,128]{1,0:T(4,128)} %bitcast.9, bf16[128,256]{1,0:T(8,128)(2,1)} %refs_5_.5, bf16[128,256]{1,0:T(8,128)(2,1)} %refs_6_.7, bf16[128,128]{1,0:T(8,128)(2,1)} %refs_2_.1, bf16[128,256]{1,0:T(8,128)(2,1)} %refs_8_.3), custom_call_target="tpu_custom_call" | custom-call | flops 10000000 | bytes 1000000 | tf_op jit(solution)/shard_map/pallas_call | solution.py:58
  3.2 12.0 %all_to_all.25.refs_0_.refs_1_ = bf16[4,168,256]{2,1,0:T(8,128)(2,1)S(1)} all-to-all(bf16[4,168,256]{2,1,0:T(8,128)(2,1)} %shard_map.153), channel_id=1, replica_groups=mesh['z'=16,'y'=4,'tp'=8] {'y'}, dimensions={0} | all-to-all | bytes 688128 | tf_op jit(solution)/shard_map/all_to_all | solution.py:499
  15.2 0.0 copy-start.1
  15.2 0.0 copy-start.8
  15.3 0.0 copy-start.9
  15.3 0.8 shard_map.154
  16.0 15.3 %all-to-all-start.1 = ((bf16[16,40,256]{2,1,0:T(8,128)(2,1)}), bf16[16,40,256]{2,1,0:T(8,128)(2,1)S(1)}, u32[]{:S(2)}, u32[]{:S(2)}) async-start(bf16[16,40,256]{2,1,0:T(8,128)(2,1)} %shard_map.154), calls=%async_computation.1 | async-start | bytes 655360 | tf_op jit(solution)/shard_map/all_to_all | solution.py:499
  31.4 0.0 copy-done.1
  31.4 0.0 copy-start.2
  31.4 2.5 %collective-permute-start = (bf16[8,2048]{1,0:T(8,128)(2,1)S(1)}, bf16[8,2048]{1,0:T(8,128)(2,1)S(1)}, u32[]{:S(2)}, u32[]{:S(2)}) collective-permute-start(bf16[8,2048]{1,0:T(8,128)(2,1)S(1)} %slice.3), channel_id=1, source_target_pairs={{0,8},{8,16},{16,24},{24,32},{32,40},{40,48},{48,56},{56,64},{64,7... | collective-permute-start | bytes 98312 | tf_op jit(solution)/shard_map/ppermute | solution.py:546
  33.9 1.6 %collective-permute-done.refs_9_ = bf16[8,2048]{1,0:T(8,128)(2,1)S(1)} collective-permute-done((bf16[8,2048]{1,0:T(8,128)(2,1)S(1)}, bf16[8,2048]{1,0:T(8,128)(2,1)S(1)}, u32[]{:S(2)}, u32[]{:S(2)}) %collective-permute-start) | collective-permute-done | bytes 32800 | tf_op jit(solution)/shard_map/ppermute | solution.py:546
  35.5 0.0 copy-done.5
  35.5 0.0 copy-done.6
  35.5 0.0 copy-done.7
  35.5 0.0 copy-done.8
  35.5 0.0 copy-done.9
  35.5 0.0 copy-done
  35.5 0.0 copy-done.3
  35.5 0.0 copy-done.4
  35.5 0.0 copy-done.2
  35.5 2.1 %shard_map.155 = (bf16[432,256]{1,0:T(8,128)(2,1)S(1)}, bf16[432,256]{1,0:T(8,128)(2,1)S(1)}, bf16[432,256]{1,0:T(8,128)(2,1)S(1)}, bf16[432,256]{1,0:T(8,128)(2,1)S(1)}, bf16[128,128]{1,0:T(8,128)(2,1)S(1)}) custom-call(f32[4,128]{1,0:T(4,128)S(1)} %bitcast.7, f32[1,4]{1,0:T(1,128)S(1)} %bitcast.13, f32[4,128]{1,0:T(4,128)S(1)} %bitcast.10, ...), custom_call_target="tpu_custom_call" | custom-call | flops 10000000 | bytes 1000000 | tf_op jit(solution)/shard_map/pallas_call | solution.py:58
  37.6 4.2 %collective-permute-start.1 = (bf16[432,256]{1,0:T(8,128)(2,1)S(1)}, bf16[432,256]{1,0:T(8,128)(2,1)S(1)}, u32[]{:S(2)}, u32[]{:S(2)}) collective-permute-start(bf16[432,256]{1,0:T(8,128)(2,1)S(1)} %get-tuple-element.38), channel_id=1, source_target_pairs={{0,8},{8,16},{16,24},{24,0},{1,9},{9,17},{17,25},{25,1},{2,10},{10... | collective-permute-start | bytes 663560 | tf_op jit(solution)/shard_map/ppermute | solution.py:508
  41.9 9.6 %collective-permute-start.2 = (bf16[432,256]{1,0:T(8,128)(2,1)S(1)}, bf16[432,256]{1,0:T(8,128)(2,1)S(1)}, u32[]{:S(2)}, u32[]{:S(2)}) collective-permute-start(bf16[432,256]{1,0:T(8,128)(2,1)S(1)} %get-tuple-element.39), channel_id=1, source_target_pairs={{0,16},{8,24},{16,0},{24,8},{1,17},{9,25},{17,1},{25,9},{2,18},{10... | collective-permute-start | bytes 663560 | tf_op jit(solution)/shard_map/ppermute | solution.py:508
  51.5 1.9 %collective-permute-start.3 = (bf16[432,256]{1,0:T(8,128)(2,1)S(1)}, bf16[432,256]{1,0:T(8,128)(2,1)S(1)}, u32[]{:S(2)}, u32[]{:S(2)}) collective-permute-start(bf16[432,256]{1,0:T(8,128)(2,1)S(1)} %get-tuple-element.40), channel_id=1, source_target_pairs={{0,24},{8,0},{16,8},{24,16},{1,25},{9,1},{17,9},{25,17},{2,26},{10... | collective-permute-start | bytes 663560 | tf_op jit(solution)/shard_map/ppermute | solution.py:508
  53.4 0.0 collective-permute-done.1.refs_3_
  53.4 2.4 %collective-permute-done.2.refs_4_ = bf16[432,256]{1,0:T(8,128)(2,1)S(1)} collective-permute-done((bf16[432,256]{1,0:T(8,128)(2,1)S(1)}, bf16[432,256]{1,0:T(8,128)(2,1)S(1)}, u32[]{:S(2)}, u32[]{:S(2)}) %collective-permute-start.2) | collective-permute-done | bytes 221216 | tf_op jit(solution)/shard_map/ppermute | solution.py:508
  55.8 3.5 %collective-permute-done.3.refs_5_ = bf16[432,256]{1,0:T(8,128)(2,1)S(1)} collective-permute-done((bf16[432,256]{1,0:T(8,128)(2,1)S(1)}, bf16[432,256]{1,0:T(8,128)(2,1)S(1)}, u32[]{:S(2)}, u32[]{:S(2)}) %collective-permute-start.3) | collective-permute-done | bytes 221216 | tf_op jit(solution)/shard_map/ppermute | solution.py:508
  59.3 0.0 all-to-all-done.1.refs_0_.refs_1_
  59.3 0.4 shard_map.156
  59.7 9.1 %all_to_all.26.refs_0_.refs_1_ = bf16[4,128,256]{2,1,0:T(8,128)(2,1)S(1)} all-to-all(bf16[4,128,256]{2,1,0:T(8,128)(2,1)S(1)} %shard_map.156), channel_id=1, replica_groups=mesh['z'=16,'y'=4,'tp'=8] {'y'}, dimensions={0} | all-to-all | bytes 524288 | tf_op jit(solution)/shard_map/all_to_all | solution.py:499
  68.8 0.9 shard_map.157
  69.8 33.4 %all_to_all.27.refs_0_ = bf16[16,40,128]{2,1,0:T(8,128)(2,1)S(1)} all-to-all(bf16[16,40,128]{2,1,0:T(8,128)(2,1)S(1)} %get-tuple-element.41), channel_id=1, replica_groups=mesh['z'=16,'y'=4,'tp'=8] {'z'}, dimensions={0} | all-to-all | bytes 327680 | tf_op jit(solution)/shard_map/all_to_all | solution.py:499
  103.2 0.7 shard_map.158
  103.9 5.3 %all-to-all-start.4 = ((bf16[64,8,128]{2,1,0:T(8,128)(2,1)}), bf16[64,8,128]{2,1,0:T(8,128)(2,1)S(1)}, u32[]{:S(2)}, u32[]{:S(2)}) async-start(bf16[64,8,128]{2,1,0:T(8,128)(2,1)} %get-tuple-element.43), calls=%async_computation.4 | async-start | bytes 262144 | tf_op jit(solution)/shard_map/all_to_all | solution.py:499
  109.2 1.3 collective-permute-start.4
  110.5 4.3 %collective-permute-done.4.refs_2_ = f32[8,128]{1,0:T(8,128)S(1)} collective-permute-done((f32[8,128]{1,0:T(8,128)S(1)}, f32[8,128]{1,0:T(8,128)S(1)}, u32[]{:S(2)}, u32[]{:S(2)}) %collective-permute-start.4) | collective-permute-done | bytes 4128 | tf_op jit(solution)/shard_map/ppermute | solution.py:573
  114.9 0.6 shard_map.161
  115.5 1.9 %collective-permute-start.5 = (bf16[4,256,128]{2,1,0:T(8,128)(2,1)S(1)}, bf16[4,256,128]{2,1,0:T(8,128)(2,1)S(1)}, u32[]{:S(2)}, u32[]{:S(2)}) collective-permute-start(bf16[4,256,128]{2,1,0:T(8,128)(2,1)S(1)} %get-tuple-element.58), channel_id=1, source_target_pairs={{0,1},{1,0},{2,3},{3,2},{4,5},{5,4},{6,7},{7,6},{8,9},{9,8},{10,11... | collective-permute-start | bytes 786440 | tf_op jit(solution)/shard_map/ppermute | solution.py:602
  117.4 1.5 %collective-permute-done.5.refs_1_ = bf16[4,256,128]{2,1,0:T(8,128)(2,1)S(1)} collective-permute-done((bf16[4,256,128]{2,1,0:T(8,128)(2,1)S(1)}, bf16[4,256,128]{2,1,0:T(8,128)(2,1)S(1)}, u32[]{:S(2)}, u32[]{:S(2)}) %collective-permute-start.5) | collective-permute-done | bytes 262176 | tf_op jit(solution)/shard_map/ppermute | solution.py:602
  118.9 0.1 shard_map.162
  119.0 2.7 %collective-permute-start.6 = (bf16[2,256,128]{2,1,0:T(8,128)(2,1)S(1)}, bf16[2,256,128]{2,1,0:T(8,128)(2,1)S(1)}, u32[]{:S(2)}, u32[]{:S(2)}) collective-permute-start(bf16[2,256,128]{2,1,0:T(8,128)(2,1)S(1)} %get-tuple-element.60), channel_id=1, source_target_pairs={{0,2},{1,3},{2,0},{3,1},{4,6},{5,7},{6,4},{7,5},{8,10},{9,11},{10,... | collective-permute-start | bytes 393224 | tf_op jit(solution)/shard_map/ppermute | solution.py:604
  121.7 4.7 %collective-permute-done.6.refs_1_ = bf16[2,256,128]{2,1,0:T(8,128)(2,1)S(1)} collective-permute-done((bf16[2,256,128]{2,1,0:T(8,128)(2,1)S(1)}, bf16[2,256,128]{2,1,0:T(8,128)(2,1)S(1)}, u32[]{:S(2)}, u32[]{:S(2)}) %collective-permute-start.6) | collective-permute-done | bytes 131104 | tf_op jit(solution)/shard_map/ppermute | solution.py:604
  126.4 2.4 %collective-permute-start.7 = (bf16[1,256,128]{2,1,0:T(8,128)(2,1)S(1)}, bf16[1,256,128]{2,1,0:T(8,128)(2,1)S(1)}, u32[]{:S(2)}, u32[]{:S(2)}) collective-permute-start(bf16[1,256,128]{2,1,0:T(8,128)(2,1)S(1)} %get-tuple-element.62), channel_id=1, source_target_pairs={{0,6},{1,7},{2,4},{3,5},{4,2},{5,3},{6,0},{7,1},{8,14},{9,15},{10,... | collective-permute-start | bytes 196616 | tf_op jit(solution)/shard_map/ppermute | solution.py:606
  128.8 1.9 %shard_map.159 = (bf16[128,256]{1,0:T(8,128)(2,1)}, f32[128,128]{1,0:T(8,128)S(1)}, f32[4,128]{1,0:T(4,128)S(1)}, f32[4,128]{1,0:T(4,128)S(1)}, f32[128,256]{1,0...) custom-call(bf16[4,128,256]{2,1,0:T(8,128)(2,1)S(1)} %all_to_all.26., ...), custom_call_target="tpu_custom_call" | custom-call | flops 10000000 | bytes 1000000 | tf_op jit(solution)/shard_map/pallas_call | solution.py:58
  130.8 3.0 %collective-permute-done.7.refs_1_ = bf16[1,256,128]{2,1,0:T(8,128)(2,1)S(1)} collective-permute-done((bf16[1,256,128]{2,1,0:T(8,128)(2,1)S(1)}, bf16[1,256,128]{2,1,0:T(8,128)(2,1)S(1)}, u32[]{:S(2)}, u32[]{:S(2)}) %collective-permute-start.7) | collective-permute-done | bytes 65568 | tf_op jit(solution)/shard_map/ppermute | solution.py:606
  133.8 0.6 shard_map.164
  134.4 0.0 all-to-all-done.4.refs_0_
  134.5 1.5 %shard_map.160 = (f32[1,128]{1,0:T(1,128)}, bf16[128,128]{1,0:T(8,128)(2,1)}, f32[4,128]{1,0:T(4,128)}, bf16[128,256]{1,0:T(8,128)(2,1)}) custom-call(bf16[64,8,128]{2,1,0:T(8,128)(2,1)S(1)} %all-to-all-done.4.refs_0_, bf16[4,128,256]{2,1,0:T(8,128)(2,1)S(1)} %all_to_all.26.refs_0_.refs_1_, bf16[128,128]{1,0:T(8,128)(2,1)S(1)} %copy-done.5, ...), custom_call_target="tpu_custom_call" | custom-call | flops 10000000 | bytes 1000000 | tf_op jit(solution)/shard_map/pallas_call | solution.py:58
  (8 shorter events, 0.0 us)
Async XLA Ops:
  15.2 16.1 %copy-start.1 = (bf16[128,2048]{1,0:T(8,128)(2,1)S(1)}, bf16[128,2048]{1,0:T(8,128)(2,1)}, u32[]{:S(2)}) copy-start(bf16[128,2048]{1,0:T(8,128)(2,1)} %refs_7_.2) | copy-start | bytes 1572868
  15.2 20.2 %copy-start.5 = (bf16[128,128]{1,0:T(8,128)(2,1)S(1)}, bf16[128,128]{1,0:T(8,128)(2,1)}, u32[]{:S(2)}) copy-start(bf16[128,128]{1,0:T(8,128)(2,1)} %refs_2_.1) | copy-start | bytes 98308
  15.2 20.2 %copy-start.6 = (f32[128,4]{0,1:T(4,128)S(1)}, f32[128,4]{0,1:T(4,128)}, u32[]{:S(2)}) copy-start(f32[128,4]{0,1:T(4,128)} %param.15) | copy-start | bytes 6148
  15.2 20.2 %copy-start.7 = (f32[128,4]{0,1:T(4,128)S(1)}, f32[128,4]{0,1:T(4,128)}, u32[]{:S(2)}) copy-start(f32[128,4]{0,1:T(4,128)} %param.17) | copy-start | bytes 6148
  15.2 20.2 %copy-start.8 = (f32[4,128]{1,0:T(4,128)S(1)}, f32[4,128]{1,0:T(4,128)}, u32[]{:S(2)}) copy-start(f32[4,128]{1,0:T(4,128)} %refs_6_.6) | copy-start | bytes 6148
  15.3 20.2 %copy-start.9 = (f32[4]{0:T(128)S(1)}, f32[4]{0:T(128)}, u32[]{:S(2)}) copy-start(f32[4]{0:T(128)} %param.16) | copy-start | bytes 52
  16.0 19.5 %copy-start = (bf16[128,2048]{1,0:T(8,128)(2,1)S(1)}, bf16[128,2048]{1,0:T(8,128)(2,1)}, u32[]{:S(2)}) copy-start(bf16[128,2048]{1,0:T(8,128)(2,1)} %refs_0_.1) | copy-start | bytes 1572868
  16.0 19.5 %copy-start.3 = (bf16[128,256]{1,0:T(8,128)(2,1)S(1)}, bf16[128,256]{1,0:T(8,128)(2,1)}, u32[]{:S(2)}) copy-start(bf16[128,256]{1,0:T(8,128)(2,1)} %refs_6_.7) | copy-start | bytes 196612
  16.0 19.5 %copy-start.4 = (bf16[128,256]{1,0:T(8,128)(2,1)S(1)}, bf16[128,256]{1,0:T(8,128)(2,1)}, u32[]{:S(2)}) copy-start(bf16[128,256]{1,0:T(8,128)(2,1)} %refs_8_.3) | copy-start | bytes 196612
  16.0 43.3 %all-to-all-start.1 = ((bf16[16,40,256]{2,1,0:T(8,128)(2,1)}), bf16[16,40,256]{2,1,0:T(8,128)(2,1)S(1)}, u32[]{:S(2)}, u32[]{:S(2)}) async-start(bf16[16,40,256]{2,1,0:T(8,128)(2,1)} %shard_map.154), calls=%async_computation.1 | async-start | bytes 655360 | tf_op jit(solution)/shard_map/all_to_all | solution.py:499
  31.4 4.1 %copy-start.2 = (bf16[128,256]{1,0:T(8,128)(2,1)S(1)}, bf16[128,256]{1,0:T(8,128)(2,1)}, u32[]{:S(2)}) copy-start(bf16[128,256]{1,0:T(8,128)(2,1)} %refs_5_.5) | copy-start | bytes 196612
  31.4 4.1 %collective-permute-start = (bf16[8,2048]{1,0:T(8,128)(2,1)S(1)}, bf16[8,2048]{1,0:T(8,128)(2,1)S(1)}, u32[]{:S(2)}, u32[]{:S(2)}) collective-permute-start(bf16[8,2048]{1,0:T(8,128)(2,1)S(1)} %slice.3), channel_id=1, source_target_pairs={{0,8},{8,16},{16,24},{24,32},{32,40},{40,48},{48,56},{56,64},{64,7... | collective-permute-start | bytes 98312 | tf_op jit(solution)/shard_map/ppermute | solution.py:546
  37.6 15.8 %collective-permute-start.1 = (bf16[432,256]{1,0:T(8,128)(2,1)S(1)}, bf16[432,256]{1,0:T(8,128)(2,1)S(1)}, u32[]{:S(2)}, u32[]{:S(2)}) collective-permute-start(bf16[432,256]{1,0:T(8,128)(2,1)S(1)} %get-tuple-element.38), channel_id=1, source_target_pairs={{0,8},{8,16},{16,24},{24,0},{1,9},{9,17},{17,25},{25,1},{2,10},{10... | collective-permute-start | bytes 663560 | tf_op jit(solution)/shard_map/ppermute | solution.py:508
  41.9 14.0 %collective-permute-start.2 = (bf16[432,256]{1,0:T(8,128)(2,1)S(1)}, bf16[432,256]{1,0:T(8,128)(2,1)S(1)}, u32[]{:S(2)}, u32[]{:S(2)}) collective-permute-start(bf16[432,256]{1,0:T(8,128)(2,1)S(1)} %get-tuple-element.39), channel_id=1, source_target_pairs={{0,16},{8,24},{16,0},{24,8},{1,17},{9,25},{17,1},{25,9},{2,18},{10... | collective-permute-start | bytes 663560 | tf_op jit(solution)/shard_map/ppermute | solution.py:508
  51.5 7.8 %collective-permute-start.3 = (bf16[432,256]{1,0:T(8,128)(2,1)S(1)}, bf16[432,256]{1,0:T(8,128)(2,1)S(1)}, u32[]{:S(2)}, u32[]{:S(2)}) collective-permute-start(bf16[432,256]{1,0:T(8,128)(2,1)S(1)} %get-tuple-element.40), channel_id=1, source_target_pairs={{0,24},{8,0},{16,8},{24,16},{1,25},{9,1},{17,9},{25,17},{2,26},{10... | collective-permute-start | bytes 663560 | tf_op jit(solution)/shard_map/ppermute | solution.py:508
  103.9 30.5 %all-to-all-start.4 = ((bf16[64,8,128]{2,1,0:T(8,128)(2,1)}), bf16[64,8,128]{2,1,0:T(8,128)(2,1)S(1)}, u32[]{:S(2)}, u32[]{:S(2)}) async-start(bf16[64,8,128]{2,1,0:T(8,128)(2,1)} %get-tuple-element.43), calls=%async_computation.4 | async-start | bytes 262144 | tf_op jit(solution)/shard_map/all_to_all | solution.py:499
  109.2 5.6 %collective-permute-start.4 = (f32[8,128]{1,0:T(8,128)S(1)}, f32[8,128]{1,0:T(8,128)S(1)}, u32[]{:S(2)}, u32[]{:S(2)}) collective-permute-start(f32[8,128]{1,0:T(8,128)S(1)} %get-tuple-element.56), channel_id=1, source_target_pairs={{32,0},{64,32},{96,64},{128,96},{160,128},{192,160},{224,192},{256... | collective-permute-start | bytes 12296 | tf_op jit(solution)/shard_map/ppermute | solution.py:573
  115.5 3.4 %collective-permute-start.5 = (bf16[4,256,128]{2,1,0:T(8,128)(2,1)S(1)}, bf16[4,256,128]{2,1,0:T(8,128)(2,1)S(1)}, u32[]{:S(2)}, u32[]{:S(2)}) collective-permute-start(bf16[4,256,128]{2,1,0:T(8,128)(2,1)S(1)} %get-tuple-element.58), channel_id=1, source_target_pairs={{0,1},{1,0},{2,3},{3,2},{4,5},{5,4},{6,7},{7,6},{8,9},{9,8},{10,11... | collective-permute-start | bytes 786440 | tf_op jit(solution)/shard_map/ppermute | solution.py:602
  119.0 7.4 %collective-permute-start.6 = (bf16[2,256,128]{2,1,0:T(8,128)(2,1)S(1)}, bf16[2,256,128]{2,1,0:T(8,128)(2,1)S(1)}, u32[]{:S(2)}, u32[]{:S(2)}) collective-permute-start(bf16[2,256,128]{2,1,0:T(8,128)(2,1)S(1)} %get-tuple-element.60), channel_id=1, source_target_pairs={{0,2},{1,3},{2,0},{3,1},{4,6},{5,7},{6,4},{7,5},{8,10},{9,11},{10,... | collective-permute-start | bytes 393224 | tf_op jit(solution)/shard_map/ppermute | solution.py:604
  126.4 7.4 %collective-permute-start.7 = (bf16[1,256,128]{2,1,0:T(8,128)(2,1)S(1)}, bf16[1,256,128]{2,1,0:T(8,128)(2,1)S(1)}, u32[]{:S(2)}, u32[]{:S(2)}) collective-permute-start(bf16[1,256,128]{2,1,0:T(8,128)(2,1)S(1)} %get-tuple-element.62), channel_id=1, source_target_pairs={{0,6},{1,7},{2,4},{3,5},{4,2},{5,3},{6,0},{7,1},{8,14},{9,15},{10,... | collective-permute-start | bytes 196616 | tf_op jit(solution)/shard_map/ppermute | solution.py:606
